TPU v7x, 256 devices: a whole 4x4x8 slice. The times are simulated.
256 devices in a mesh: sp: 64 (over z, x, core), tp: 4 (over y).
Axes of the slice: x: 4, y: 4, z: 8, core: 2. Of those that a mesh axis runs over, the one named last changes fastest.
Arguments:
- stratum_source_matrix: bfloat16 [8192, 2048], P('sp'), may hold values from -70 to 70
- acceptance_query: bfloat16 [2, 8192, 1024], P(None, 'sp', 'tp'), may hold values from -6 to 6
- cluster_lookup_matrix: bfloat16 [2, 8192, 1024], P(None, 'sp', 'tp'), may hold values from -6 to 6
- cluster_payload_matrix: bfloat16 [2, 8192, 1024], P(None, 'sp', 'tp'), may hold values from -6 to 6
- fading_logit: bfloat16 [2, 8192, 1024], P(None, 'sp', 'tp'), may hold values from -17 to 2
- adaptation_speed_logit: bfloat16 [2, 8192, 1024], P(None, 'sp', 'tp'), may hold values from -14 to 5
- additional_fading_exponent: float32 [2, 8192, 1024], P(None, 'sp', 'tp'), may hold values from -0.7 to 0
- result_switch_pair: bfloat16 [2, 8192, 1024], P(None, 'sp', 'tp'), may hold values from -6 to 6
- attender_scaling_factor: float32 [2, 1024], P(None, 'tp'), may hold values from 0.1 to 1.9
- present_item_factor: float32 [2, 1024], P(None, 'tp'), may hold values from -0.9 to 0.9
- final_mapping_matrix: bfloat16 [2, 1024, 2048], P(None, 'tp'), may hold values from -0.125 to 0.125
- perceptron_scaling_factor: float32 [2048], replicated, may hold values from 0.1 to 1.9
- switching_matrix: bfloat16 [2048, 5632], P('sp', 'tp'), may hold values from -0.125 to 0.125
- widening_matrix: bfloat16 [2048, 5632], P('sp', 'tp'), may hold values from -0.125 to 0.125
- shrinking_matrix: bfloat16 [5632, 2048], P('tp', 'sp'), may hold values from -0.078125 to 0.078125
Outputs:
- layer_out: bfloat16 [8192, 2048], P('sp', 'tp')
All inputs are finite; a program needn't handle non-finite values.
Results may differ from a plain program's by a relative error of at most 0.014.
Values may be sent and summed in bfloat16 or wider, within the bound.
No kernel may reach another device: no remote copies, remote signals or barrier semaphores. Data moves between devices by JAX's collectives and lax.ppermute only.
A program may use at most 128 MiB of HBM per device.

v0:
```python
import jax
import jax.numpy as jnp
from jax import lax
from jax.sharding import Mesh
from jax.sharding import PartitionSpec as P

DS = 64
DL = 128
BLOCK = 64
SP = ("sp_0", "sp_1", "sp_2")


highest = lax.Precision.HIGHEST
norm_epsilon = 1e-06
head_epsilon = 0.00064
key_epsilon = 1e-06


def side_by_side(arrays, axis, dim, along):
    widths = [a.shape[along] for a in arrays]
    both = jnp.concatenate(arrays, axis=along)
    out = lax.all_gather(both, axis, axis=dim, tiled=True)
    return tuple(jnp.split(out, [sum(widths[:k]) for k in range(1, len(widths))], axis=along))


def filled_with(value, identity):
    return jax.tree.map(
        lambda part, zero: jnp.zeros_like(part) + jnp.asarray(zero, part.dtype), value, identity
    )


def prefix_by_axis(value, axes, combine, identity):
    before = start = filled_with(value, identity)
    so_far = value
    for axis in reversed(axes):
        devices, position = (lax.axis_size(axis), lax.axis_index(axis))
        pieces = jax.tree.map(
            lambda part, kind: lax.all_gather(part.astype(kind), axis),
            so_far,
            jax.tree.map(lambda a: jnp.bfloat16 if a.dtype == jnp.float32 else a.dtype, value),
        )
        inside, so_far = (start, start)
        for k in range(devices):
            passed = k < position
            so_far = combine(
                so_far, jax.tree.map(lambda part, own: part[k].astype(own.dtype), pieces, value)
            )
            inside = jax.tree.map(lambda new, old: jnp.where(passed, new, old), so_far, inside)
        before = combine(inside, before)
    return before


def from_everyone(value, axis):
    devices = lax.axis_size(axis)
    return lax.all_to_all(
        jnp.broadcast_to(value[None], (devices, *value.shape)), axis, 0, 0, tiled=True
    )


def of_everyone(value, axis):
    everything = from_everyone(value, axis)
    return jnp.sum(everything.astype(jnp.float32), axis=0)


def split_up(value, dim, devices):
    dims = value.shape
    tiles = value.reshape(*dims[:dim], devices, dims[dim] // devices, *dims[dim + 1 :])
    return jnp.moveaxis(tiles, dim, 0)


def sum_at_owner(value, axis, dim):
    tiles = split_up(value, dim, lax.axis_size(axis))
    arrived = lax.all_to_all(tiles, axis, split_axis=0, concat_axis=0, tiled=True)
    return arrived.astype(jnp.float32).sum(axis=0)


def per_head_terms(
    acceptance_query,
    cluster_lookup_matrix,
    cluster_payload_matrix,
    fading_logit,
    adaptation_speed_logit,
    additional_fading_exponent,
    attender_feature_count,
):
    row_count, channels = acceptance_query.shape
    lattice_layout = (row_count, channels // attender_feature_count, attender_feature_count)
    acceptance_lines = acceptance_query.astype(jnp.float32).reshape(lattice_layout)
    mapped_lookups = cluster_lookup_matrix.astype(jnp.float32).reshape(lattice_layout)
    mapped_payloads = cluster_payload_matrix.astype(jnp.float32).reshape(lattice_layout)
    learning_rate_logarithm = -jax.nn.softplus(-fading_logit.astype(jnp.float32)) - 0.5
    decay_logarithm = (additional_fading_exponent - jnp.exp(learning_rate_logarithm)).reshape(
        lattice_layout
    )
    learn_rate = jax.nn.sigmoid(adaptation_speed_logit.astype(jnp.float32)).reshape(lattice_layout)
    removal = mapped_lookups * lax.rsqrt(
        jnp.sum(mapped_lookups * mapped_lookups, axis=-1, keepdims=True) + key_epsilon
    )
    return (
        acceptance_lines,
        mapped_lookups,
        mapped_payloads,
        decay_logarithm,
        -removal,
        learn_rate * removal,
    )


def entire_cluster(
    raw_retrieval,
    acceptance_lines,
    mapped_lookups,
    mapped_payloads,
    scaling_array,
    diagonal_reward_array,
    switch_amounts,
):
    row_count, attender_count, attender_feature_count = raw_retrieval.shape
    row_mean = jnp.mean(raw_retrieval, axis=-1, keepdims=True)
    centered = raw_retrieval - row_mean
    variance = jnp.mean(centered * centered, axis=-1, keepdims=True)
    normed = (
        centered
        * lax.rsqrt(variance + head_epsilon)
        * scaling_array.reshape(attender_count, attender_feature_count)
    )
    diagonal_item_contribution = (
        jnp.sum(
            acceptance_lines
            * mapped_lookups
            * diagonal_reward_array.reshape(attender_count, attender_feature_count),
            axis=-1,
            keepdims=True,
        )
        * mapped_payloads
    )
    joined = (normed + diagonal_item_contribution).reshape(
        row_count, attender_count * attender_feature_count
    )
    return (joined * switch_amounts.astype(jnp.float32)).astype(jnp.bfloat16)


def to_blocks(array_in):
    row_count, attender_count, attender_feature_count = array_in.shape
    return array_in.reshape(
        row_count // BLOCK, BLOCK, attender_count, attender_feature_count
    ).transpose(0, 2, 1, 3)


def block_pieces(
    acceptance_lines, mapped_lookups, mapped_payloads, decay_logarithm, remove_left, remove_right
):
    (
        acceptance_lines,
        mapped_lookups,
        mapped_payloads,
        decay_logarithm,
        remove_left,
        remove_right,
    ) = [
        to_blocks(array_in)
        for array_in in (
            acceptance_lines,
            mapped_lookups,
            mapped_payloads,
            decay_logarithm,
            remove_left,
            remove_right,
        )
    ]
    attender_feature_count = acceptance_lines.shape[3]
    places = jnp.arange(BLOCK)
    inclusive = places[:, None] >= places[None, :]
    strict = places[:, None] > places[None, :]
    lower_ones = inclusive.astype(jnp.float32)
    cumulative = jnp.einsum("ts,nhsj->nhtj", lower_ones, decay_logarithm, precision=highest)
    middle = cumulative[:, :, BLOCK // 2 : BLOCK // 2 + 1, :]
    forward = jnp.exp(cumulative - middle)
    backward = jnp.exp(middle - cumulative)
    queries = jnp.concatenate(
        [remove_left * jnp.exp(-decay_logarithm) * forward, acceptance_lines * forward], axis=2
    )
    sources = jnp.concatenate([remove_right * backward, mapped_lookups * backward], axis=2)
    pair_terms = jnp.einsum("nhtj,nhsj->nhts", queries, sources, precision=highest)
    remove_remove = jnp.where(strict, pair_terms[:, :, :BLOCK, :BLOCK], 0.0)
    remove_key = jnp.where(strict, pair_terms[:, :, :BLOCK, BLOCK:], 0.0)
    read_remove = jnp.where(inclusive, pair_terms[:, :, BLOCK:, :BLOCK], 0.0)
    read_key = jnp.where(inclusive, pair_terms[:, :, BLOCK:, BLOCK:], 0.0)
    eye_block = jnp.eye(BLOCK, dtype=jnp.float32)
    targets = jnp.concatenate(
        [
            jnp.einsum("nhts,nhsj->nhtj", remove_key, mapped_payloads, precision=highest),
            remove_left * jnp.exp(cumulative - decay_logarithm),
        ],
        axis=-1,
    )
    solved = jax.scipy.linalg.solve_triangular(
        eye_block - remove_remove, targets, lower=True, unit_diagonal=True
    )
    carried_part = solved[..., :attender_feature_count]
    start_part = solved[..., attender_feature_count:]
    local_out = jnp.einsum(
        "nhts,nhsj->nhtj", read_remove, carried_part, precision=highest
    ) + jnp.einsum("nhts,nhsj->nhtj", read_key, mapped_payloads, precision=highest)
    start_read = acceptance_lines * jnp.exp(cumulative) + jnp.einsum(
        "nhts,nhsj->nhtj", read_remove, start_part, precision=highest
    )
    final_log = cumulative[:, :, BLOCK - 1 :, :]
    tail_decay = jnp.exp(final_log - cumulative)
    transit = jnp.einsum(
        "nhsi,nhsj->nhij", start_part, remove_right * tail_decay, precision=highest
    ) + jnp.eye(attender_feature_count, dtype=jnp.float32) * jnp.exp(final_log)
    added = jnp.einsum(
        "nhsi,nhsj->nhij",
        jnp.concatenate([carried_part, mapped_payloads], axis=2),
        jnp.concatenate([remove_right * tail_decay, mapped_lookups * tail_decay], axis=2),
        precision=highest,
    )
    return (local_out, start_read, transit, added)


def join_pair(earlier, later):
    return (
        jnp.einsum("hik,hkj->hij", earlier[0], later[0], precision=highest),
        jnp.einsum("hik,hkj->hij", earlier[1], later[0], precision=highest) + later[1],
    )


def join_groups(earlier, later):
    return (join_pair(earlier[0], later[0]), join_pair(earlier[1], later[1]))


def block_prefix(transit, added):
    attender_count, attender_feature_count = (transit.shape[1], transit.shape[2])
    identity_block = jnp.broadcast_to(
        jnp.eye(attender_feature_count, dtype=jnp.float32),
        (attender_count, attender_feature_count, attender_feature_count),
    )

    def advance(carried, pieces):
        return (join_pair(carried, pieces), carried)

    totals, prefixes = lax.scan(
        advance, (identity_block, jnp.zeros_like(identity_block)), (transit, added)
    )
    return (totals, prefixes)


def on_device(
    stratum_source_matrix,
    acceptance_query,
    cluster_lookup_matrix,
    cluster_payload_matrix,
    fading_logit,
    adaptation_speed_logit,
    additional_fading_exponent,
    result_switch_pair,
    attender_scaling_factor,
    present_item_factor,
    final_mapping_matrix,
    perceptron_scaling_factor,
    switching_matrix,
    widening_matrix,
    shrinking_matrix,
):
    gate_whole, up_whole = side_by_side((switching_matrix, widening_matrix), SP, 0, 1)
    group_widths = (DS, DL)
    group_terms, group_pieces, group_totals, group_prefixes, identities = ([], [], [], [], [])
    for cluster_ordinal in range(2):
        aggregated_contributions = per_head_terms(
            acceptance_query[cluster_ordinal],
            cluster_lookup_matrix[cluster_ordinal],
            cluster_payload_matrix[cluster_ordinal],
            fading_logit[cluster_ordinal],
            adaptation_speed_logit[cluster_ordinal],
            additional_fading_exponent[cluster_ordinal],
            group_widths[cluster_ordinal],
        )
        local_out, start_read, transit, added = block_pieces(*aggregated_contributions)
        totals, prefixes = block_prefix(transit, added)
        group_terms.append(aggregated_contributions)
        group_pieces.append((local_out, start_read))
        group_totals.append(totals)
        group_prefixes.append(prefixes)
        identities.append(
            (
                jnp.broadcast_to(
                    jnp.eye(group_widths[cluster_ordinal], dtype=jnp.float32), totals[0].shape
                ),
                jnp.zeros_like(totals[1]),
            )
        )
    starts = prefix_by_axis(
        (group_totals[0], group_totals[1]), SP, join_groups, (identities[0], identities[1])
    )
    mixed_groups = []
    for cluster_ordinal in range(2):
        acceptance_lines, mapped_lookups, mapped_payloads = (
            group_terms[cluster_ordinal][0],
            group_terms[cluster_ordinal][1],
            group_terms[cluster_ordinal][2],
        )
        row_count, attender_count, attender_feature_count = acceptance_lines.shape
        local_out, start_read = group_pieces[cluster_ordinal]
        prefix_transit, prefix_added = group_prefixes[cluster_ordinal]
        block_start = (
            jnp.einsum(
                "hik,nhkj->nhij", starts[cluster_ordinal][1], prefix_transit, precision=highest
            )
            + prefix_added
        )
        raw_retrieval = local_out + jnp.einsum(
            "nhtj,nhij->nhti", start_read, block_start, precision=highest
        )
        raw_retrieval = raw_retrieval.transpose(0, 2, 1, 3).reshape(
            row_count, attender_count, attender_feature_count
        )
        mixed_groups.append(
            entire_cluster(
                raw_retrieval,
                acceptance_lines,
                mapped_lookups,
                mapped_payloads,
                attender_scaling_factor[cluster_ordinal],
                present_item_factor[cluster_ordinal],
                result_switch_pair[cluster_ordinal],
            )
        )
    blended_result = jnp.concatenate(mixed_groups, axis=1)
    partial_value = jnp.dot(
        blended_result,
        final_mapping_matrix.reshape(-1, final_mapping_matrix.shape[2]),
        preferred_element_type=jnp.float32,
    )
    columns = perceptron_scaling_factor.shape[0] // lax.axis_size("tp")
    own_start = lax.axis_index("tp") * columns
    residual_float = stratum_source_matrix.astype(jnp.float32)
    attention = of_everyone(partial_value.astype(jnp.bfloat16), "tp").astype(jnp.float32)
    state_float = (residual_float + attention).astype(jnp.bfloat16).astype(jnp.float32)
    mean_square = jnp.mean(state_float * state_float, axis=1, keepdims=True)
    normed = (
        state_float * lax.rsqrt(mean_square + norm_epsilon) * perceptron_scaling_factor
    ).astype(jnp.bfloat16)
    own_state = lax.dynamic_slice_in_dim(state_float, own_start, columns, 1)
    gate_pre = jnp.dot(normed, gate_whole, preferred_element_type=jnp.float32)
    up_pre = jnp.dot(normed, up_whole, preferred_element_type=jnp.float32)
    activated = (jax.nn.silu(gate_pre) * up_pre).astype(jnp.bfloat16)
    down_terms = jnp.dot(
        activated,
        lax.all_gather(shrinking_matrix, SP, axis=1, tiled=True),
        preferred_element_type=jnp.float32,
    )
    mixer = sum_at_owner(down_terms.astype(jnp.bfloat16), "tp", 1)
    return (own_state + mixer).astype(jnp.bfloat16)


def solution(mesh):
    split = Mesh(mesh.devices.reshape(8, 4, 2, mesh.shape["tp"]), ("sp_0", "sp_1", "sp_2", "tp"))
    return jax.shard_map(
        on_device,
        mesh=split,
        in_specs=(
            P(SP, None),
            P(None, SP, "tp"),
            P(None, SP, "tp"),
            P(None, SP, "tp"),
            P(None, SP, "tp"),
            P(None, SP, "tp"),
            P(None, SP, "tp"),
            P(None, SP, "tp"),
            P(None, "tp"),
            P(None, "tp"),
            P(None, "tp", None),
            P(),
            P(SP, "tp"),
            P(SP, "tp"),
            P("tp", SP),
        ),
        out_specs=P(SP, "tp"),
        check_vma=False,
    )
```

profile of v0, /device:TPU:2, one launch (start us, length us, event | category | flops | bytes accessed | tf_op | source)
XLA Modules:
  0.0 384.9 jit_solution(7021839164730229028)
XLA Ops:
  6.5 1.8 pad_maximum_fusion
  15.3 1.6 fusion.319
  18.4 1.6 add_divide_fusion.1
  22.5 1.6 bitcast_multiply_fusion.12
  25.0 20.3 %custom-call.9 = f32[2,2,1,64,64]{3,4,2,1,0:T(8,128)} custom-call(f32[2,2,1,64,64]{4,3,2,1,0:T(8,128)S(1)} %fusion.118), custom_call_target="InvertDiagBlocksLowerTriangular" | custom-call | tf_op jit(solution)/shard_map/jit(_solve_triangular)/vmap(vmap())/triangular_solve | solution.py:197
  50.6 1.6 fusion.92
  53.0 3.2 while.35
  56.3 1.9 all-gather.6
  58.7 13.4 %all-gather.7 = bf16[8,128,128]{2,1,0:T(8,128)(2,1)S(1)} all-gather(bf16[2,128,128]{2,1,0:T(8,128)(2,1)S(1)} %get-tuple-element.303), channel_id=9, replica_groups=mesh['sp_0'=8,'sp_1'=4,'sp_2'=2,'tp'=4] {'sp_1'}, dimensions={0}, use_global_device_ids=true | all-gather | bytes 327680 | tf_op jit(solution)/shard_map/all_gather | solution.py:38
  72.2 2.0 all-gather.9
  75.2 13.4 %all-gather.10 = bf16[8,128,128]{2,1,0:T(8,128)(2,1)S(1)} all-gather(bf16[2,128,128]{2,1,0:T(8,128)(2,1)S(1)} %get-tuple-element.301), channel_id=12, replica_groups=mesh['sp_0'=8,'sp_1'=4,'sp_2'=2,'tp'=4] {'sp_1'}, dimensions={0}, use_global_device_ids=true | all-gather | bytes 327680 | tf_op jit(solution)/shard_map/all_gather | solution.py:38
  92.5 29.4 %all-gather.8 = bf16[16,128,128]{2,1,0:T(8,128)(2,1)S(1)} all-gather(bf16[2,128,128]{2,1,0:T(8,128)(2,1)S(1)} %get-tuple-element.307), channel_id=10, replica_groups=mesh['sp_0'=8,'sp_1'=4,'sp_2'=2,'tp'=4] {'sp_0'}, dimensions={0}, use_global_device_ids=true | all-gather | bytes 589824 | tf_op jit(solution)/shard_map/all_gather | solution.py:38
  121.9 25.4 %all-gather.11 = bf16[16,128,128]{2,1,0:T(8,128)(2,1)S(1)} all-gather(bf16[2,128,128]{2,1,0:T(8,128)(2,1)S(1)} %get-tuple-element.305), channel_id=13, replica_groups=mesh['sp_0'=8,'sp_1'=4,'sp_2'=2,'tp'=4] {'sp_0'}, dimensions={0}, use_global_device_ids=true | all-gather | bytes 589824 | tf_op jit(solution)/shard_map/all_gather | solution.py:38
  170.7 2.4 bitcast_multiply_fusion.2
  179.3 40.7 %custom-call.8 = f32[2,4,1,64,64]{3,4,2,1,0:T(8,128)} custom-call(f32[2,4,1,64,64]{4,3,2,1,0:T(8,128)} %fusion.70), custom_call_target="InvertDiagBlocksLowerTriangular" | custom-call | tf_op jit(solution)/shard_map/jit(_solve_triangular)/vmap(vmap())/triangular_solve | solution.py:197
  219.9 2.3 fusion.52
  222.3 1.7 convolution_add_fusion.2
  223.9 2.4 fusion.56
  226.4 5.0 %while.34 = (s32[]{:T(128)}, f32[4,64,64]{1,2,0:T(8,128)S(1)}, f32[4,64,64]{1,2,0:T(8,128)S(1)}, f32[2,4,64,64]{2,3,1,0:T(8,128)}, f32[2,4,64,64]{2,3,1,0:T(8,12...) while((s32[]{:T(128)}, f32[4,64,64]{1,2,0:T(8,128)S(1)}, ...), condition=%wide.region_2.3_spmd.clone, body=%wide.region_1.2_spmd.clone.sunk | while | flops 25214980 | bytes 1443436 | solution.py:243
  231.4 1.9 all-gather
  234.4 12.5 %all-gather.1 = bf16[16,64,64]{2,1,0:T(8,128)(2,1)S(1)} all-gather(bf16[4,64,64]{2,1,0:T(8,128)(2,1)S(1)} %get-tuple-element.293), channel_id=3, replica_groups=mesh['sp_0'=8,'sp_1'=4,'sp_2'=2,'tp'=4] {'sp_1'}, dimensions={0}, use_global_device_ids=true | all-gather | bytes 163840 | tf_op jit(solution)/shard_map/all_gather | solution.py:38
  247.0 2.0 all-gather.3
  251.2 12.6 %all-gather.4 = bf16[16,64,64]{2,1,0:T(8,128)(2,1)S(1)} all-gather(bf16[4,64,64]{2,1,0:T(8,128)(2,1)S(1)} %get-tuple-element.291), channel_id=6, replica_groups=mesh['sp_0'=8,'sp_1'=4,'sp_2'=2,'tp'=4] {'sp_1'}, dimensions={0}, use_global_device_ids=true | all-gather | bytes 163840 | tf_op jit(solution)/shard_map/all_gather | solution.py:38
  264.5 25.9 %all-gather.2 = bf16[32,64,64]{2,1,0:T(8,128)(2,1)S(1)} all-gather(bf16[4,64,64]{2,1,0:T(8,128)(2,1)S(1)} %get-tuple-element.297), channel_id=4, replica_groups=mesh['sp_0'=8,'sp_1'=4,'sp_2'=2,'tp'=4] {'sp_0'}, dimensions={0}, use_global_device_ids=true | all-gather | bytes 294912 | tf_op jit(solution)/shard_map/all_gather | solution.py:38
  291.3 25.3 %all-gather.5 = bf16[32,64,64]{2,1,0:T(8,128)(2,1)S(1)} all-gather(bf16[4,64,64]{2,1,0:T(8,128)(2,1)S(1)} %get-tuple-element.295), channel_id=7, replica_groups=mesh['sp_0'=8,'sp_1'=4,'sp_2'=2,'tp'=4] {'sp_0'}, dimensions={0}, use_global_device_ids=true | all-gather | bytes 294912 | tf_op jit(solution)/shard_map/all_gather | solution.py:38
  327.9 21.2 %all_to_all.10 = bf16[4,128,2048]{2,1,0:T(8,128)(2,1)S(1)} all-to-all(bf16[4,128,2048]{2,1,0:T(8,128)(2,1)S(1)} %broadcast_in_dim.122), channel_id=1, replica_groups=mesh['sp_0'=8,'sp_1'=4,'sp_2'=2,'tp'=4] {'tp'}, dimensions={0} | all-to-all | bytes 4194304 | tf_op jit(solution)/shard_map/all_to_all | solution.py:55
  349.8 4.9 %fusion.26 = f32[128,1408]{1,0:T(8,128)} fusion(bf16[2048,2816]{1,0:T(8,128)(2,1)} %all-gather.15.cloned.1.call-done, f32[128,2048]{1,0:T(8,128)S(1)} %get-tuple-element.243, f32[2048]{0:T(1024)S(1)} %copy-done.28, f32[128]{0:T(128)S(1)} %add_rsqrt_fusion.4), kind=kOutput, calls=%fused_computation.34 | convolution fusion | flops 738983936 | bytes 7545344 | tf_op jit(solution)/shard_map/dot_general | solution.py:345
  354.6 8.2 %convolution_convert_fusion.1 = bf16[128,2048]{1,0:T(8,128)(2,1)} fusion(bf16[1408,2048]{0,1:T(8,128)(2,1)} %all-gather.17.cloned.1.call-done, bf16[2048,2816]{1,0:T(8,128)(2,1)} %all-gather.15.cloned.1.call-done, f32[128,1408]{1,0:T(8,128)} %fusion.26, f32[128,2048]{1,0:T(8,128)S(1)} %get-tuple-element.243, f32[2048]{0:T(1024)S(1)} %copy-done.28, ...), kind=kOutput, calls=%fused_computation.40 | convolution fusion | flops 1478524928 | bytes 13836800 | tf_op jit(solution)/shard_map/dot_general | solution.py:348
  362.9 1.9 copy.448
  364.8 3.5 all-to-all-start.1
  368.3 8.0 %all-to-all-done.1 = bf16[4,128,512]{2,1,0:T(8,128)(2,1)S(1)} async-done(((bf16[4,128,512]{2,1,0:T(8,128)(2,1)}), bf16[4,128,512]{2,1,0:T(8,128)(2,1)S(1)}, u32[]{:S(2)}, u32[]{:S(2)}) %all-to-all-start.1) | async-done | bytes 524320 | tf_op jit(solution)/shard_map/all_to_all | solution.py:73
  376.4 1.7 add_convert_fusion.1
  (244 shorter events, 77.0 us)
Async XLA Ops:
  6.5 320.6 %copy-start = (bf16[2,256,2048]{2,1,0:T(8,128)(2,1)S(1)}, bf16[2,256,2048]{2,1,0:T(8,128)(2,1)}, u32[]{:S(2)}) copy-start(bf16[2,256,2048]{2,1,0:T(8,128)(2,1)} %param.29) | copy-start | bytes 6291460
  6.5 343.2 %all-gather.15.cloned.1.call-start = ((), (), s32[]{:S(2)}) async-start(), calls=%async_computation.2 | async-start | bytes 11714560 | tf_op jit(solution)/shard_map/all_gather | solution.py:22
  8.3 346.3 %all-gather.17.cloned.1.call-start = ((), (), s32[]{:S(2)}) async-start(), calls=%async_computation.3 | async-start | bytes 5857280 | tf_op jit(solution)/shard_map/all_gather | solution.py:350
  20.3 25.1 %copy-start.24 = (pred[64,64]{1,0:T(8,128)(4,1)}, pred[64,64]{1,0:T(8,128)(4,1)S(1)}, u32[]{:S(2)}) copy-start(pred[64,64]{1,0:T(8,128)(4,1)S(1)} %get-tuple-element.312) | copy-start | bytes 12292
  21.8 27.5 %copy-start.13 = (bf16[2,64,2,128]{3,2,1,0:T(2,128)(2,1)}, bf16[2,64,2,128]{3,2,1,0:T(2,128)(2,1)S(1)}, u32[]{:S(2)}) copy-start(bf16[2,64,2,128]{3,2,1,0:T(2,128)(2,1)S(1)} %reshape_reshape.5) | copy-start | bytes 196612
  74.4 14.5 %copy-start.11 = (f32[2,128,128]{2,1,0:T(8,128)}, f32[2,128,128]{2,1,0:T(8,128)S(1)}, u32[]{:S(2)}) copy-start(f32[2,128,128]{2,1,0:T(8,128)S(1)} %convolution_add_fusion.17) | copy-start | bytes 393220
  147.4 1.3 copy-start.5
  147.6 0.6 copy-start.10
  148.7 0.6 copy-start.9
  152.6 17.1 %copy-start.14 = (f32[1,128,256]{2,1,0:T(8,128)S(1)}, f32[1,128,256]{2,1,0:T(8,128)}, u32[]{:S(2)}) copy-start(f32[1,128,256]{2,1,0:T(8,128)} %get-tuple-element.272) | copy-start | bytes 393220
  158.5 17.2 %copy-start.23 = (bf16[1,128,256]{2,1,0:T(8,128)(2,1)S(1)}, bf16[1,128,256]{2,1,0:T(8,128)(2,1)}, u32[]{:S(2)}) copy-start(bf16[1,128,256]{2,1,0:T(8,128)(2,1)} %get-tuple-element.270) | copy-start | bytes 196612
  162.2 10.9 %copy-start.3 = (f32[2,64,4,64]{1,0,3,2:T(2,128)}, f32[2,64,4,64]{1,0,3,2:T(2,128)S(1)}, u32[]{:S(2)}) copy-start(f32[2,64,4,64]{1,0,3,2:T(2,128)S(1)} %reshape.497) | copy-start | bytes 393220
  168.5 53.8 %copy-start.1 = (f32[2,4,64,64]{2,3,1,0:T(8,128)}, f32[2,4,64,64]{2,3,1,0:T(8,128)S(1)}, u32[]{:S(2)}) copy-start(f32[2,4,64,64]{2,3,1,0:T(8,128)S(1)} %convolution_bitcast_fusion.6) | copy-start | bytes 393220
  169.6 52.7 %copy-start.25 = (f32[2,4,64]{2,1,0:T(4,128)S(1)}, f32[2,4,64]{2,1,0:T(4,128)}, u32[]{:S(2)}) copy-start(f32[2,4,64]{2,1,0:T(4,128)} %get-tuple-element.211) | copy-start | bytes 6148
  175.8 44.1 %copy-start.6 = (bf16[2,64,4,64]{3,2,1,0:T(4,128)(2,1)}, bf16[2,64,4,64]{3,2,1,0:T(4,128)(2,1)S(1)}, u32[]{:S(2)}) copy-start(bf16[2,64,4,64]{3,2,1,0:T(4,128)(2,1)S(1)} %reshape_reshape.4) | copy-start | bytes 196612
  233.3 1.0 copy-start.12
  247.0 71.0 %copy-start.15 = (f32[4,64,64]{2,1,0:T(8,128)S(1)}, f32[4,64,64]{2,1,0:T(8,128)}, u32[]{:S(2)}) copy-start(f32[4,64,64]{2,1,0:T(8,128)} %get-tuple-element.294) | copy-start | bytes 196612
  263.9 56.3 %copy-start.20 = (f32[2,4,64,64]{2,3,1,0:T(8,128)S(1)}, f32[2,4,64,64]{2,3,1,0:T(8,128)}, u32[]{:S(2)}) copy-start(f32[2,4,64,64]{2,3,1,0:T(8,128)} %get-tuple-element.85) | copy-start | bytes 393220
  263.9 56.3 %copy-start.21 = (f32[2,4,64,64]{2,3,1,0:T(8,128)S(1)}, f32[2,4,64,64]{2,3,1,0:T(8,128)}, u32[]{:S(2)}) copy-start(f32[2,4,64,64]{2,3,1,0:T(8,128)} %get-tuple-element.88) | copy-start | bytes 393220
  264.5 56.1 %copy-start.7 = (bf16[2,64,4,64]{3,2,1,0:T(4,128)(2,1)S(1)}, bf16[2,64,4,64]{3,2,1,0:T(4,128)(2,1)}, u32[]{:S(2)}) copy-start(bf16[2,64,4,64]{3,2,1,0:T(4,128)(2,1)} %copy-done.6) | copy-start | bytes 196612
  290.6 30.5 %copy-start.2 = (f32[2,4,64,64]{2,3,1,0:T(8,128)S(1)}, f32[2,4,64,64]{2,3,1,0:T(8,128)}, u32[]{:S(2)}) copy-start(f32[2,4,64,64]{2,3,1,0:T(8,128)} %copy-done.1) | copy-start | bytes 393220
  290.6 30.5 %copy-start.4 = (f32[2,64,4,64]{1,0,3,2:T(2,128)S(1)}, f32[2,64,4,64]{1,0,3,2:T(2,128)}, u32[]{:S(2)}) copy-start(f32[2,64,4,64]{1,0,3,2:T(2,128)} %copy-done.3) | copy-start | bytes 393220
  318.0 5.4 %copy-start.26 = (f32[2,256]{1,0:T(2,128)S(1)}, f32[2,256]{1,0:T(2,128)}, u32[]{:S(2)}) copy-start(f32[2,256]{1,0:T(2,128)} %param.28) | copy-start | bytes 6148
  318.3 6.3 %copy-start.16 = (f32[1,128,256]{2,1,0:T(8,128)S(1)}, f32[1,128,256]{2,1,0:T(8,128)}, u32[]{:S(2)}) copy-start(f32[1,128,256]{2,1,0:T(8,128)} %get-tuple-element.284) | copy-start | bytes 393220
  318.3 6.4 %copy-start.27 = (f32[2,256]{1,0:T(2,128)S(1)}, f32[2,256]{1,0:T(2,128)}, u32[]{:S(2)}) copy-start(f32[2,256]{1,0:T(2,128)} %param.27) | copy-start | bytes 6148
  318.6 7.4 %copy-start.22 = (f32[2,64,2]{2,1,0:T(8,128)S(1)}, f32[2,64,2]{2,1,0:T(8,128)}, u32[]{:S(2)}) copy-start(f32[2,64,2]{2,1,0:T(8,128)} %copy.347) | copy-start | bytes 3076
  318.8 7.4 %copy-start.18 = (bf16[2,128,256]{2,1,0:T(8,128)(2,1)S(1)}, bf16[2,128,256]{2,1,0:T(8,128)(2,1)}, u32[]{:S(2)}) copy-start(bf16[2,128,256]{2,1,0:T(8,128)(2,1)} %param.22) | copy-start | bytes 393220
  318.8 7.4 %copy-start.19 = (f32[2,64,2,128]{3,2,1,0:T(2,128)S(1)}, f32[2,64,2,128]{3,2,1,0:T(2,128)}, u32[]{:S(2)}) copy-start(f32[2,64,2,128]{3,2,1,0:T(2,128)} %copy.316) | copy-start | bytes 393220
  327.1 22.3 %copy-start.17 = (bf16[128,2048]{1,0:T(8,128)(2,1)S(1)}, bf16[128,2048]{1,0:T(8,128)(2,1)}, u32[]{:S(2)}) copy-start(bf16[128,2048]{1,0:T(8,128)(2,1)} %param.19) | copy-start | bytes 1572868
  327.6 22.1 %copy-start.28 = (f32[2048]{0:T(1024)S(1)}, f32[2048]{0:T(1024)}, u32[]{:S(2)}) copy-start(f32[2048]{0:T(1024)} %param.30) | copy-start | bytes 24580
  349.7 13.2 %copy-start.8 = (f32[128,2048]{1,0:T(8,128)}, f32[128,2048]{1,0:T(8,128)S(1)}, u32[]{:S(2)}) copy-start(f32[128,2048]{1,0:T(8,128)S(1)} %get-tuple-element.243) | copy-start | bytes 3145732
  364.8 11.5 %all-to-all-start.1 = ((bf16[4,128,512]{2,1,0:T(8,128)(2,1)}), bf16[4,128,512]{2,1,0:T(8,128)(2,1)S(1)}, u32[]{:S(2)}, u32[]{:S(2)}) async-start(bf16[4,128,512]{2,1,0:T(8,128)(2,1)} %bitcast.256), calls=%async_computation.1 | async-start | bytes 1048576 | tf_op jit(solution)/shard_map/all_to_all | solution.py:73
Sparse Core Ops, SparseCore 0:
  10.1 93.0 all-gather.14
  105.9 77.6 all-gather.16
where the time goes:
time: 386 us; the launch traced here: 385 us
  blocking collectives  187 us (48%)
  other arithmetic  87.4 us (23%)
  matrix products  61.2 us (16%)
  local copies, waits for them, and re-layouts  22.2 us (6%)
  between operations  14.7 us (4%)
  waiting for transfers between devices  8.78 us (2%)
    all_gather x12, blocking collectives, prefix_by_axis(): lax.all_gather(part.astype(kind), axis)  166 us
    another operation x5, other arithmetic, block_pieces(): jax.scipy.linalg.solve_triangular(eye_block - remove_remove, targets, low...  62.5 us
    all_to_all x1, blocking collectives, from_everyone(): lax.all_to_all(jnp.broadcast_to(value[None], (devices, *value.shape)), ax...  21.2 us
    dot_general x38, matrix products, join_pair(): jnp.einsum('hik,hkj->hij', earlier[1], later[0], precision=highest)  17.1 us
    dot_general x1, matrix products, on_device(): jnp.dot(activated, lax.all_gather(shrinking_matrix, SP, axis=1, tiled=Tru...  8.25 us
    all_to_all x1, waiting for transfers between devices, sum_at_owner(): lax.all_to_all(tiles, axis, split_axis=0, concat_axis=0, tiled=True)  8.04 us
  transfers between devices with their start and end apart: 3, of which 1 were waited for; matrix products, arithmetic and copies ran while one was open for 41% of the time, Pallas kernels for 0%

commit v1 on v0

v1 whole, which is shorter than its diff:
```python
import jax
import jax.numpy as jnp
from jax import lax
from jax.experimental import pallas as pl
from jax.experimental.pallas import tpu as pltpu
from jax.sharding import Mesh
from jax.sharding import PartitionSpec as P

SP = ("sp_0", "sp_1", "sp_2")
ROW = ("sp_1", "sp_2")
TOK = 128
LANES = 128
HALF = 64
SHARES = 8

norm_epsilon = 1e-06
head_epsilon = 0.00064
key_epsilon = 1e-06

f32 = jnp.float32
bf16 = jnp.bfloat16


def dot_nn(a, b):
    return lax.dot_general(a, b, (((1,), (0,)), ((), ())), preferred_element_type=f32)


def dot_nt(a, b):
    return lax.dot_general(a, b, (((1,), (1,)), ((), ())), preferred_element_type=f32)


def dot_tn(a, b):
    return lax.dot_general(a, b, (((0,), (0,)), ((), ())), preferred_element_type=f32)


def halves(a):
    high = a.astype(bf16)
    return high, (a - high.astype(f32)).astype(bf16)


def mm(a, b):
    ah, al = a
    bh, bl = b
    return dot_nn(jnp.concatenate([ah, al], 1), jnp.concatenate([bh, bh], 0)) + dot_nn(ah, bl)


def mm_nt(a, b):
    ah, al = a
    bh, bl = b
    return dot_nt(jnp.concatenate([ah, al], 1), jnp.concatenate([bh, bh], 1)) + dot_nt(ah, bl)


def mm_tn(a, b):
    ah, al = a
    bh, bl = b
    return dot_tn(jnp.concatenate([ah, al], 0), jnp.concatenate([bh, bh], 0)) + dot_tn(ah, bl)


def head_masks(group):
    lane = lax.broadcasted_iota(jnp.int32, (1, LANES), 1)
    if group == 0:
        return [(lane < HALF).astype(f32), (lane >= HALF).astype(f32)]
    return [None]


def head_sum(a, masks):
    if masks[0] is None:
        return jnp.sum(a, axis=1, keepdims=True)
    return sum(jnp.sum(a * m, axis=1, keepdims=True) * m for m in masks)


def masked(a, mask):
    return a if mask is None else a * mask


def local_kernel(q_ref, k_ref, v_ref, f_ref, l_ref, e_ref, send_ref, out_ref, read_ref):
    row = lax.broadcasted_iota(jnp.int32, (TOK, TOK), 0)
    col = lax.broadcasted_iota(jnp.int32, (TOK, TOK), 1)
    strict = row > col
    inclusive = row >= col
    eye = (row == col).astype(f32)
    ones = inclusive.astype(bf16)
    slots = []
    heads = []
    for slot in range(4):
        group, cut = slot // 2, (slot % 2) * LANES
        lanes = slice(cut, cut + LANES)
        q = q_ref[group, :, lanes].astype(f32)
        k = k_ref[group, :, lanes].astype(f32)
        v = v_ref[group, :, lanes].astype(f32)
        fade = f_ref[group, :, lanes].astype(f32)
        speed = l_ref[group, :, lanes].astype(f32)
        log_decay = e_ref[group, :, lanes] - jnp.exp(-0.5) / (1.0 + jnp.exp(-fade))
        learn = 1.0 / (1.0 + jnp.exp(-speed))
        masks = head_masks(group)
        removal = k * lax.rsqrt(head_sum(k * k, masks) + key_epsilon)
        d0, rest = log_decay.astype(bf16), None
        rest = log_decay - d0.astype(f32)
        d1 = rest.astype(bf16)
        d2 = (rest - d1.astype(f32)).astype(bf16)
        cum = dot_nn(ones, d0) + dot_nn(ones, d1) + dot_nn(ones, d2)
        middle = cum[TOK // 2 : TOK // 2 + 1, :]
        forward = jnp.exp(cum - middle)
        backward = jnp.exp(middle - cum)
        undo = jnp.exp(-log_decay)
        right = learn * removal
        queries = jnp.concatenate([-removal * undo * forward, q * forward], 0)
        sources = halves(jnp.concatenate([right * backward, k * backward], 0))
        grown = jnp.exp(cum)
        final = cum[TOK - 1 : TOK, :]
        tail = jnp.exp(final - cum)
        slots.append(
            dict(
                masks=masks,
                v=halves(v),
                start=-removal * jnp.exp(cum - log_decay),
                grown=q * grown,
                right=halves(right * tail),
                keys=halves(k * tail),
                kept=jnp.exp(final),
                heads=[],
            )
        )
        for mask in masks:
            pairs = mm_nt(halves(masked(queries, mask)), sources)
            head = dict(
                slot=slot,
                mask=mask,
                n=jnp.where(strict, pairs[:TOK, :TOK], 0.0),
                rk=jnp.where(strict, pairs[:TOK, TOK:], 0.0),
                qr=jnp.where(inclusive, pairs[TOK:, :TOK], 0.0),
                qk=jnp.where(inclusive, pairs[TOK:, TOK:], 0.0),
            )
            heads.append(head)
            slots[slot]["heads"].append(head)
    same = (row // 8) == (col // 8)
    for head in heads:
        head["m"] = jnp.where(same, head["n"], 0.0)
        head["x"] = eye + head["m"]
    for _ in range(2):
        for head in heads:
            m = halves(head["m"])
            head["m"] = mm(m, m)
        for head in heads:
            head["x"] = head["x"] + mm(halves(head["x"]), halves(head["m"]))
    size = 8
    while size < TOK:
        below = (row // (2 * size) == col // (2 * size)) & (row // size != col // size)
        for head in heads:
            off = halves(jnp.where(below, head["n"], 0.0))
            head["y"] = halves(mm(off, halves(head["x"])))
        for head in heads:
            head["x"] = head["x"] + mm(halves(head["x"]), head["y"])
        size *= 2
    for slot, part in enumerate(slots):
        carried = start = local = read = None
        for head in part["heads"]:
            mask = head["mask"]
            target = jnp.concatenate([mm(halves(head["rk"]), part["v"]), part["start"]], 1)
            solved = mm(halves(head["x"]), halves(target))
            from_solved = mm(halves(head["qr"]), halves(solved))
            pieces = [
                masked(solved[:, :LANES], mask),
                masked(solved[:, LANES:], mask),
                masked(from_solved[:, :LANES] + mm(halves(head["qk"]), part["v"]), mask),
                masked(from_solved[:, LANES:], mask),
            ]
            if carried is None:
                carried, start, local, read = pieces
            else:
                carried, start, local, read = (
                    carried + pieces[0],
                    start + pieces[1],
                    local + pieces[2],
                    read + pieces[3],
                )
        transit = mm_tn(halves(start), part["right"])
        added = mm_tn(halves(carried), part["right"]) + mm_tn(part["v"], part["keys"])
        if len(part["heads"]) == 2:
            block = (row // HALF) == (col // HALF)
            transit = jnp.where(block, transit, 0.0)
            added = jnp.where(block, added, 0.0)
        transit = (transit + eye * part["kept"]).astype(bf16)
        added = added.astype(bf16)
        for half in range(2):
            send_ref[2 * slot + half, :LANES, :] = transit
            send_ref[2 * slot + half, LANES:, :] = added[half * HALF : (half + 1) * HALF, :]
        out_ref[slot] = local
        read_ref[slot] = part["grown"] + read


def row_kernel(got_ref, prefix_ref, total_ref):
    row = lax.broadcasted_iota(jnp.int32, (LANES + HALF, LANES), 0)
    col = lax.broadcasted_iota(jnp.int32, (LANES + HALF, LANES), 1)
    zero = jnp.zeros((LANES, LANES), f32)
    prefix_ref[0] = (row == col).astype(f32)
    run = got_ref[0].astype(f32)
    for k in range(1, SHARES):
        prefix_ref[k] = run
        got = got_ref[k]
        step = got[:LANES]
        high, low = halves(run)
        run = dot_nn(jnp.concatenate([high, low], 1), jnp.concatenate([step, step], 0))
        run = run + jnp.concatenate([zero, got[LANES:].astype(f32)], 0)
    total = run.astype(bf16)
    for k in range(total_ref.shape[0]):
        total_ref[k] = total


def state_kernel(place_ref, every_ref, prefix_ref, send_ref):
    place = place_ref[0]
    state = jnp.zeros((HALF, LANES), f32)
    for k in range(every_ref.shape[0] - 1):
        got = every_ref[k]
        step = got[:LANES]
        high, low = halves(state)
        grown = dot_nn(jnp.concatenate([high, low], 1), jnp.concatenate([step, step], 0))
        state = jnp.where(k < place, grown + got[LANES:].astype(f32), state)
    split = halves(state)
    for k in range(SHARES):
        moved = mm(split, halves(prefix_ref[k, :LANES, :]))
        send_ref[k] = (moved + prefix_ref[k, LANES:, :]).astype(bf16)


def mix_kernel(
    out_ref, read_ref, state_ref, q_ref, k_ref, v_ref, gate_ref, gain_ref, own_ref, w_ref, y_ref
):
    mixed = []
    for slot in range(4):
        group, cut = slot // 2, (slot % 2) * LANES
        lanes = slice(cut, cut + LANES)
        width = HALF if group == 0 else LANES
        masks = head_masks(group)
        state = jnp.concatenate([state_ref[2 * slot], state_ref[2 * slot + 1]], 0)
        high, low = halves(read_ref[slot])
        raw = out_ref[slot] + dot_nt(
            jnp.concatenate([high, low], 1), jnp.concatenate([state, state], 1)
        )
        centered = raw - head_sum(raw, masks) * (1.0 / width)
        variance = head_sum(centered * centered, masks) * (1.0 / width)
        normed = centered * lax.rsqrt(variance + head_epsilon) * gain_ref[group : group + 1, lanes]
        q = q_ref[group, :, lanes].astype(f32)
        k = k_ref[group, :, lanes].astype(f32)
        v = v_ref[group, :, lanes].astype(f32)
        own = head_sum(q * k * own_ref[group : group + 1, lanes], masks) * v
        mixed.append(((normed + own) * gate_ref[group, :, lanes].astype(f32)).astype(bf16))
    y_ref[...] = dot_nn(jnp.concatenate(mixed, 1), w_ref[...]).astype(bf16)


def call(kernel, outs, scalars=0):
    spec = pl.BlockSpec(memory_space=pltpu.VMEM)
    return lambda *args: pl.pallas_call(
        kernel,
        out_shape=outs,
        in_specs=[pl.BlockSpec(memory_space=pltpu.SMEM)] * scalars + [spec] * (len(args) - scalars),
        out_specs=jax.tree.map(lambda _: spec, outs),
        compiler_params=pltpu.CompilerParams(vmem_limit_bytes=32 * 1024 * 1024),
    )(*args)


def array(dims, kind):
    return jax.ShapeDtypeStruct(dims, kind)


def exchange(value, axis):
    return lax.all_to_all(value, axis, 0, 0, tiled=True)


def from_everyone(value, axis):
    devices = lax.axis_size(axis)
    return exchange(jnp.broadcast_to(value[None], (devices, *value.shape)), axis)


def on_device(
    stratum_source_matrix,
    acceptance_query,
    cluster_lookup_matrix,
    cluster_payload_matrix,
    fading_logit,
    adaptation_speed_logit,
    additional_fading_exponent,
    result_switch_pair,
    attender_scaling_factor,
    present_item_factor,
    final_mapping_matrix,
    perceptron_scaling_factor,
    switching_matrix,
    widening_matrix,
    shrinking_matrix,
):
    hidden = switching_matrix.shape[1]
    features = perceptron_scaling_factor.shape[0]
    whole = lax.all_gather(
        jnp.concatenate([switching_matrix, widening_matrix, shrinking_matrix.T], axis=1),
        SP,
        axis=0,
        tiled=True,
    )
    blocks = array((4, TOK, LANES), f32)
    send, local_out, start_read = call(
        local_kernel, (array((SHARES, LANES + HALF, LANES), bf16), blocks, blocks)
    )(
        acceptance_query,
        cluster_lookup_matrix,
        cluster_payload_matrix,
        fading_logit,
        adaptation_speed_logit,
        additional_fading_exponent,
    )
    planes = lax.axis_size("sp_0")
    prefix, total = call(
        row_kernel,
        (
            array((SHARES, LANES + HALF, LANES), f32),
            array((planes, LANES + HALF, LANES), bf16),
        ),
    )(exchange(send, ROW))
    states = call(state_kernel, array((SHARES, HALF, LANES), bf16), 1)(
        lax.axis_index("sp_0").astype(jnp.int32).reshape(1), exchange(total, "sp_0"), prefix
    )
    partial_value = call(mix_kernel, array((TOK, features), bf16))(
        local_out,
        start_read,
        exchange(states, ROW),
        acceptance_query,
        cluster_lookup_matrix,
        cluster_payload_matrix,
        result_switch_pair,
        attender_scaling_factor,
        present_item_factor,
        final_mapping_matrix.reshape(-1, features),
    )
    columns = features // lax.axis_size("tp")
    own_start = lax.axis_index("tp") * columns
    residual_float = stratum_source_matrix.astype(f32)
    attention = jnp.sum(from_everyone(partial_value, "tp").astype(f32), axis=0)
    state_float = (residual_float + attention).astype(bf16).astype(f32)
    mean_square = jnp.mean(state_float * state_float, axis=1, keepdims=True)
    normed = (
        state_float * lax.rsqrt(mean_square + norm_epsilon) * perceptron_scaling_factor
    ).astype(bf16)
    own_state = lax.dynamic_slice_in_dim(state_float, own_start, columns, 1)
    gate_pre = jnp.dot(normed, whole[:, :hidden], preferred_element_type=f32)
    up_pre = jnp.dot(normed, whole[:, hidden : 2 * hidden], preferred_element_type=f32)
    activated = (jax.nn.silu(gate_pre) * up_pre).astype(bf16)
    down_terms = dot_nt(activated, whole[:, 2 * hidden :]).astype(bf16)
    tiles = jnp.moveaxis(down_terms.reshape(TOK, features // columns, columns), 1, 0)
    mixer = jnp.sum(exchange(tiles, "tp").astype(f32), axis=0)
    return (own_state + mixer).astype(bf16)


def solution(mesh):
    split = Mesh(mesh.devices.reshape(8, 4, 2, mesh.shape["tp"]), ("sp_0", "sp_1", "sp_2", "tp"))
    heads = P(None, SP, "tp")
    return jax.shard_map(
        on_device,
        mesh=split,
        in_specs=(
            P(SP, None),
            heads,
            heads,
            heads,
            heads,
            heads,
            heads,
            heads,
            P(None, "tp"),
            P(None, "tp"),
            P(None, "tp", None),
            P(),
            P(SP, "tp"),
            P(SP, "tp"),
            P("tp", SP),
        ),
        out_specs=P(SP, "tp"),
        check_vma=False,
    )
```

time: 386 us -> 150 us (0.39)
  blocking collectives: 187 us -> 54.8 us
  other arithmetic: 87.4 us -> 3.24 us
  matrix products: 61.2 us -> 10.9 us
  waiting for transfers between devices: 8.78 us -> 30.9 us
  Pallas kernels: 0 us -> 9.18 us
  starting transfers between devices: 3.51 us -> 11.9 us
  local copies, waits for them, and re-layouts: 22.2 us -> 14 us
    all_gather x12 -> x0, blocking collectives: 166 us -> none  [prefix_by_axis(): lax.all_gather(part.astype(kind), axis)]
    another operation x7 -> x0, other arithmetic: 62.5 us -> none  [the longest x5 62.5 us: block_pieces(): jax.scipy.linalg.solve_triangular(eye_block - remove_remove, targets, low...]
    dot_general x81 -> x2, matrix products: 57.5 us -> 10.9 us  [the longest x1 7.27 us: dot_nt(): lax.dot_general(a, b, (((1,), (1,)), ((), ())), preferred_element_type=f32)]
    all_to_all x1 -> x3, blocking collectives: 21.2 us -> 54.8 us  [exchange(): return lax.all_to_all(value, axis, 0, 0, tiled=True)]
    all_to_all x1 -> x2, waiting for transfers between devices: 8.04 us -> 24.9 us  [exchange(): return lax.all_to_all(value, axis, 0, 0, tiled=True)]
    unnamed x62 -> x36, local copies, waits for them, and re-layouts: 3.48 us -> 12.9 us
    pallas_call x0 -> x4, Pallas kernels: none -> 9.18 us  [call(): pl.pallas_call(kernel, out_shape=outs, in_specs=[pl.BlockSpec(memory_spac...]
    all_to_all x1 -> x2, starting transfers between devices: 3.47 us -> 11.9 us  [exchange(): return lax.all_to_all(value, axis, 0, 0, tiled=True)]
  transfers between devices with their start and end apart: 3 -> 3, of which waited for: 1 -> 3; matrix products, arithmetic and copies ran while one was open for 41% -> 1% of each run, Pallas kernels for 0% -> 6%
where the time goes in v1:
time: 150 us; the launch traced here: 148 us
  blocking collectives  54.8 us (37%)
  waiting for transfers between devices  30.9 us (21%)
  local copies, waits for them, and re-layouts  14 us (9%)
  between operations  13.5 us (9%)
  starting transfers between devices  11.9 us (8%)
  matrix products  10.9 us (7%)
  Pallas kernels  9.18 us (6%)
  other arithmetic  3.24 us (2%)
    all_to_all x3, blocking collectives, exchange(): return lax.all_to_all(value, axis, 0, 0, tiled=True)  54.8 us
    all_to_all x2, waiting for transfers between devices, exchange(): return lax.all_to_all(value, axis, 0, 0, tiled=True)  24.9 us
    unnamed x36, local copies, waits for them, and re-layouts  12.9 us
    all_to_all x2, starting transfers between devices, exchange(): return lax.all_to_all(value, axis, 0, 0, tiled=True)  11.9 us
    pallas_call x4, Pallas kernels, call(): pl.pallas_call(kernel, out_shape=outs, in_specs=[pl.BlockSpec(memory_spac...  9.18 us
    dot_general x1, matrix products, dot_nt(): lax.dot_general(a, b, (((1,), (1,)), ((), ())), preferred_element_type=f32)  7.27 us
    all_gather x1, waiting for transfers between devices, on_device(): lax.all_gather(jnp.concatenate([switching_matrix, widening_matrix, shrink...  5.98 us
    dot_general x1, matrix products, on_device(): gate_pre = jnp.dot(normed, whole[:, :hidden], preferred_element_type=f32)  3.67 us
  transfers between devices with their start and end apart: 3, of which 3 were waited for; matrix products, arithmetic and copies ran while one was open for 1% of the time, Pallas kernels for 6%

profile of v1, /device:TPU:2, one launch (start us, length us, event | category | flops | bytes accessed | tf_op | source)
XLA Modules:
  0.0 148.5 jit_solution(4082389060909997049)
XLA Ops:
  6.5 1.9 %pad_maximum_fusion = bf16[32,4224]{1,0:T(8,128)(2,1)} fusion(bf16[32,1408]{1,0:T(8,128)(2,1)} %bitcast.12, bf16[32,1408]{1,0:T(8,128)(2,1)} %param.28, bf16[32,1408]{1,0:T(8,128)(2,1)} %param.27), kind=kLoop, calls=%fused_computation.22 | loop fusion | flops 811008 | bytes 540672 | tf_op jit(solution)/shard_map/concatenate | solution.py:294
  8.4 0.9 copy-done.1
  9.3 0.9 copy-done.3
  10.2 0.9 copy-done.5
  11.1 0.9 copy-done.8
  12.1 0.9 copy-done.11
  13.0 0.9 copy-done.12
  13.9 6.3 %shard_map.145 = (bf16[8,192,128]{2,1,0:T(8,128)(2,1)S(1)}, f32[4,128,128]{2,1,0:T(8,128)S(1)}, f32[4,128,128]{2,1,0:T(8,128)S(1)}) custom-call(bf16[2,128,256]{2,1,0:T(8,128)(2,1)S(1)} %copy-done.1, bf16[2,128,256]{2,1,0:T(8,128)(2,1)S(1)} %copy-done.3, bf16[2,128,256]{2,1,0:T(8,128)(2,1)S(1)} %copy-done.5, bf16[2,128,256]{2,1,0:T(8,128)(2,1)S(1)} %copy-done.11, ...), custom_call_target="tpu_custom_call" | custom-call | tf_op jit(solution)/shard_map/pallas_call | solution.py:252
  20.2 0.7 copy-done.9
  20.9 14.7 %all_to_all.25.got_ref = bf16[8,192,128]{2,1,0:T(8,128)(2,1)S(1)} all-to-all(bf16[8,192,128]{2,1,0:T(8,128)(2,1)S(1)} %get-tuple-element.12), channel_id=1, replica_groups=mesh['sp_0'=8,'sp_1'=4,'sp_2'=2,'tp'=4] {'sp_1','sp_2'}, dimensions={0} | all-to-all | bytes 786432 | tf_op jit(solution)/shard_map/all_to_all | solution.py:266
  35.6 0.9 shard_map.146
  36.6 0.7 copy-done.7
  37.3 7.6 %all-to-all-start.1 = ((bf16[8,192,128]{2,1,0:T(8,128)(2,1)}), bf16[8,192,128]{2,1,0:T(8,128)(2,1)S(1)}, u32[]{:S(2)}, u32[]{:S(2)}) async-start(bf16[8,192,128]{2,1,0:T(8,128)(2,1)} %copy-done.7), calls=%async_computation.1 | async-start | bytes 786432 | tf_op jit(solution)/shard_map/all_to_all | solution.py:266
  44.9 15.0 %all-to-all-done.1.every_ref = bf16[8,192,128]{2,1,0:T(8,128)(2,1)S(1)} async-done(((bf16[8,192,128]{2,1,0:T(8,128)(2,1)}), bf16[8,192,128]{2,1,0:T(8,128)(2,1)S(1)}, u32[]{:S(2)}, u32[]{:S(2)}) %all-to-all-start.1) | async-done | bytes 393248 | tf_op jit(solution)/shard_map/all_to_all | solution.py:266
  59.9 1.1 shard_map.147
  61.0 9.3 %all_to_all.26.state_ref = bf16[8,64,128]{2,1,0:T(8,128)(2,1)S(1)} all-to-all(bf16[8,64,128]{2,1,0:T(8,128)(2,1)S(1)} %shard_map.147), channel_id=1, replica_groups=mesh['sp_0'=8,'sp_1'=4,'sp_2'=2,'tp'=4] {'sp_1','sp_2'}, dimensions={0} | all-to-all | bytes 262144 | tf_op jit(solution)/shard_map/all_to_all | solution.py:266
  70.4 0.9 copy-done.2
  71.3 0.9 copy-done.4
  72.2 0.9 copy-done.6
  73.1 1.0 copy-done.10
  74.1 0.9 copy-done.13
  75.0 0.7 copy-done.14
  75.7 0.7 copy-done.15
  76.4 0.8 shard_map.148
  77.5 30.8 %all_to_all.27 = bf16[4,128,2048]{2,1,0:T(8,128)(2,1)S(1)} all-to-all(bf16[4,128,2048]{2,1,0:T(8,128)(2,1)S(1)} %broadcast_in_dim.2), channel_id=1, replica_groups=mesh['sp_0'=8,'sp_1'=4,'sp_2'=2,'tp'=4] {'tp'}, dimensions={0} | all-to-all | bytes 4194304 | tf_op jit(solution)/shard_map/all_to_all | solution.py:266
  108.9 6.0 %all-gather.2.cloned.1.call-done = bf16[2048,4224]{1,0:T(8,128)(2,1)} async-done(((bf16[32,4224]{1,0:T(8,128)(2,1)}), bf16[2048,4224]{1,0:T(8,128)(2,1)}) %all-gather.2.cloned.1.call-update) | async-done | bytes 17301520 | tf_op jit(solution)/shard_map/all_gather | solution.py:293
  114.9 3.7 %fusion.4 = f32[128,1408]{1,0:T(8,128)S(1)} fusion(bf16[2048,4224]{1,0:T(8,128)(2,1)} %all-gather.2.cloned.1.call-done, f32[128,2048]{1,0:T(8,128)S(1)} %get-tuple-element.16, f32[2048]{0:T(1024)S(1)} %copy-done.17, f32[128]{0:T(128)S(1)} %add_rsqrt_fusion), kind=kOutput, calls=%fused_computation.4 | convolution fusion | flops 738983936 | bytes 7545344 | tf_op jit(solution)/shard_map/dot_general | solution.py:343
  118.5 7.3 %fusion.9 = bf16[128,2048]{1,0:T(8,128)(2,1)S(1)} fusion(bf16[2048,4224]{1,0:T(8,128)(2,1)} %all-gather.2.cloned.1.call-done, f32[128,1408]{1,0:T(8,128)S(1)} %fusion.4, f32[128,2048]{1,0:T(8,128)S(1)} %get-tuple-element.16, f32[2048]{0:T(1024)S(1)} %copy-done.17, f32[128]{0:T(128)S(1)} %add_rsqrt_fusion), kind=kOutput, calls=%fused_computation.8 | convolution fusion | flops 1478524928 | bytes 13836800 | tf_op jit(solution)/shard_map/dot_general | solution.py:29
  125.8 0.8 copy.20
  126.7 4.3 %all-to-all-start.4 = ((bf16[4,128,512]{2,1,0:T(8,128)(2,1)}), bf16[4,128,512]{2,1,0:T(8,128)(2,1)S(1)}, u32[]{:S(2)}, u32[]{:S(2)}) async-start(bf16[4,128,512]{2,1,0:T(8,128)(2,1)} %bitcast.9), calls=%async_computation.4 | async-start | bytes 1048576 | tf_op jit(solution)/shard_map/all_to_all | solution.py:266
  130.9 9.9 %all-to-all-done.4 = bf16[4,128,512]{2,1,0:T(8,128)(2,1)S(1)} async-done(((bf16[4,128,512]{2,1,0:T(8,128)(2,1)}), bf16[4,128,512]{2,1,0:T(8,128)(2,1)S(1)}, u32[]{:S(2)}, u32[]{:S(2)}) %all-to-all-start.4) | async-done | bytes 524320 | tf_op jit(solution)/shard_map/all_to_all | solution.py:266
  140.9 0.7 add_convert_fusion.1
  (28 shorter events, 1.0 us)
Async XLA Ops:
  6.5 63.8 %copy-start = (bf16[2,256,2048]{2,1,0:T(8,128)(2,1)S(1)}, bf16[2,256,2048]{2,1,0:T(8,128)(2,1)}, u32[]{:S(2)}) copy-start(bf16[2,256,2048]{2,1,0:T(8,128)(2,1)} %param.25) | copy-start | bytes 6291460
  6.5 108.3 %all-gather.2.cloned.1.call-start = ((), (), s32[]{:S(2)}) async-start(), calls=%async_computation.5 | async-start | bytes 17571840 | tf_op jit(solution)/shard_map/all_gather | solution.py:293
  8.4 0.9 copy-start.1
  9.3 0.9 copy-start.3
  10.2 0.9 copy-start.5
  11.1 0.9 copy-start.8
  12.1 0.9 copy-start.11
  13.0 0.9 copy-start.12
  20.2 0.7 copy-start.9
  36.6 0.7 copy-start.7
  37.3 22.6 %all-to-all-start.1 = ((bf16[8,192,128]{2,1,0:T(8,128)(2,1)}), bf16[8,192,128]{2,1,0:T(8,128)(2,1)S(1)}, u32[]{:S(2)}, u32[]{:S(2)}) async-start(bf16[8,192,128]{2,1,0:T(8,128)(2,1)} %copy-done.7), calls=%async_computation.1 | async-start | bytes 786432 | tf_op jit(solution)/shard_map/all_to_all | solution.py:266
  70.4 0.9 copy-start.2
  71.3 0.9 copy-start.4
  72.2 0.9 copy-start.6
  73.1 1.0 copy-start.10
  74.1 0.9 copy-start.13
  75.0 0.7 copy-start.14
  75.7 0.7 copy-start.15
  77.2 31.5 %copy-start.16 = (bf16[128,2048]{1,0:T(8,128)(2,1)S(1)}, bf16[128,2048]{1,0:T(8,128)(2,1)}, u32[]{:S(2)}) copy-start(bf16[128,2048]{1,0:T(8,128)(2,1)} %param.15) | copy-start | bytes 1572868
  77.2 37.7 %copy-start.17 = (f32[2048]{0:T(1024)S(1)}, f32[2048]{0:T(1024)}, u32[]{:S(2)}) copy-start(f32[2048]{0:T(1024)} %param.26) | copy-start | bytes 24580
  126.7 14.2 %all-to-all-start.4 = ((bf16[4,128,512]{2,1,0:T(8,128)(2,1)}), bf16[4,128,512]{2,1,0:T(8,128)(2,1)S(1)}, u32[]{:S(2)}, u32[]{:S(2)}) async-start(bf16[4,128,512]{2,1,0:T(8,128)(2,1)} %bitcast.9), calls=%async_computation.4 | async-start | bytes 1048576 | tf_op jit(solution)/shard_map/all_to_all | solution.py:266
Sparse Core Ops, SparseCore 0:
  10.1 104.7 all-gather.1

commit v2 on v1

--- a/solution.py
+++ b/solution.py
@@ -73,7 +73,19 @@
     return a if mask is None else a * mask
 
 
-def local_kernel(q_ref, k_ref, v_ref, f_ref, l_ref, e_ref, send_ref, out_ref, read_ref):
+def fetch(sources, targets, sems):
+    copies = [pltpu.make_async_copy(a, b, sems.at[k]) for k, (a, b) in enumerate(zip(sources, targets))]
+    for copy in copies:
+        copy.start()
+    return copies
+
+
+def local_kernel(*refs):
+    inputs, outputs, scratch, sems = refs[:9], refs[9:14], refs[14:23], refs[23]
+    send_ref, out_ref, read_ref, scale_ref, extra_ref = outputs
+    q_ref, k_ref, v_ref, f_ref, l_ref, e_ref, gate_ref, gain_ref, own_ref = scratch
+    for copy in fetch(inputs, scratch, sems):
+        copy.wait()
     row = lax.broadcasted_iota(jnp.int32, (TOK, TOK), 0)
     col = lax.broadcasted_iota(jnp.int32, (TOK, TOK), 1)
     strict = row > col
@@ -94,7 +106,11 @@
         learn = 1.0 / (1.0 + jnp.exp(-speed))
         masks = head_masks(group)
         removal = k * lax.rsqrt(head_sum(k * k, masks) + key_epsilon)
-        d0, rest = log_decay.astype(bf16), None
+        gate = gate_ref[group, :, lanes].astype(f32)
+        scale_ref[slot] = gain_ref[group : group + 1, lanes] * gate
+        own = head_sum(q * k * own_ref[group : group + 1, lanes], masks)
+        extra_ref[slot] = own * v * gate
+        d0 = log_decay.astype(bf16)
         rest = log_decay - d0.astype(f32)
         d1 = rest.astype(bf16)
         d2 = (rest - d1.astype(f32)).astype(bf16)
@@ -186,7 +202,9 @@
             send_ref[2 * slot + half, :LANES, :] = transit
             send_ref[2 * slot + half, LANES:, :] = added[half * HALF : (half + 1) * HALF, :]
         out_ref[slot] = local
-        read_ref[slot] = part["grown"] + read
+        high, low = halves(part["grown"] + read)
+        read_ref[slot, :, :LANES] = high
+        read_ref[slot, :, LANES:] = low
 
 
 def row_kernel(got_ref, prefix_ref, total_ref):
@@ -223,39 +241,97 @@
 
 
 def mix_kernel(
-    out_ref, read_ref, state_ref, q_ref, k_ref, v_ref, gate_ref, gain_ref, own_ref, w_ref, y_ref
+    out_ref, read_ref, scale_ref, extra_ref, state_ref, weight_ref, y_ref, w_ref, sems
 ):
+    (copy,) = fetch([weight_ref], [w_ref], sems)
     mixed = []
     for slot in range(4):
-        group, cut = slot // 2, (slot % 2) * LANES
-        lanes = slice(cut, cut + LANES)
-        width = HALF if group == 0 else LANES
-        masks = head_masks(group)
+        width = HALF if slot < 2 else LANES
+        masks = head_masks(slot // 2)
         state = jnp.concatenate([state_ref[2 * slot], state_ref[2 * slot + 1]], 0)
-        high, low = halves(read_ref[slot])
-        raw = out_ref[slot] + dot_nt(
-            jnp.concatenate([high, low], 1), jnp.concatenate([state, state], 1)
-        )
+        raw = out_ref[slot] + dot_nt(read_ref[slot], jnp.concatenate([state, state], 1))
         centered = raw - head_sum(raw, masks) * (1.0 / width)
         variance = head_sum(centered * centered, masks) * (1.0 / width)
-        normed = centered * lax.rsqrt(variance + head_epsilon) * gain_ref[group : group + 1, lanes]
-        q = q_ref[group, :, lanes].astype(f32)
-        k = k_ref[group, :, lanes].astype(f32)
-        v = v_ref[group, :, lanes].astype(f32)
-        own = head_sum(q * k * own_ref[group : group + 1, lanes], masks) * v
-        mixed.append(((normed + own) * gate_ref[group, :, lanes].astype(f32)).astype(bf16))
+        normed = centered * lax.rsqrt(variance + head_epsilon) * scale_ref[slot]
+        mixed.append((normed + extra_ref[slot]).astype(bf16))
+    copy.wait()
     y_ref[...] = dot_nn(jnp.concatenate(mixed, 1), w_ref[...]).astype(bf16)
 
 
-def call(kernel, outs, scalars=0):
-    spec = pl.BlockSpec(memory_space=pltpu.VMEM)
-    return lambda *args: pl.pallas_call(
+AHEAD = 4
+
+
+def feed_kernel(x_ref, whole_ref, y_ref, pair_ref, down_ref, act_ref, sems):
+    hidden = whole_ref.shape[1] // 3
+    steps = hidden // LANES
+    tiles, _, rows = y_ref.shape
+    waves = []
+    for k in range(steps):
+        for part in range(2):
+            lanes = pl.ds(part * hidden + k * LANES, LANES)
+            target = pair_ref.at[k, :, pl.ds(part * LANES, LANES)]
+            waves.append((whole_ref.at[:, lanes], target))
+    for k in range(tiles):
+        waves.append((whole_ref.at[pl.ds(k * rows, rows), pl.ds(2 * hidden, hidden)], down_ref.at[k]))
+    copies = [pltpu.make_async_copy(a, b, sems.at[k]) for k, (a, b) in enumerate(waves)]
+    for copy in copies[: 2 * AHEAD]:
+        copy.start()
+    sent = 2 * AHEAD
+    x = x_ref[...]
+    for k in range(steps):
+        copies[2 * k].wait()
+        copies[2 * k + 1].wait()
+        for _ in range(2):
+            if sent < len(copies):
+                copies[sent].start()
+                sent += 1
+        both = dot_nn(x, pair_ref[k])
+        gate = both[:, :LANES]
+        active = gate / (1.0 + jnp.exp(-gate)) * both[:, LANES:]
+        act_ref[:, k * LANES : (k + 1) * LANES] = active.astype(bf16)
+    active = act_ref[...]
+    for k in range(tiles):
+        copies[2 * steps + k].wait()
+        y_ref[k] = dot_nt(active, down_ref[k]).astype(bf16)
+
+
+def feed_forward(normed, whole, tiles):
+    tokens, features = normed.shape
+    hidden = whole.shape[1] // 3
+    steps = hidden // LANES
+    rows = features // tiles
+    return pl.pallas_call(
+        feed_kernel,
+        out_shape=array((tiles, tokens, rows), bf16),
+        in_specs=[VMEM, HBM],
+        out_specs=VMEM,
+        scratch_shapes=[
+            pltpu.VMEM((steps, features, 2 * LANES), bf16),
+            pltpu.VMEM((tiles, rows, hidden), bf16),
+            pltpu.VMEM((tokens, hidden), bf16),
+            pltpu.SemaphoreType.DMA((2 * steps + tiles,)),
+        ],
+        compiler_params=pltpu.CompilerParams(vmem_limit_bytes=40 * 1024 * 1024),
+    )(normed, whole)
+
+
+VMEM = pl.BlockSpec(memory_space=pltpu.VMEM)
+HBM = pl.BlockSpec(memory_space=pltpu.HBM)
+SMEM = pl.BlockSpec(memory_space=pltpu.SMEM)
+
+
+def call(kernel, outs, specs, fetched=(), limit=24 * 1024 * 1024):
+    scratch = [pltpu.VMEM(a.shape, a.dtype) for a in fetched]
+    if scratch:
+        scratch.append(pltpu.SemaphoreType.DMA((len(scratch),)))
+    return pl.pallas_call(
         kernel,
         out_shape=outs,
-        in_specs=[pl.BlockSpec(memory_space=pltpu.SMEM)] * scalars + [spec] * (len(args) - scalars),
-        out_specs=jax.tree.map(lambda _: spec, outs),
-        compiler_params=pltpu.CompilerParams(vmem_limit_bytes=32 * 1024 * 1024),
-    )(*args)
+        in_specs=specs,
+        out_specs=jax.tree.map(lambda _: VMEM, outs),
+        scratch_shapes=scratch,
+        compiler_params=pltpu.CompilerParams(vmem_limit_bytes=limit),
+    )
 
 
 def array(dims, kind):
@@ -288,7 +364,6 @@
     widening_matrix,
     shrinking_matrix,
 ):
-    hidden = switching_matrix.shape[1]
     features = perceptron_scaling_factor.shape[0]
     whole = lax.all_gather(
         jnp.concatenate([switching_matrix, widening_matrix, shrinking_matrix.T], axis=1),
@@ -297,16 +372,30 @@
         tiled=True,
     )
     blocks = array((4, TOK, LANES), f32)
-    send, local_out, start_read = call(
-        local_kernel, (array((SHARES, LANES + HALF, LANES), bf16), blocks, blocks)
-    )(
+    inputs = (
         acceptance_query,
         cluster_lookup_matrix,
         cluster_payload_matrix,
         fading_logit,
         adaptation_speed_logit,
         additional_fading_exponent,
-    )
+        result_switch_pair,
+        attender_scaling_factor,
+        present_item_factor,
+    )
+    send, local_out, start_read, scale, extra = call(
+        local_kernel,
+        (
+            array((SHARES, LANES + HALF, LANES), bf16),
+            blocks,
+            array((4, TOK, 2 * LANES), bf16),
+            blocks,
+            blocks,
+        ),
+        [HBM] * len(inputs),
+        inputs,
+        66_400_000,
+    )(*inputs)
     planes = lax.axis_size("sp_0")
     prefix, total = call(
         row_kernel,
@@ -314,21 +403,14 @@
             array((SHARES, LANES + HALF, LANES), f32),
             array((planes, LANES + HALF, LANES), bf16),
         ),
+        [VMEM],
     )(exchange(send, ROW))
-    states = call(state_kernel, array((SHARES, HALF, LANES), bf16), 1)(
+    states = call(state_kernel, array((SHARES, HALF, LANES), bf16), [SMEM, VMEM, VMEM])(
         lax.axis_index("sp_0").astype(jnp.int32).reshape(1), exchange(total, "sp_0"), prefix
     )
-    partial_value = call(mix_kernel, array((TOK, features), bf16))(
-        local_out,
-        start_read,
-        exchange(states, ROW),
-        acceptance_query,
-        cluster_lookup_matrix,
-        cluster_payload_matrix,
-        result_switch_pair,
-        attender_scaling_factor,
-        present_item_factor,
-        final_mapping_matrix.reshape(-1, features),
+    mapping = final_mapping_matrix.reshape(-1, features)
+    partial_value = call(mix_kernel, array((TOK, features), bf16), [VMEM] * 5 + [HBM], (mapping,), 64_000_000)(
+        local_out, start_read, scale, extra, exchange(states, ROW), mapping
     )
     columns = features // lax.axis_size("tp")
     own_start = lax.axis_index("tp") * columns
@@ -340,11 +422,7 @@
         state_float * lax.rsqrt(mean_square + norm_epsilon) * perceptron_scaling_factor
     ).astype(bf16)
     own_state = lax.dynamic_slice_in_dim(state_float, own_start, columns, 1)
-    gate_pre = jnp.dot(normed, whole[:, :hidden], preferred_element_type=f32)
-    up_pre = jnp.dot(normed, whole[:, hidden : 2 * hidden], preferred_element_type=f32)
-    activated = (jax.nn.silu(gate_pre) * up_pre).astype(bf16)
-    down_terms = dot_nt(activated, whole[:, 2 * hidden :]).astype(bf16)
-    tiles = jnp.moveaxis(down_terms.reshape(TOK, features // columns, columns), 1, 0)
+    tiles = feed_forward(normed, whole, features // columns)
     mixer = jnp.sum(exchange(tiles, "tp").astype(f32), axis=0)
     return (own_state + mixer).astype(bf16)
 

time: 150 us -> 149 us (level)
  Pallas kernels: 9.18 us -> 25.2 us
  local copies, waits for them, and re-layouts: 14 us -> 2.41 us
  matrix products: 10.9 us -> 0 us
  waiting for transfers between devices: 30.9 us -> 37.5 us
  blocking collectives: 54.8 us -> 52.9 us
    pallas_call x4 -> x5, Pallas kernels: 9.18 us -> 25.2 us  [the longest x1 9.58 us: feed_forward(): pl.pallas_call(feed_kernel, out_shape=array((tiles, tokens, rows), bf16),...]
    unnamed x36 -> x4, local copies, waits for them, and re-layouts: 12.9 us -> 1.13 us
    dot_general x2 -> x0, matrix products: 10.9 us -> none  [the longest x1 7.27 us: dot_nt(): lax.dot_general(a, b, (((1,), (1,)), ((), ())), preferred_element_type=f32)]
    all_gather x1, waiting for transfers between devices: 5.98 us -> 9.83 us  [on_device(): lax.all_gather(jnp.concatenate([switching_matrix, widening_matrix, shrink...]
    all_to_all x2, waiting for transfers between devices: 24.9 us -> 27.7 us  [exchange(): return lax.all_to_all(value, axis, 0, 0, tiled=True)]
    all_to_all x3, blocking collectives: 54.8 us -> 52.9 us  [exchange(): return lax.all_to_all(value, axis, 0, 0, tiled=True)]
  transfers between devices with their start and end apart: 3 -> 3, of which waited for: 3 -> 3; matrix products, arithmetic and copies ran while one was open for 1% -> 1% of each run, Pallas kernels for 6% -> 11%
where the time goes in v2:
time: 149 us; the launch traced here: 147 us
  blocking collectives  52.9 us (36%)
  waiting for transfers between devices  37.5 us (25%)
  Pallas kernels  25.2 us (17%)
  between operations  13.5 us (9%)
  starting transfers between devices  12.1 us (8%)
  other arithmetic  3.23 us (2%)
  local copies, waits for them, and re-layouts  2.41 us (2%)
    all_to_all x3, blocking collectives, exchange(): return lax.all_to_all(value, axis, 0, 0, tiled=True)  52.9 us
    all_to_all x2, waiting for transfers between devices, exchange(): return lax.all_to_all(value, axis, 0, 0, tiled=True)  27.7 us
    all_to_all x2, starting transfers between devices, exchange(): return lax.all_to_all(value, axis, 0, 0, tiled=True)  12.1 us
    all_gather x1, waiting for transfers between devices, on_device(): lax.all_gather(jnp.concatenate([switching_matrix, widening_matrix, shrink...  9.83 us
    pallas_call x1, Pallas kernels, feed_forward(): pl.pallas_call(feed_kernel, out_shape=array((tiles, tokens, rows), bf16),...  9.58 us
    pallas_call x1, Pallas kernels, on_device(): call(local_kernel, (array((SHARES, LANES + HALF, LANES), bf16), blocks, a...  8.73 us
    pallas_call x1, Pallas kernels, on_device(): call(mix_kernel, array((TOK, features), bf16), [VMEM] * 5 + [HBM], (mappi...  4.05 us
  transfers between devices with their start and end apart: 3, of which 3 were waited for; matrix products, arithmetic and copies ran while one was open for 1% of the time, Pallas kernels for 11%

profile of v2, /device:TPU:2, one launch (start us, length us, event | category | flops | bytes accessed | tf_op | source)
XLA Modules:
  0.0 146.7 jit_solution(13030872128095184324)
XLA Ops:
  6.5 0.0 all-gather.2.cloned.1.call-start
  6.5 1.7 %pad_maximum_fusion = bf16[32,4224]{1,0:T(8,128)(2,1)} fusion(bf16[32,1408]{1,0:T(8,128)(2,1)} %bitcast.4, bf16[32,1408]{1,0:T(8,128)(2,1)} %param.28, bf16[32,1408]{1,0:T(8,128)(2,1)} %param.27), kind=kLoop, calls=%fused_computation.6 | loop fusion | flops 811008 | bytes 540672 | tf_op jit(solution)/shard_map/concatenate | solution.py:369
  8.2 0.0 all-gather.2.cloned.1.call-update
  8.3 8.7 %shard_map.145 = (bf16[8,192,128]{2,1,0:T(8,128)(2,1)}, f32[4,128,128]{2,1,0:T(8,128)}, bf16[4,128,256]{2,1,0:T(8,128)(2,1)}, f32[4,128,128]{2,1,0:T(8,128)}, f32[4,128,128]{2,1,0:T(8,128)}) custom-call(bf16[2,128,256]{2,1,0:T(8,128)(2,1)} %refs_0_.1, bf16[2,128,256]{2,1,0:T(8,128)(2,1)} %refs_1_.1, bf16[2,128,256]{2,1,0:T(8,128)(2,1)} %refs_2_.1, ...), custom_call_target="tpu_custom_call" | custom-call | tf_op jit(solution)/shard_map/pallas_call | solution.py:386
  17.0 14.6 %all_to_all.25.got_ref = bf16[8,192,128]{2,1,0:T(8,128)(2,1)S(1)} all-to-all(bf16[8,192,128]{2,1,0:T(8,128)(2,1)} %get-tuple-element.16), channel_id=1, replica_groups=mesh['sp_0'=8,'sp_1'=4,'sp_2'=2,'tp'=4] {'sp_1','sp_2'}, dimensions={0} | all-to-all | bytes 786432 | tf_op jit(solution)/shard_map/all_to_all | solution.py:342
  31.6 1.7 %shard_map.146 = (f32[8,192,128]{2,1,0:T(8,128)S(1)}, bf16[8,192,128]{2,1,0:T(8,128)(2,1)}) custom-call(bf16[8,192,128]{2,1,0:T(8,128)(2,1)S(1)} %all_to_all.25.got_ref), custom_call_target="tpu_custom_call" | custom-call | tf_op jit(solution)/shard_map/pallas_call | solution.py:400
  33.3 7.8 %all-to-all-start.1 = ((bf16[8,192,128]{2,1,0:T(8,128)(2,1)}), bf16[8,192,128]{2,1,0:T(8,128)(2,1)S(1)}, u32[]{:S(2)}, u32[]{:S(2)}) async-start(bf16[8,192,128]{2,1,0:T(8,128)(2,1)} %get-tuple-element.17), calls=%async_computation.1 | async-start | bytes 786432 | tf_op jit(solution)/shard_map/all_to_all | solution.py:342
  41.1 17.8 %all-to-all-done.1.every_ref = bf16[8,192,128]{2,1,0:T(8,128)(2,1)S(1)} async-done(((bf16[8,192,128]{2,1,0:T(8,128)(2,1)}), bf16[8,192,128]{2,1,0:T(8,128)(2,1)S(1)}, u32[]{:S(2)}, u32[]{:S(2)}) %all-to-all-start.1) | async-done | bytes 393248 | tf_op jit(solution)/shard_map/all_to_all | solution.py:342
  58.9 1.1 shard_map.147
  60.0 8.2 %all_to_all.26.state_ref = bf16[8,64,128]{2,1,0:T(8,128)(2,1)} all-to-all(bf16[8,64,128]{2,1,0:T(8,128)(2,1)S(1)} %shard_map.147), channel_id=1, replica_groups=mesh['sp_0'=8,'sp_1'=4,'sp_2'=2,'tp'=4] {'sp_1','sp_2'}, dimensions={0} | all-to-all | bytes 262144 | tf_op jit(solution)/shard_map/all_to_all | solution.py:342
  68.1 4.0 %shard_map.148 = bf16[128,2048]{1,0:T(8,128)(2,1)} custom-call(f32[4,128,128]{2,1,0:T(8,128)} %get-tuple-element.12.out_ref, bf16[4,128,256]{2,1,0:T(8,128)(2,1)} %get-tuple-element.13.read_ref, f32[4,128,128]{2,1,0:T(8,128)} %get-tuple-element.14.scale_ref, f32[4,128,128]{2,1,0:T(8,128)} %get-tuple-element.15.extra_ref, ...), custom_call_target="tpu_custom_call" | custom-call | tf_op jit(solution)/shard_map/pallas_call | solution.py:412
  72.2 1.3 broadcast_in_dim.2
  73.5 30.1 %all_to_all.27 = bf16[4,128,2048]{2,1,0:T(8,128)(2,1)S(1)} all-to-all(bf16[4,128,2048]{2,1,0:T(8,128)(2,1)S(1)} %broadcast_in_dim.2), channel_id=1, replica_groups=mesh['sp_0'=8,'sp_1'=4,'sp_2'=2,'tp'=4] {'tp'}, dimensions={0} | all-to-all | bytes 4194304 | tf_op jit(solution)/shard_map/all_to_all | solution.py:342
  103.6 0.0 copy-start
  103.6 0.4 convert_reduce_fusion
  104.0 0.7 copy-done
  104.6 0.0 copy-start.1
  104.6 0.2 multiply_reduce_fusion
  104.9 0.5 copy-done.1
  105.3 0.2 multiply_convert_fusion.x_ref
  105.5 9.8 %all-gather.2.cloned.1.call-done.whole_ref = bf16[2048,4224]{1,0:T(8,128)(2,1)} async-done(((bf16[32,4224]{1,0:T(8,128)(2,1)}), bf16[2048,4224]{1,0:T(8,128)(2,1)}) %all-gather.2.cloned.1.call-update) | async-done | bytes 17301520 | tf_op jit(solution)/shard_map/all_gather | solution.py:368
  115.3 9.6 %shard_map.149 = bf16[4,128,512]{2,1,0:T(8,128)(2,1)} custom-call(bf16[128,2048]{1,0:T(8,128)(2,1)S(1)} %multiply_convert_fusion.x_ref, bf16[2048,4224]{1,0:T(8,128)(2,1)} %all-gather.2.cloned.1.call-done.whole_ref), custom_call_target="tpu_custom_call" | custom-call | tf_op jit(solution)/shard_map/pallas_call | solution.py:303
  124.9 4.3 %all-to-all-start.4 = ((bf16[4,128,512]{2,1,0:T(8,128)(2,1)}), bf16[4,128,512]{2,1,0:T(8,128)(2,1)S(1)}, u32[]{:S(2)}, u32[]{:S(2)}) async-start(bf16[4,128,512]{2,1,0:T(8,128)(2,1)} %shard_map.149), calls=%async_computation.4 | async-start | bytes 1048576 | tf_op jit(solution)/shard_map/all_to_all | solution.py:342
  129.2 9.9 %all-to-all-done.4 = bf16[4,128,512]{2,1,0:T(8,128)(2,1)S(1)} async-done(((bf16[4,128,512]{2,1,0:T(8,128)(2,1)}), bf16[4,128,512]{2,1,0:T(8,128)(2,1)S(1)}, u32[]{:S(2)}, u32[]{:S(2)}) %all-to-all-start.4) | async-done | bytes 524320 | tf_op jit(solution)/shard_map/all_to_all | solution.py:342
  139.1 0.1 convert_reduce_fusion.1
  139.2 0.7 add_convert_fusion.1
  (1 shorter events, 0.0 us)
Async XLA Ops:
  6.5 108.8 %all-gather.2.cloned.1.call-start = ((), (), s32[]{:S(2)}) async-start(), calls=%async_computation.5 | async-start | bytes 17571840 | tf_op jit(solution)/shard_map/all_gather | solution.py:368
  33.3 25.6 %all-to-all-start.1 = ((bf16[8,192,128]{2,1,0:T(8,128)(2,1)}), bf16[8,192,128]{2,1,0:T(8,128)(2,1)S(1)}, u32[]{:S(2)}, u32[]{:S(2)}) async-start(bf16[8,192,128]{2,1,0:T(8,128)(2,1)} %get-tuple-element.17), calls=%async_computation.1 | async-start | bytes 786432 | tf_op jit(solution)/shard_map/all_to_all | solution.py:342
  103.6 1.1 copy-start
  104.6 0.7 copy-start.1
  124.9 14.2 %all-to-all-start.4 = ((bf16[4,128,512]{2,1,0:T(8,128)(2,1)}), bf16[4,128,512]{2,1,0:T(8,128)(2,1)S(1)}, u32[]{:S(2)}, u32[]{:S(2)}) async-start(bf16[4,128,512]{2,1,0:T(8,128)(2,1)} %shard_map.149), calls=%async_computation.4 | async-start | bytes 1048576 | tf_op jit(solution)/shard_map/all_to_all | solution.py:342
Sparse Core Ops, SparseCore 0:
  10.1 105.2 all-gather.1

commit v3 on v2

--- a/solution.py
+++ b/solution.py
@@ -6,8 +6,11 @@
 from jax.sharding import Mesh
 from jax.sharding import PartitionSpec as P
 
-SP = ("sp_0", "sp_1", "sp_2")
-ROW = ("sp_1", "sp_2")
+PLANE, FAR, NEAR, CORE, TP = "plane", "far", "near", "core", "tp"
+SP = (PLANE, FAR, NEAR, CORE)
+ROW = (FAR, NEAR, CORE)
+GATHER = (PLANE, NEAR, CORE)
+POOL = (FAR, TP)
 TOK = 128
 LANES = 128
 HALF = 64
@@ -240,10 +243,12 @@
         send_ref[k] = (moved + prefix_ref[k, LANES:, :]).astype(bf16)
 
 
-def mix_kernel(
-    out_ref, read_ref, scale_ref, extra_ref, state_ref, weight_ref, y_ref, w_ref, sems
-):
-    (copy,) = fetch([weight_ref], [w_ref], sems)
+def mix_kernel(*refs):
+    inputs, y_ref, scratch, sems = refs[:6], refs[6], refs[7:13], refs[13]
+    out_ref, read_ref, scale_ref, extra_ref, state_ref, w_ref = scratch
+    copies = fetch(inputs, scratch, sems)
+    for copy in copies[:5]:
+        copy.wait()
     mixed = []
     for slot in range(4):
         width = HALF if slot < 2 else LANES
@@ -254,65 +259,110 @@
         variance = head_sum(centered * centered, masks) * (1.0 / width)
         normed = centered * lax.rsqrt(variance + head_epsilon) * scale_ref[slot]
         mixed.append((normed + extra_ref[slot]).astype(bf16))
-    copy.wait()
-    y_ref[...] = dot_nn(jnp.concatenate(mixed, 1), w_ref[...]).astype(bf16)
+    mixed = jnp.concatenate(mixed, 1)
+    copies[5].wait()
+    tiles, _, columns = y_ref.shape
+    for k in range(tiles):
+        y_ref[k] = dot_nn(mixed, w_ref[:, k * columns : (k + 1) * columns]).astype(bf16)
 
 
 AHEAD = 4
 
 
-def feed_kernel(x_ref, whole_ref, y_ref, pair_ref, down_ref, act_ref, sems):
-    hidden = whole_ref.shape[1] // 3
-    steps = hidden // LANES
-    tiles, _, rows = y_ref.shape
-    waves = []
-    for k in range(steps):
-        for part in range(2):
-            lanes = pl.ds(part * hidden + k * LANES, LANES)
-            target = pair_ref.at[k, :, pl.ds(part * LANES, LANES)]
-            waves.append((whole_ref.at[:, lanes], target))
+def feed_kernel(far_ref, x_ref, gain_ref, whole_ref, y_ref, w_ref, n_ref, acc_ref, sems):
+    planes, sides, near, rows, width = w_ref.shape
+    third = width // 3
+    far = far_ref[0]
+    copies = [
+        [
+            pltpu.make_async_copy(
+                whole_ref.at[k, :, jnp.where(far == side, 0, 1)],
+                w_ref.at[k, side],
+                sems.at[k, side],
+            )
+            for side in range(sides)
+        ]
+        for k in range(planes)
+    ]
+    for k in range(AHEAD):
+        for copy in copies[k]:
+            copy.start()
+    shares, tokens, columns = x_ref.shape
+    tiles = shares // sides
+    for side in range(sides):
+        parts = [x_ref[side * tiles + k].astype(f32) for k in range(tiles)]
+        total = sum(jnp.sum(a * a, axis=1, keepdims=True) for a in parts)
+        scale = lax.rsqrt(total * (1.0 / (tiles * columns)) + norm_epsilon)
+        for k, a in enumerate(parts):
+            lanes = slice(k * columns, (k + 1) * columns)
+            n_ref[side * tokens : (side + 1) * tokens, lanes] = (
+                a * scale * gain_ref[:, lanes]
+            ).astype(bf16)
+    block = sides * near * rows
+    for k in range(0, planes, 2):
+        for step in (k, k + 1):
+            for copy in copies[step]:
+                copy.wait()
+            if step + AHEAD < planes:
+                for copy in copies[step + AHEAD]:
+                    copy.start()
+        part = dot_nn(
+            n_ref[:, k * block : (k + 2) * block],
+            w_ref[k : k + 2, :, :, :, : 2 * third].reshape(2 * block, 2 * third),
+        )
+        if k == 0:
+            acc_ref[...] = part
+        else:
+            acc_ref[...] += part
+    gate = acc_ref[:, :third]
+    active = (gate / (1.0 + jnp.exp(-gate)) * acc_ref[:, third:]).astype(bf16)
+    per = planes // tiles
     for k in range(tiles):
-        waves.append((whole_ref.at[pl.ds(k * rows, rows), pl.ds(2 * hidden, hidden)], down_ref.at[k]))
-    copies = [pltpu.make_async_copy(a, b, sems.at[k]) for k, (a, b) in enumerate(waves)]
-    for copy in copies[: 2 * AHEAD]:
-        copy.start()
-    sent = 2 * AHEAD
-    x = x_ref[...]
-    for k in range(steps):
-        copies[2 * k].wait()
-        copies[2 * k + 1].wait()
-        for _ in range(2):
-            if sent < len(copies):
-                copies[sent].start()
-                sent += 1
-        both = dot_nn(x, pair_ref[k])
-        gate = both[:, :LANES]
-        active = gate / (1.0 + jnp.exp(-gate)) * both[:, LANES:]
-        act_ref[:, k * LANES : (k + 1) * LANES] = active.astype(bf16)
-    active = act_ref[...]
-    for k in range(tiles):
-        copies[2 * steps + k].wait()
-        y_ref[k] = dot_nt(active, down_ref[k]).astype(bf16)
-
-
-def feed_forward(normed, whole, tiles):
-    tokens, features = normed.shape
-    hidden = whole.shape[1] // 3
-    steps = hidden // LANES
-    rows = features // tiles
+        down = w_ref[k * per : (k + 1) * per, :, :, :, 2 * third :].reshape(per * block, third)
+        out = dot_nt(active, down).astype(bf16)
+        for side in range(sides):
+            y_ref[side * tiles + k] = out[side * tokens : (side + 1) * tokens]
+
+
+def feed_forward(far, state, gain, whole):
+    planes, near, sides, rows, width = whole.shape
+    shares, tokens, columns = state.shape
     return pl.pallas_call(
         feed_kernel,
-        out_shape=array((tiles, tokens, rows), bf16),
-        in_specs=[VMEM, HBM],
+        out_shape=array((shares, tokens, columns), bf16),
+        in_specs=[SMEM, VMEM, VMEM, HBM],
         out_specs=VMEM,
         scratch_shapes=[
-            pltpu.VMEM((steps, features, 2 * LANES), bf16),
-            pltpu.VMEM((tiles, rows, hidden), bf16),
-            pltpu.VMEM((tokens, hidden), bf16),
-            pltpu.SemaphoreType.DMA((2 * steps + tiles,)),
+            pltpu.VMEM((planes, sides, near, rows, width), bf16),
+            pltpu.VMEM((sides * tokens, gain.shape[1]), bf16),
+            pltpu.VMEM((sides * tokens, 2 * width // 3), f32),
+            pltpu.SemaphoreType.DMA((planes, sides)),
         ],
-        compiler_params=pltpu.CompilerParams(vmem_limit_bytes=40 * 1024 * 1024),
-    )(normed, whole)
+        compiler_params=pltpu.CompilerParams(vmem_limit_bytes=60_000_000),
+    )(far, state, gain, whole)
+
+
+def halved(value, side, wide):
+    part = value[:, side * wide : (side + 1) * wide]
+    return jnp.pad(part, ((0, 0), (0, wide - part.shape[1])))
+
+
+def swapped(parts):
+    rows, hidden = parts[0].shape
+    wide = -(-hidden // (2 * LANES)) * LANES
+    packed = [jnp.concatenate([halved(a, side, wide) for a in parts], axis=1) for side in range(2)]
+    first = lax.axis_index(FAR) == 0
+    kept = jnp.where(first, packed[0], packed[1])
+    given = jnp.where(first, packed[1], packed[0])
+    return kept, lax.ppermute(given, FAR, [(0, 1), (1, 0)])
+
+
+def gathered(kept, taken):
+    both = jnp.concatenate([kept, taken], axis=0)
+    whole = lax.all_gather(both, GATHER, axis=0, tiled=True)
+    planes = lax.axis_size(PLANE)
+    near = lax.axis_size(NEAR) * lax.axis_size(CORE)
+    return whole.reshape(planes, near, 2, *kept.shape)
 
 
 VMEM = pl.BlockSpec(memory_space=pltpu.VMEM)
@@ -343,7 +393,7 @@
 
 
 def from_everyone(value, axis):
-    devices = lax.axis_size(axis)
+    devices = lax.psum(1, axis)
     return exchange(jnp.broadcast_to(value[None], (devices, *value.shape)), axis)
 
 
@@ -365,12 +415,8 @@
     shrinking_matrix,
 ):
     features = perceptron_scaling_factor.shape[0]
-    whole = lax.all_gather(
-        jnp.concatenate([switching_matrix, widening_matrix, shrinking_matrix.T], axis=1),
-        SP,
-        axis=0,
-        tiled=True,
-    )
+    columns = features // lax.axis_size(TP)
+    kept, taken = swapped([switching_matrix, widening_matrix, shrinking_matrix.T])
     blocks = array((4, TOK, LANES), f32)
     inputs = (
         acceptance_query,
@@ -396,7 +442,9 @@
         inputs,
         66_400_000,
     )(*inputs)
-    planes = lax.axis_size("sp_0")
+    send, taken = lax.optimization_barrier((send, taken))
+    whole = gathered(kept, taken)
+    planes = lax.axis_size(PLANE)
     prefix, total = call(
         row_kernel,
         (
@@ -406,29 +454,40 @@
         [VMEM],
     )(exchange(send, ROW))
     states = call(state_kernel, array((SHARES, HALF, LANES), bf16), [SMEM, VMEM, VMEM])(
-        lax.axis_index("sp_0").astype(jnp.int32).reshape(1), exchange(total, "sp_0"), prefix
-    )
-    mapping = final_mapping_matrix.reshape(-1, features)
-    partial_value = call(mix_kernel, array((TOK, features), bf16), [VMEM] * 5 + [HBM], (mapping,), 64_000_000)(
-        local_out, start_read, scale, extra, exchange(states, ROW), mapping
-    )
-    columns = features // lax.axis_size("tp")
-    own_start = lax.axis_index("tp") * columns
-    residual_float = stratum_source_matrix.astype(f32)
-    attention = jnp.sum(from_everyone(partial_value, "tp").astype(f32), axis=0)
-    state_float = (residual_float + attention).astype(bf16).astype(f32)
-    mean_square = jnp.mean(state_float * state_float, axis=1, keepdims=True)
-    normed = (
-        state_float * lax.rsqrt(mean_square + norm_epsilon) * perceptron_scaling_factor
-    ).astype(bf16)
-    own_state = lax.dynamic_slice_in_dim(state_float, own_start, columns, 1)
-    tiles = feed_forward(normed, whole, features // columns)
-    mixer = jnp.sum(exchange(tiles, "tp").astype(f32), axis=0)
-    return (own_state + mixer).astype(bf16)
+        lax.axis_index(PLANE).astype(jnp.int32).reshape(1), exchange(total, PLANE), prefix
+    )
+    mixing = (
+        local_out,
+        start_read,
+        scale,
+        extra,
+        exchange(states, ROW),
+        final_mapping_matrix.reshape(-1, features),
+    )
+    terms = call(
+        mix_kernel,
+        array((features // columns, TOK, columns), bf16),
+        [HBM] * len(mixing),
+        mixing,
+        64_000_000,
+    )(*mixing)
+    residual = lax.dynamic_slice_in_dim(
+        stratum_source_matrix, lax.axis_index(TP) * columns, columns, 1
+    )
+    attention = jnp.sum(exchange(terms, TP).astype(f32), axis=0)
+    own_state = (residual.astype(f32) + attention).astype(bf16)
+    tiles = feed_forward(
+        lax.axis_index(FAR).astype(jnp.int32).reshape(1),
+        from_everyone(own_state, POOL),
+        perceptron_scaling_factor.reshape(1, features),
+        whole,
+    )
+    mixer = jnp.sum(exchange(tiles, POOL).astype(f32), axis=0)
+    return (own_state.astype(f32) + mixer).astype(bf16)
 
 
 def solution(mesh):
-    split = Mesh(mesh.devices.reshape(8, 4, 2, mesh.shape["tp"]), ("sp_0", "sp_1", "sp_2", "tp"))
+    split = Mesh(mesh.devices.reshape(8, 2, 2, 2, mesh.shape["tp"]), (*SP, TP))
     heads = P(None, SP, "tp")
     return jax.shard_map(
         on_device,
@@ -442,14 +501,14 @@
             heads,
             heads,
             heads,
-            P(None, "tp"),
-            P(None, "tp"),
-            P(None, "tp", None),
+            P(None, TP),
+            P(None, TP),
+            P(None, TP, None),
             P(),
-            P(SP, "tp"),
-            P(SP, "tp"),
-            P("tp", SP),
+            P(SP, TP),
+            P(SP, TP),
+            P(TP, SP),
         ),
-        out_specs=P(SP, "tp"),
+        out_specs=P(SP, TP),
         check_vma=False,
     )

time: 149 us -> 151 us (1.013)
  blocking collectives: 52.9 us -> 63 us
  waiting for transfers between devices: 37.5 us -> 28.2 us
  starting transfers between devices: 12.1 us -> 15.1 us
  Pallas kernels: 25.2 us -> 22.5 us
  local copies, waits for them, and re-layouts: 2.41 us -> 4.83 us
    all_to_all x3 -> x4, blocking collectives: 52.9 us -> 63 us  [exchange(): return lax.all_to_all(value, axis, 0, 0, tiled=True)]
    all_gather x1, waiting for transfers between devices: 9.83 us -> 0.01 us  [gathered(): whole = lax.all_gather(both, GATHER, axis=0, tiled=True)]
    slice x0 -> x6, local copies, waits for them, and re-layouts: none -> 4.75 us  [halved(): part = value[:, side * wide:(side + 1) * wide]]
    pallas_call x2, Pallas kernels: 13.6 us -> 10.9 us  [the longest x1 7.65 us: feed_forward(): pl.pallas_call(feed_kernel, out_shape=array((shares, tokens, columns), bf...]
    ppermute x0 -> x1, starting transfers between devices: none -> 2.21 us  [swapped(): return (kept, lax.ppermute(given, FAR, [(0, 1), (1, 0)]))]
  transfers between devices with their start and end apart: 3 -> 4, of which waited for: 3 -> 2; matrix products, arithmetic and copies ran while one was open for 1% -> 1% of each run, Pallas kernels for 11% -> 10%
where the time goes in v3:
time: 151 us; the launch traced here: 150 us
  blocking collectives  63 us (42%)
  waiting for transfers between devices  28.2 us (19%)
  Pallas kernels  22.5 us (15%)
  starting transfers between devices  15.1 us (10%)
  between operations  13.5 us (9%)
  local copies, waits for them, and re-layouts  4.83 us (3%)
  other arithmetic  2.62 us (2%)
    all_to_all x4, blocking collectives, exchange(): return lax.all_to_all(value, axis, 0, 0, tiled=True)  63 us
    all_to_all x2, waiting for transfers between devices, exchange(): return lax.all_to_all(value, axis, 0, 0, tiled=True)  28.2 us
    all_to_all x2, starting transfers between devices, exchange(): return lax.all_to_all(value, axis, 0, 0, tiled=True)  12.9 us
    pallas_call x1, Pallas kernels, on_device(): call(local_kernel, (array((SHARES, LANES + HALF, LANES), bf16), blocks, a...  8.72 us
    pallas_call x1, Pallas kernels, feed_forward(): pl.pallas_call(feed_kernel, out_shape=array((shares, tokens, columns), bf...  7.65 us
    slice x6, local copies, waits for them, and re-layouts, halved(): part = value[:, side * wide:(side + 1) * wide]  4.75 us
    pallas_call x1, Pallas kernels, on_device(): call(mix_kernel, array((features // columns, TOK, columns), bf16), [HBM]...  3.3 us
  transfers between devices with their start and end apart: 4, of which 2 were waited for; matrix products, arithmetic and copies ran while one was open for 1% of the time, Pallas kernels for 10%

profile of v3, /device:TPU:2, one launch (start us, length us, event | category | flops | bytes accessed | tf_op | source)
XLA Modules:
  0.0 149.7 jit_solution(7531756945226595198)
XLA Ops:
  6.5 0.0 all-gather.2.cloned.1.call-start
  6.5 0.8 slice.25
  7.3 0.8 slice.24
  8.1 0.8 slice.21
  8.9 0.8 slice.18
  9.7 0.8 slice.22
  10.5 0.8 slice.19
  11.3 0.1 broadcast_select_fusion
  11.3 2.2 %collective-permute-start = (bf16[32,2304]{1,0:T(8,128)(2,1)S(1)}, bf16[32,2304]{1,0:T(8,128)(2,1)S(1)}, u32[]{:S(2)}, u32[]{:S(2)}) collective-permute-start(bf16[32,2304]{1,0:T(8,128)(2,1)S(1)} %get-tuple-element.24), channel_id=1, source_target_pairs={{0,16},{16,0},{1,17},{17,1},{2,18},{18,2},{3,19},{19,3},{4,20},{20... | collective-permute-start | bytes 442376 | tf_op jit(solution)/shard_map/ppermute | solution.py:357
  13.6 8.7 %shard_map.145 = (bf16[8,192,128]{2,1,0:T(8,128)(2,1)}, f32[4,128,128]{2,1,0:T(8,128)}, bf16[4,128,256]{2,1,0:T(8,128)(2,1)}, f32[4,128,128]{2,1,0:T(8,128)}, f32[4,128,128]{2,1,0:T(8,128)}) custom-call(bf16[2,128,256]{2,1,0:T(8,128)(2,1)} %refs_0_.1, bf16[2,128,256]{2,1,0:T(8,128)(2,1)} %refs_1_.1, bf16[2,128,256]{2,1,0:T(8,128)(2,1)} %refs_2_.1, ...), custom_call_target="tpu_custom_call" | custom-call | tf_op jit(solution)/shard_map/pallas_call | solution.py:432
  22.3 0.0 collective-permute-done
  22.3 0.7 pad_maximum_fusion
  23.0 0.0 all-gather.2.cloned.1.call-update
  23.1 12.4 %all_to_all.30.got_ref = bf16[8,192,128]{2,1,0:T(8,128)(2,1)S(1)} all-to-all(bf16[8,192,128]{2,1,0:T(8,128)(2,1)} %get-tuple-element.19), channel_id=1, replica_groups=mesh['plane'=8,'far'=2,'near'=2,'core'=2,'tp'=4] {'far','near','core'}, dimensions={0} | all-to-all | bytes 786432 | tf_op jit(solution)/shard_map/all_to_all | solution.py:392
  35.4 1.7 %shard_map.146 = (f32[8,192,128]{2,1,0:T(8,128)S(1)}, bf16[8,192,128]{2,1,0:T(8,128)(2,1)}) custom-call(bf16[8,192,128]{2,1,0:T(8,128)(2,1)S(1)} %all_to_all.30.got_ref), custom_call_target="tpu_custom_call" | custom-call | tf_op jit(solution)/shard_map/pallas_call | solution.py:448
  37.1 8.3 %all-to-all-start.1 = ((bf16[8,192,128]{2,1,0:T(8,128)(2,1)}), bf16[8,192,128]{2,1,0:T(8,128)(2,1)S(1)}, u32[]{:S(2)}, u32[]{:S(2)}) async-start(bf16[8,192,128]{2,1,0:T(8,128)(2,1)} %get-tuple-element.20), calls=%async_computation.1 | async-start | bytes 786432 | tf_op jit(solution)/shard_map/all_to_all | solution.py:392
  45.5 19.3 %all-to-all-done.1.every_ref = bf16[8,192,128]{2,1,0:T(8,128)(2,1)S(1)} async-done(((bf16[8,192,128]{2,1,0:T(8,128)(2,1)}), bf16[8,192,128]{2,1,0:T(8,128)(2,1)S(1)}, u32[]{:S(2)}, u32[]{:S(2)}) %all-to-all-start.1) | async-done | bytes 393248 | tf_op jit(solution)/shard_map/all_to_all | solution.py:392
  64.8 1.1 shard_map.147
  65.9 10.7 %all_to_all.31.refs_4_ = bf16[8,64,128]{2,1,0:T(8,128)(2,1)} all-to-all(bf16[8,64,128]{2,1,0:T(8,128)(2,1)S(1)} %shard_map.147), channel_id=1, replica_groups=mesh['plane'=8,'far'=2,'near'=2,'core'=2,'tp'=4] {'far','near','core'}, dimensions={0} | all-to-all | bytes 262144 | tf_op jit(solution)/shard_map/all_to_all | solution.py:392
  76.6 3.3 %shard_map.148 = bf16[4,128,512]{2,1,0:T(8,128)(2,1)} custom-call(f32[4,128,128]{2,1,0:T(8,128)} %get-tuple-element.14.refs_0_, bf16[4,128,256]{2,1,0:T(8,128)(2,1)} %get-tuple-element.15.refs_1_, f32[4,128,128]{2,1,0:T(8,128)} %get-tuple-element.16.refs_2_, f32[4,128,128]{2,1,0:T(8,128)} %get-tuple-element.17.refs_3_, ...), custom_call_target="tpu_custom_call" | custom-call | tf_op jit(solution)/shard_map/pallas_call | solution.py:467
  79.9 4.5 %all-to-all-start.3 = ((bf16[4,128,512]{2,1,0:T(8,128)(2,1)}), bf16[4,128,512]{2,1,0:T(8,128)(2,1)S(1)}, u32[]{:S(2)}, u32[]{:S(2)}) async-start(bf16[4,128,512]{2,1,0:T(8,128)(2,1)} %shard_map.148), calls=%async_computation.3 | async-start | bytes 1048576 | tf_op jit(solution)/shard_map/all_to_all | solution.py:392
  84.4 8.9 %all-to-all-done.3 = bf16[4,128,512]{2,1,0:T(8,128)(2,1)S(1)} async-done(((bf16[4,128,512]{2,1,0:T(8,128)(2,1)}), bf16[4,128,512]{2,1,0:T(8,128)(2,1)S(1)}, u32[]{:S(2)}, u32[]{:S(2)}) %all-to-all-start.3) | async-done | bytes 524320 | tf_op jit(solution)/shard_map/all_to_all | solution.py:392
  93.3 0.1 convert_reduce_fusion.1
  93.4 0.9 add_convert_fusion.1
  94.3 0.1 broadcast_in_dim.2
  94.4 21.2 %all_to_all.32.x_ref = bf16[8,128,512]{2,1,0:T(8,128)(2,1)} all-to-all(bf16[8,128,512]{2,1,0:T(8,128)(2,1)S(1)} %broadcast_in_dim.2), channel_id=1, replica_groups=mesh['plane'=8,'far'=2,'near'=2,'core'=2,'tp'=4] {'far','tp'}, dimensions={0} | all-to-all | bytes 2097152 | tf_op jit(solution)/shard_map/all_to_all | solution.py:392
  115.6 0.0 all-gather.2.cloned.1.call-done
  115.6 7.6 %shard_map.149 = bf16[8,128,512]{2,1,0:T(8,128)(2,1)} custom-call(s32[1]{0:T(128)} %bitcast.3.far_ref, bf16[8,128,512]{2,1,0:T(8,128)(2,1)} %all_to_all.32.x_ref, f32[1,2048]{1,0:T(1,128)} %bitcast.10, bf16[8,4,2,32,2304]{4,3,2,1,0:T(8,128)(2,1)} %bitcast.6), custom_call_target="tpu_custom_call" | custom-call | tf_op jit(solution)/shard_map/pallas_call | solution.py:330
  123.2 18.7 %all_to_all.33 = bf16[8,128,512]{2,1,0:T(8,128)(2,1)S(1)} all-to-all(bf16[8,128,512]{2,1,0:T(8,128)(2,1)} %shard_map.149), channel_id=1, replica_groups=mesh['plane'=8,'far'=2,'near'=2,'core'=2,'tp'=4] {'far','tp'}, dimensions={0} | all-to-all | bytes 2097152 | tf_op jit(solution)/shard_map/all_to_all | solution.py:392
  142.0 0.1 convert_reduce_fusion
  142.1 0.7 add_convert_fusion
Async XLA Ops:
  6.5 109.0 %all-gather.2.cloned.1.call-start = ((), (), s32[]{:S(2)}) async-start(), calls=%async_computation.6 | async-start | bytes 9732096 | tf_op jit(solution)/shard_map/all_gather | solution.py:362
  11.3 10.9 %collective-permute-start = (bf16[32,2304]{1,0:T(8,128)(2,1)S(1)}, bf16[32,2304]{1,0:T(8,128)(2,1)S(1)}, u32[]{:S(2)}, u32[]{:S(2)}) collective-permute-start(bf16[32,2304]{1,0:T(8,128)(2,1)S(1)} %get-tuple-element.24), channel_id=1, source_target_pairs={{0,16},{16,0},{1,17},{17,1},{2,18},{18,2},{3,19},{19,3},{4,20},{20... | collective-permute-start | bytes 442376 | tf_op jit(solution)/shard_map/ppermute | solution.py:357
  37.1 27.6 %all-to-all-start.1 = ((bf16[8,192,128]{2,1,0:T(8,128)(2,1)}), bf16[8,192,128]{2,1,0:T(8,128)(2,1)S(1)}, u32[]{:S(2)}, u32[]{:S(2)}) async-start(bf16[8,192,128]{2,1,0:T(8,128)(2,1)} %get-tuple-element.20), calls=%async_computation.1 | async-start | bytes 786432 | tf_op jit(solution)/shard_map/all_to_all | solution.py:392
  79.9 13.4 %all-to-all-start.3 = ((bf16[4,128,512]{2,1,0:T(8,128)(2,1)}), bf16[4,128,512]{2,1,0:T(8,128)(2,1)S(1)}, u32[]{:S(2)}, u32[]{:S(2)}) async-start(bf16[4,128,512]{2,1,0:T(8,128)(2,1)} %shard_map.148), calls=%async_computation.3 | async-start | bytes 1048576 | tf_op jit(solution)/shard_map/all_to_all | solution.py:392
Sparse Core Ops, SparseCore 0:
  23.2 82.6 all-gather.1

commit v4 on v3

--- a/solution.py
+++ b/solution.py
@@ -84,11 +84,23 @@
 
 
 def local_kernel(*refs):
-    inputs, outputs, scratch, sems = refs[:9], refs[9:14], refs[14:23], refs[23]
-    send_ref, out_ref, read_ref, scale_ref, extra_ref = outputs
+    inputs, outputs, scratch, results = refs[:9], refs[9:14], refs[14:23], refs[23:28]
+    sems, out_sems = refs[28:]
+    send_ref, out_ref, read_ref, scale_ref, extra_ref = results
     q_ref, k_ref, v_ref, f_ref, l_ref, e_ref, gate_ref, gain_ref, own_ref = scratch
-    for copy in fetch(inputs, scratch, sems):
+    copies = fetch(inputs, scratch, sems)
+    for copy in copies:
         copy.wait()
+    pending = []
+
+    def put(which, slot, count):
+        part = pl.ds(slot * count, count)
+        copy = pltpu.make_async_copy(
+            results[which].at[part], outputs[which].at[part], out_sems.at[which, slot]
+        )
+        copy.start()
+        pending.append(copy)
+
     row = lax.broadcasted_iota(jnp.int32, (TOK, TOK), 0)
     col = lax.broadcasted_iota(jnp.int32, (TOK, TOK), 1)
     strict = row > col
@@ -113,6 +125,8 @@
         scale_ref[slot] = gain_ref[group : group + 1, lanes] * gate
         own = head_sum(q * k * own_ref[group : group + 1, lanes], masks)
         extra_ref[slot] = own * v * gate
+        put(3, slot, 1)
+        put(4, slot, 1)
         d0 = log_decay.astype(bf16)
         rest = log_decay - d0.astype(f32)
         d1 = rest.astype(bf16)
@@ -204,10 +218,15 @@
         for half in range(2):
             send_ref[2 * slot + half, :LANES, :] = transit
             send_ref[2 * slot + half, LANES:, :] = added[half * HALF : (half + 1) * HALF, :]
+        put(0, slot, 2)
         out_ref[slot] = local
         high, low = halves(part["grown"] + read)
         read_ref[slot, :, :LANES] = high
         read_ref[slot, :, LANES:] = low
+        put(1, slot, 1)
+        put(2, slot, 1)
+    for copy in pending:
+        copy.wait()
 
 
 def row_kernel(got_ref, prefix_ref, total_ref):
@@ -342,18 +361,29 @@
     )(far, state, gain, whole)
 
 
-def halved(value, side, wide):
-    part = value[:, side * wide : (side + 1) * wide]
-    return jnp.pad(part, ((0, 0), (0, wide - part.shape[1])))
-
-
-def swapped(parts):
+def pack_kernel(far_ref, *refs):
+    inputs, (kept_ref, given_ref), scratch, sems = refs[:3], refs[3:5], refs[5:8], refs[8]
+    copies = fetch(inputs, scratch, sems)
+    wide = kept_ref.shape[1] // 3
+    first = far_ref[0] == 0
+    for k, copy in enumerate(copies):
+        copy.wait()
+        lanes = slice(k * wide, (k + 1) * wide)
+        near = scratch[k][:, :wide]
+        rest = scratch[k][:, wide:]
+        blank = jnp.zeros((rest.shape[0], 2 * wide - scratch[k].shape[1]), bf16)
+        far = jnp.concatenate([rest, blank], axis=1)
+        kept_ref[:, lanes] = jnp.where(first, near, far)
+        given_ref[:, lanes] = jnp.where(first, far, near)
+
+
+def swapped(far, parts):
     rows, hidden = parts[0].shape
     wide = -(-hidden // (2 * LANES)) * LANES
-    packed = [jnp.concatenate([halved(a, side, wide) for a in parts], axis=1) for side in range(2)]
-    first = lax.axis_index(FAR) == 0
-    kept = jnp.where(first, packed[0], packed[1])
-    given = jnp.where(first, packed[1], packed[0])
+    packed = array((rows, 3 * wide), bf16)
+    kept, given = call(pack_kernel, (packed, packed), [SMEM] + [HBM] * 3, parts, 62_000_000)(
+        far, *parts
+    )
     return kept, lax.ppermute(given, FAR, [(0, 1), (1, 0)])
 
 
@@ -370,15 +400,21 @@
 SMEM = pl.BlockSpec(memory_space=pltpu.SMEM)
 
 
-def call(kernel, outs, specs, fetched=(), limit=24 * 1024 * 1024):
+def call(kernel, outs, specs, fetched=(), limit=24 * 1024 * 1024, written=0):
     scratch = [pltpu.VMEM(a.shape, a.dtype) for a in fetched]
-    if scratch:
-        scratch.append(pltpu.SemaphoreType.DMA((len(scratch),)))
+    where = VMEM
+    if written:
+        where = HBM
+        scratch += [pltpu.VMEM(a.shape, a.dtype) for a in outs]
+    if fetched:
+        scratch.append(pltpu.SemaphoreType.DMA((len(fetched),)))
+    if written:
+        scratch.append(pltpu.SemaphoreType.DMA((len(outs), written)))
     return pl.pallas_call(
         kernel,
         out_shape=outs,
         in_specs=specs,
-        out_specs=jax.tree.map(lambda _: VMEM, outs),
+        out_specs=jax.tree.map(lambda _: where, outs),
         scratch_shapes=scratch,
         compiler_params=pltpu.CompilerParams(vmem_limit_bytes=limit),
     )
@@ -416,7 +452,8 @@
 ):
     features = perceptron_scaling_factor.shape[0]
     columns = features // lax.axis_size(TP)
-    kept, taken = swapped([switching_matrix, widening_matrix, shrinking_matrix.T])
+    far = lax.axis_index(FAR).astype(jnp.int32).reshape(1)
+    kept, taken = swapped(far, [switching_matrix, widening_matrix, shrinking_matrix.T])
     blocks = array((4, TOK, LANES), f32)
     inputs = (
         acceptance_query,
@@ -441,6 +478,7 @@
         [HBM] * len(inputs),
         inputs,
         66_400_000,
+        4,
     )(*inputs)
     send, taken = lax.optimization_barrier((send, taken))
     whole = gathered(kept, taken)
@@ -477,7 +515,7 @@
     attention = jnp.sum(exchange(terms, TP).astype(f32), axis=0)
     own_state = (residual.astype(f32) + attention).astype(bf16)
     tiles = feed_forward(
-        lax.axis_index(FAR).astype(jnp.int32).reshape(1),
+        far,
         from_everyone(own_state, POOL),
         perceptron_scaling_factor.reshape(1, features),
         whole,

time: 151 us -> 148 us (0.980)
  local copies, waits for them, and re-layouts: 4.83 us -> 0.08 us
  Pallas kernels: 22.5 us -> 24.3 us
    slice x6 -> x0, local copies, waits for them, and re-layouts: 4.75 us -> none  [halved(): part = value[:, side * wide:(side + 1) * wide]]
    pallas_call x0 -> x1, Pallas kernels: none -> 1.73 us  [swapped(): call(pack_kernel, (packed, packed), [SMEM] + [HBM] * 3, parts, 62000000)]
where the time goes in v4:
time: 148 us
  blocking collectives  62.6 us (42%)
  waiting for transfers between devices  28.5 us (19%)
  Pallas kernels  24.3 us (16%)
  starting transfers between devices  15.1 us (10%)
  between operations  13.5 us (9%)
  other arithmetic  3.49 us (2%)
    all_to_all x4, blocking collectives, exchange(): return lax.all_to_all(value, axis, 0, 0, tiled=True)  62.6 us
    all_to_all x2, waiting for transfers between devices, exchange(): return lax.all_to_all(value, axis, 0, 0, tiled=True)  28.5 us
    all_to_all x2, starting transfers between devices, exchange(): return lax.all_to_all(value, axis, 0, 0, tiled=True)  12.9 us
    pallas_call x1, Pallas kernels, on_device(): call(local_kernel, (array((SHARES, LANES + HALF, LANES), bf16), blocks, a...  8.83 us
    pallas_call x1, Pallas kernels, feed_forward(): pl.pallas_call(feed_kernel, out_shape=array((shares, tokens, columns), bf...  7.64 us
    pallas_call x1, Pallas kernels, on_device(): call(mix_kernel, array((features // columns, TOK, columns), bf16), [HBM]...  3.3 us
  transfers between devices with their start and end apart: 4, of which 2 were waited for; matrix products, arithmetic and copies ran while one was open for 1% of the time, Pallas kernels for 10%

profile of v4, /device:TPU:2, one launch (start us, length us, event | category | flops | bytes accessed | tf_op | source)
XLA Modules:
  0.0 147.6 jit_solution(1937431313964998883)
XLA Ops:
  6.5 0.0 all-gather.2.cloned.1.call-start
  6.5 1.7 %shard_map.146 = (bf16[32,2304]{1,0:T(8,128)(2,1)}, bf16[32,2304]{1,0:T(8,128)(2,1)}) custom-call(s32[1]{0:T(128)} %bitcast.1.far_ref, bf16[32,1408]{1,0:T(8,128)(2,1)} %refs_0_.3, bf16[32,1408]{1,0:T(8,128)(2,1)} %refs_1_.3, bf16[32,1408]{1,0:T(8,128)(2,1)} %bitcast.8), custom_call_target="tpu_custom_call" | custom-call | tf_op jit(solution)/shard_map/pallas_call | solution.py:384
  8.3 2.2 %collective-permute-start = (bf16[32,2304]{1,0:T(8,128)(2,1)}, bf16[32,2304]{1,0:T(8,128)(2,1)S(1)}, u32[]{:S(2)}, u32[]{:S(2)}) collective-permute-start(bf16[32,2304]{1,0:T(8,128)(2,1)} %get-tuple-element.21), channel_id=1, source_target_pairs={{0,16},{16,0},{1,17},{17,1},{2,18},{18,2},{3,19},{19,3},{4,20},{20... | collective-permute-start | bytes 442376 | tf_op jit(solution)/shard_map/ppermute | solution.py:387
  10.5 8.8 %shard_map.145 = (bf16[8,192,128]{2,1,0:T(8,128)(2,1)}, f32[4,128,128]{2,1,0:T(8,128)}, bf16[4,128,256]{2,1,0:T(8,128)(2,1)}, f32[4,128,128]{2,1,0:T(8,128)}, f32[4,128,128]{2,1,0:T(8,128)}) custom-call(bf16[2,128,256]{2,1,0:T(8,128)(2,1)} %refs_0_.2, bf16[2,128,256]{2,1,0:T(8,128)(2,1)} %refs_1_.2, bf16[2,128,256]{2,1,0:T(8,128)(2,1)} %refs_2_.1, ...), custom_call_target="tpu_custom_call" | custom-call | tf_op jit(solution)/shard_map/pallas_call | solution.py:469
  19.3 0.0 collective-permute-done
  19.3 1.6 %pad_maximum_fusion = bf16[64,2304]{1,0:T(8,128)(2,1)} fusion(bf16[32,2304]{1,0:T(8,128)(2,1)S(1)} %collective-permute-done, bf16[32,2304]{1,0:T(8,128)(2,1)} %get-tuple-element.25), kind=kLoop, calls=%fused_computation.2 | loop fusion | flops 589824 | bytes 589824 | tf_op jit(solution)/shard_map/concatenate | solution.py:391
  21.0 0.0 all-gather.2.cloned.1.call-update
  21.0 12.4 %all_to_all.30.got_ref = bf16[8,192,128]{2,1,0:T(8,128)(2,1)S(1)} all-to-all(bf16[8,192,128]{2,1,0:T(8,128)(2,1)} %get-tuple-element.22), channel_id=1, replica_groups=mesh['plane'=8,'far'=2,'near'=2,'core'=2,'tp'=4] {'far','near','core'}, dimensions={0} | all-to-all | bytes 786432 | tf_op jit(solution)/shard_map/all_to_all | solution.py:428
  33.4 1.7 %shard_map.147 = (f32[8,192,128]{2,1,0:T(8,128)S(1)}, bf16[8,192,128]{2,1,0:T(8,128)(2,1)}) custom-call(bf16[8,192,128]{2,1,0:T(8,128)(2,1)S(1)} %all_to_all.30.got_ref), custom_call_target="tpu_custom_call" | custom-call | tf_op jit(solution)/shard_map/pallas_call | solution.py:486
  35.1 8.3 %all-to-all-start.1 = ((bf16[8,192,128]{2,1,0:T(8,128)(2,1)}), bf16[8,192,128]{2,1,0:T(8,128)(2,1)S(1)}, u32[]{:S(2)}, u32[]{:S(2)}) async-start(bf16[8,192,128]{2,1,0:T(8,128)(2,1)} %get-tuple-element.23), calls=%async_computation.1 | async-start | bytes 786432 | tf_op jit(solution)/shard_map/all_to_all | solution.py:428
  43.4 19.3 %all-to-all-done.1.every_ref = bf16[8,192,128]{2,1,0:T(8,128)(2,1)S(1)} async-done(((bf16[8,192,128]{2,1,0:T(8,128)(2,1)}), bf16[8,192,128]{2,1,0:T(8,128)(2,1)S(1)}, u32[]{:S(2)}, u32[]{:S(2)}) %all-to-all-start.1) | async-done | bytes 393248 | tf_op jit(solution)/shard_map/all_to_all | solution.py:428
  62.7 1.1 shard_map.148
  63.8 10.6 %all_to_all.31.refs_4_ = bf16[8,64,128]{2,1,0:T(8,128)(2,1)} all-to-all(bf16[8,64,128]{2,1,0:T(8,128)(2,1)S(1)} %shard_map.148), channel_id=1, replica_groups=mesh['plane'=8,'far'=2,'near'=2,'core'=2,'tp'=4] {'far','near','core'}, dimensions={0} | all-to-all | bytes 262144 | tf_op jit(solution)/shard_map/all_to_all | solution.py:428
  74.5 3.3 %shard_map.149 = bf16[4,128,512]{2,1,0:T(8,128)(2,1)} custom-call(f32[4,128,128]{2,1,0:T(8,128)} %get-tuple-element.16.refs_0_, bf16[4,128,256]{2,1,0:T(8,128)(2,1)} %get-tuple-element.17.refs_1_, f32[4,128,128]{2,1,0:T(8,128)} %get-tuple-element.18.refs_2_, f32[4,128,128]{2,1,0:T(8,128)} %get-tuple-element.19.refs_3_, ...), custom_call_target="tpu_custom_call" | custom-call | tf_op jit(solution)/shard_map/pallas_call | solution.py:505
  77.8 4.6 %all-to-all-start.3 = ((bf16[4,128,512]{2,1,0:T(8,128)(2,1)}), bf16[4,128,512]{2,1,0:T(8,128)(2,1)S(1)}, u32[]{:S(2)}, u32[]{:S(2)}) async-start(bf16[4,128,512]{2,1,0:T(8,128)(2,1)} %shard_map.149), calls=%async_computation.3 | async-start | bytes 1048576 | tf_op jit(solution)/shard_map/all_to_all | solution.py:428
  82.4 9.2 %all-to-all-done.3 = bf16[4,128,512]{2,1,0:T(8,128)(2,1)S(1)} async-done(((bf16[4,128,512]{2,1,0:T(8,128)(2,1)}), bf16[4,128,512]{2,1,0:T(8,128)(2,1)S(1)}, u32[]{:S(2)}, u32[]{:S(2)}) %all-to-all-start.3) | async-done | bytes 524320 | tf_op jit(solution)/shard_map/all_to_all | solution.py:428
  91.6 0.1 convert_reduce_fusion.1
  91.6 0.9 add_convert_fusion.1
  92.6 0.1 broadcast_in_dim.2
  92.7 20.9 %all_to_all.32.x_ref = bf16[8,128,512]{2,1,0:T(8,128)(2,1)} all-to-all(bf16[8,128,512]{2,1,0:T(8,128)(2,1)S(1)} %broadcast_in_dim.2), channel_id=1, replica_groups=mesh['plane'=8,'far'=2,'near'=2,'core'=2,'tp'=4] {'far','tp'}, dimensions={0} | all-to-all | bytes 2097152 | tf_op jit(solution)/shard_map/all_to_all | solution.py:428
  113.6 0.0 all-gather.2.cloned.1.call-done
  113.6 7.6 %shard_map.150 = bf16[8,128,512]{2,1,0:T(8,128)(2,1)} custom-call(s32[1]{0:T(128)} %bitcast.1.far_ref, bf16[8,128,512]{2,1,0:T(8,128)(2,1)} %all_to_all.32.x_ref, f32[1,2048]{1,0:T(1,128)} %bitcast.9, bf16[8,4,2,32,2304]{4,3,2,1,0:T(8,128)(2,1)} %bitcast.6), custom_call_target="tpu_custom_call" | custom-call | tf_op jit(solution)/shard_map/pallas_call | solution.py:349
  121.2 18.7 %all_to_all.33 = bf16[8,128,512]{2,1,0:T(8,128)(2,1)S(1)} all-to-all(bf16[8,128,512]{2,1,0:T(8,128)(2,1)} %shard_map.150), channel_id=1, replica_groups=mesh['plane'=8,'far'=2,'near'=2,'core'=2,'tp'=4] {'far','tp'}, dimensions={0} | all-to-all | bytes 2097152 | tf_op jit(solution)/shard_map/all_to_all | solution.py:428
  139.9 0.1 convert_reduce_fusion
  140.1 0.7 add_convert_fusion
Async XLA Ops:
  6.5 107.1 %all-gather.2.cloned.1.call-start = ((), (), s32[]{:S(2)}) async-start(), calls=%async_computation.6 | async-start | bytes 9732096 | tf_op jit(solution)/shard_map/all_gather | solution.py:392
  8.3 11.1 %collective-permute-start = (bf16[32,2304]{1,0:T(8,128)(2,1)}, bf16[32,2304]{1,0:T(8,128)(2,1)S(1)}, u32[]{:S(2)}, u32[]{:S(2)}) collective-permute-start(bf16[32,2304]{1,0:T(8,128)(2,1)} %get-tuple-element.21), channel_id=1, source_target_pairs={{0,16},{16,0},{1,17},{17,1},{2,18},{18,2},{3,19},{19,3},{4,20},{20... | collective-permute-start | bytes 442376 | tf_op jit(solution)/shard_map/ppermute | solution.py:387
  35.1 27.6 %all-to-all-start.1 = ((bf16[8,192,128]{2,1,0:T(8,128)(2,1)}), bf16[8,192,128]{2,1,0:T(8,128)(2,1)S(1)}, u32[]{:S(2)}, u32[]{:S(2)}) async-start(bf16[8,192,128]{2,1,0:T(8,128)(2,1)} %get-tuple-element.23), calls=%async_computation.1 | async-start | bytes 786432 | tf_op jit(solution)/shard_map/all_to_all | solution.py:428
  77.8 13.8 %all-to-all-start.3 = ((bf16[4,128,512]{2,1,0:T(8,128)(2,1)}), bf16[4,128,512]{2,1,0:T(8,128)(2,1)S(1)}, u32[]{:S(2)}, u32[]{:S(2)}) async-start(bf16[4,128,512]{2,1,0:T(8,128)(2,1)} %shard_map.149), calls=%async_computation.3 | async-start | bytes 1048576 | tf_op jit(solution)/shard_map/all_to_all | solution.py:428
Sparse Core Ops, SparseCore 0:
  21.1 82.8 all-gather.1

commit v5 on v4

--- a/solution.py
+++ b/solution.py
@@ -85,12 +85,17 @@
 
 def local_kernel(*refs):
     inputs, outputs, scratch, results = refs[:9], refs[9:14], refs[14:23], refs[23:28]
-    sems, out_sems = refs[28:]
+    sems, small_sems, out_sems = refs[28:]
     send_ref, out_ref, read_ref, scale_ref, extra_ref = results
     q_ref, k_ref, v_ref, f_ref, l_ref, e_ref, gate_ref, gain_ref, own_ref = scratch
-    copies = fetch(inputs, scratch, sems)
+    copies = [
+        pltpu.make_async_copy(a.at[group], b.at[group], sems.at[k, group])
+        for group in range(2)
+        for k, (a, b) in enumerate(zip(inputs[:7], scratch[:7]))
+    ]
+    small = fetch(inputs[7:], scratch[7:], small_sems)
     for copy in copies:
-        copy.wait()
+        copy.start()
     pending = []
 
     def put(which, slot, count):
@@ -111,6 +116,10 @@
     heads = []
     for slot in range(4):
         group, cut = slot // 2, (slot % 2) * LANES
+        if cut == 0:
+            for copy in copies[group * 7 : group * 7 + 7] + small:
+                copy.wait()
+            small = []
         lanes = slice(cut, cut + LANES)
         q = q_ref[group, :, lanes].astype(f32)
         k = k_ref[group, :, lanes].astype(f32)
@@ -400,14 +409,13 @@
 SMEM = pl.BlockSpec(memory_space=pltpu.SMEM)
 
 
-def call(kernel, outs, specs, fetched=(), limit=24 * 1024 * 1024, written=0):
+def call(kernel, outs, specs, fetched=(), limit=24 * 1024 * 1024, written=0, sems=()):
     scratch = [pltpu.VMEM(a.shape, a.dtype) for a in fetched]
     where = VMEM
     if written:
         where = HBM
         scratch += [pltpu.VMEM(a.shape, a.dtype) for a in outs]
-    if fetched:
-        scratch.append(pltpu.SemaphoreType.DMA((len(fetched),)))
+    scratch += [pltpu.SemaphoreType.DMA(a) for a in sems or [(len(fetched),)] if fetched]
     if written:
         scratch.append(pltpu.SemaphoreType.DMA((len(outs), written)))
     return pl.pallas_call(
@@ -479,8 +487,11 @@
         inputs,
         66_400_000,
         4,
+        [(7, 2), (2,)],
     )(*inputs)
-    send, taken = lax.optimization_barrier((send, taken))
+    place = lax.axis_index(PLANE).astype(jnp.int32).reshape(1)
+    first_column = (lax.axis_index(TP) * columns).astype(jnp.uint32)
+    send, taken, place, first_column = lax.optimization_barrier((send, taken, place, first_column))
     whole = gathered(kept, taken)
     planes = lax.axis_size(PLANE)
     prefix, total = call(
@@ -492,7 +503,7 @@
         [VMEM],
     )(exchange(send, ROW))
     states = call(state_kernel, array((SHARES, HALF, LANES), bf16), [SMEM, VMEM, VMEM])(
-        lax.axis_index(PLANE).astype(jnp.int32).reshape(1), exchange(total, PLANE), prefix
+        place, exchange(total, PLANE), prefix
     )
     mixing = (
         local_out,
@@ -509,8 +520,8 @@
         mixing,
         64_000_000,
     )(*mixing)
-    residual = lax.dynamic_slice_in_dim(
-        stratum_source_matrix, lax.axis_index(TP) * columns, columns, 1
+    residual = lax.dynamic_slice(
+        stratum_source_matrix, (jnp.uint32(0), first_column), (TOK, columns)
     )
     attention = jnp.sum(exchange(terms, TP).astype(f32), axis=0)
     own_state = (residual.astype(f32) + attention).astype(bf16)

time: 148 us -> 148 us (level)
  blocking collectives: 62.6 us -> 105 us
  waiting for transfers between devices: 28.5 us -> 0.02 us
  starting transfers between devices: 15.1 us -> 2.21 us
    all_to_all x4 -> x6, blocking collectives: 62.6 us -> 105 us  [exchange(): return lax.all_to_all(value, axis, 0, 0, tiled=True)]
    all_to_all x2 -> x0, waiting for transfers between devices: 28.5 us -> none  [exchange(): return lax.all_to_all(value, axis, 0, 0, tiled=True)]
    all_to_all x2 -> x0, starting transfers between devices: 12.9 us -> none  [exchange(): return lax.all_to_all(value, axis, 0, 0, tiled=True)]
  transfers between devices with their start and end apart: 4 -> 2, of which waited for: 2 -> 0; matrix products, arithmetic and copies ran while one was open for 1% -> 1% of each run, Pallas kernels for 10% -> 10%
where the time goes in v5:
time: 148 us
  blocking collectives  105 us (71%)
  Pallas kernels  23.5 us (16%)
  between operations  13.5 us (9%)
  other arithmetic  3.58 us (2%)
  starting transfers between devices  2.21 us (1%)
    all_to_all x6, blocking collectives, exchange(): return lax.all_to_all(value, axis, 0, 0, tiled=True)  105 us
    pallas_call x1, Pallas kernels, on_device(): call(local_kernel, (array((SHARES, LANES + HALF, LANES), bf16), blocks, a...  8.77 us
    pallas_call x1, Pallas kernels, feed_forward(): pl.pallas_call(feed_kernel, out_shape=array((shares, tokens, columns), bf...  7.64 us
    pallas_call x1, Pallas kernels, on_device(): call(mix_kernel, array((features // columns, TOK, columns), bf16), [HBM]...  3.33 us
  transfers between devices with their start and end apart: 2, of which 0 were waited for; matrix products, arithmetic and copies ran while one was open for 1% of the time, Pallas kernels for 10%

profile of v5, /device:TPU:2, one launch (start us, length us, event | category | flops | bytes accessed | tf_op | source)
XLA Modules:
  0.0 147.9 jit_solution(7218226907864521357)
XLA Ops:
  6.5 0.0 all-gather.2.cloned.1.call-start
  6.5 1.7 %shard_map.146 = (bf16[32,2304]{1,0:T(8,128)(2,1)}, bf16[32,2304]{1,0:T(8,128)(2,1)}) custom-call(s32[1]{0:T(128)} %bitcast.far_ref, bf16[32,1408]{1,0:T(8,128)(2,1)} %refs_0_.3, bf16[32,1408]{1,0:T(8,128)(2,1)} %refs_1_.3, bf16[32,1408]{1,0:T(8,128)(2,1)} %bitcast.8), custom_call_target="tpu_custom_call" | custom-call | tf_op jit(solution)/shard_map/pallas_call | solution.py:393
  8.3 2.2 %collective-permute-start = (bf16[32,2304]{1,0:T(8,128)(2,1)}, bf16[32,2304]{1,0:T(8,128)(2,1)S(1)}, u32[]{:S(2)}, u32[]{:S(2)}) collective-permute-start(bf16[32,2304]{1,0:T(8,128)(2,1)} %get-tuple-element.19), channel_id=1, source_target_pairs={{0,16},{16,0},{1,17},{17,1},{2,18},{18,2},{3,19},{19,3},{4,20},{20... | collective-permute-start | bytes 442376 | tf_op jit(solution)/shard_map/ppermute | solution.py:396
  10.5 8.8 %shard_map.145 = (bf16[8,192,128]{2,1,0:T(8,128)(2,1)}, f32[4,128,128]{2,1,0:T(8,128)}, bf16[4,128,256]{2,1,0:T(8,128)(2,1)}, f32[4,128,128]{2,1,0:T(8,128)}, f32[4,128,128]{2,1,0:T(8,128)}) custom-call(bf16[2,128,256]{2,1,0:T(8,128)(2,1)} %refs_0_.2, bf16[2,128,256]{2,1,0:T(8,128)(2,1)} %refs_1_.2, bf16[2,128,256]{2,1,0:T(8,128)(2,1)} %refs_2_.1, ...), custom_call_target="tpu_custom_call" | custom-call | tf_op jit(solution)/shard_map/pallas_call | solution.py:477
  19.3 0.0 collective-permute-done
  19.3 1.7 %pad_maximum_fusion = bf16[64,2304]{1,0:T(8,128)(2,1)} fusion(bf16[32,2304]{1,0:T(8,128)(2,1)S(1)} %collective-permute-done, bf16[32,2304]{1,0:T(8,128)(2,1)} %get-tuple-element.29), kind=kLoop, calls=%fused_computation.2 | loop fusion | flops 589824 | bytes 589824 | tf_op jit(solution)/shard_map/concatenate | solution.py:400
  20.9 0.0 all-gather.2.cloned.1.call-update
  21.0 12.4 %all_to_all.30.got_ref = bf16[8,192,128]{2,1,0:T(8,128)(2,1)S(1)} all-to-all(bf16[8,192,128]{2,1,0:T(8,128)(2,1)} %get-tuple-element.26), channel_id=1, replica_groups=mesh['plane'=8,'far'=2,'near'=2,'core'=2,'tp'=4] {'far','near','core'}, dimensions={0} | all-to-all | bytes 786432 | tf_op jit(solution)/shard_map/all_to_all | solution.py:436
  33.3 0.9 shard_map.147
  34.3 27.3 %all_to_all.31.every_ref = bf16[8,192,128]{2,1,0:T(8,128)(2,1)S(1)} all-to-all(bf16[8,192,128]{2,1,0:T(8,128)(2,1)S(1)} %get-tuple-element.27), channel_id=1, replica_groups=mesh['plane'=8,'far'=2,'near'=2,'core'=2,'tp'=4] {'plane'}, dimensions={0} | all-to-all | bytes 786432 | tf_op jit(solution)/shard_map/all_to_all | solution.py:436
  61.5 1.1 shard_map.148
  62.7 10.7 %all_to_all.32.refs_4_ = bf16[8,64,128]{2,1,0:T(8,128)(2,1)} all-to-all(bf16[8,64,128]{2,1,0:T(8,128)(2,1)S(1)} %shard_map.148), channel_id=1, replica_groups=mesh['plane'=8,'far'=2,'near'=2,'core'=2,'tp'=4] {'far','near','core'}, dimensions={0} | all-to-all | bytes 262144 | tf_op jit(solution)/shard_map/all_to_all | solution.py:436
  73.4 3.3 %shard_map.149 = bf16[4,128,512]{2,1,0:T(8,128)(2,1)} custom-call(f32[4,128,128]{2,1,0:T(8,128)} %get-tuple-element.21.refs_0_, bf16[4,128,256]{2,1,0:T(8,128)(2,1)} %get-tuple-element.22.refs_1_, f32[4,128,128]{2,1,0:T(8,128)} %get-tuple-element.23.refs_2_, f32[4,128,128]{2,1,0:T(8,128)} %get-tuple-element.24.refs_3_, ...), custom_call_target="tpu_custom_call" | custom-call | tf_op jit(solution)/shard_map/pallas_call | solution.py:516
  76.8 13.4 %all_to_all.33 = bf16[4,128,512]{2,1,0:T(8,128)(2,1)S(1)} all-to-all(bf16[4,128,512]{2,1,0:T(8,128)(2,1)} %shard_map.149), channel_id=1, replica_groups=mesh['plane'=8,'far'=2,'near'=2,'core'=2,'tp'=4] {'tp'}, dimensions={0} | all-to-all | bytes 1048576 | tf_op jit(solution)/shard_map/all_to_all | solution.py:436
  90.2 0.1 convert_reduce_fusion.1
  90.3 1.0 add_convert_fusion.1
  91.3 0.1 broadcast_in_dim.2
  91.4 22.0 %all_to_all.34.x_ref = bf16[8,128,512]{2,1,0:T(8,128)(2,1)} all-to-all(bf16[8,128,512]{2,1,0:T(8,128)(2,1)S(1)} %broadcast_in_dim.2), channel_id=1, replica_groups=mesh['plane'=8,'far'=2,'near'=2,'core'=2,'tp'=4] {'far','tp'}, dimensions={0} | all-to-all | bytes 2097152 | tf_op jit(solution)/shard_map/all_to_all | solution.py:436
  113.4 0.0 all-gather.2.cloned.1.call-done
  113.4 7.6 %shard_map.150 = bf16[8,128,512]{2,1,0:T(8,128)(2,1)} custom-call(s32[1]{0:T(128)} %bitcast.far_ref, bf16[8,128,512]{2,1,0:T(8,128)(2,1)} %all_to_all.34.x_ref, f32[1,2048]{1,0:T(1,128)} %bitcast.9, bf16[8,4,2,32,2304]{4,3,2,1,0:T(8,128)(2,1)} %bitcast.6), custom_call_target="tpu_custom_call" | custom-call | tf_op jit(solution)/shard_map/pallas_call | solution.py:358
  121.0 19.2 %all_to_all.35 = bf16[8,128,512]{2,1,0:T(8,128)(2,1)S(1)} all-to-all(bf16[8,128,512]{2,1,0:T(8,128)(2,1)} %shard_map.150), channel_id=1, replica_groups=mesh['plane'=8,'far'=2,'near'=2,'core'=2,'tp'=4] {'far','tp'}, dimensions={0} | all-to-all | bytes 2097152 | tf_op jit(solution)/shard_map/all_to_all | solution.py:436
  140.2 0.1 convert_reduce_fusion
  140.4 0.7 add_convert_fusion
Async XLA Ops:
  6.5 106.8 %all-gather.2.cloned.1.call-start = ((), (), s32[]{:S(2)}) async-start(), calls=%async_computation.6 | async-start | bytes 9732096 | tf_op jit(solution)/shard_map/all_gather | solution.py:401
  8.3 11.0 %collective-permute-start = (bf16[32,2304]{1,0:T(8,128)(2,1)}, bf16[32,2304]{1,0:T(8,128)(2,1)S(1)}, u32[]{:S(2)}, u32[]{:S(2)}) collective-permute-start(bf16[32,2304]{1,0:T(8,128)(2,1)} %get-tuple-element.19), channel_id=1, source_target_pairs={{0,16},{16,0},{1,17},{17,1},{2,18},{18,2},{3,19},{19,3},{4,20},{20... | collective-permute-start | bytes 442376 | tf_op jit(solution)/shard_map/ppermute | solution.py:396
Sparse Core Ops, SparseCore 0:
  21.1 83.1 all-gather.1

commit v6 on v5

--- a/solution.py
+++ b/solution.py
@@ -9,8 +9,6 @@
 PLANE, FAR, NEAR, CORE, TP = "plane", "far", "near", "core", "tp"
 SP = (PLANE, FAR, NEAR, CORE)
 ROW = (FAR, NEAR, CORE)
-GATHER = (PLANE, NEAR, CORE)
-POOL = (FAR, TP)
 TOK = 128
 LANES = 128
 HALF = 64
@@ -297,46 +295,38 @@
 AHEAD = 4
 
 
-def feed_kernel(far_ref, x_ref, gain_ref, whole_ref, y_ref, w_ref, n_ref, acc_ref, sems):
-    planes, sides, near, rows, width = w_ref.shape
+def feed_kernel(x_ref, gain_ref, whole_ref, y_ref, w_ref, n_ref, acc_ref, sems):
+    blocks, rows, width = w_ref.shape
     third = width // 3
-    far = far_ref[0]
+    parts = [pl.ds(0, 2 * third), pl.ds(2 * third, third)]
+    waves = [(k, part) for part in range(2) for k in range(blocks)]
     copies = [
-        [
-            pltpu.make_async_copy(
-                whole_ref.at[k, :, jnp.where(far == side, 0, 1)],
-                w_ref.at[k, side],
-                sems.at[k, side],
-            )
-            for side in range(sides)
-        ]
-        for k in range(planes)
+        pltpu.make_async_copy(
+            whole_ref.at[k, :, parts[part]], w_ref.at[k, :, parts[part]], sems.at[part, k]
+        )
+        for k, part in waves
     ]
-    for k in range(AHEAD):
-        for copy in copies[k]:
-            copy.start()
-    shares, tokens, columns = x_ref.shape
-    tiles = shares // sides
-    for side in range(sides):
-        parts = [x_ref[side * tiles + k].astype(f32) for k in range(tiles)]
-        total = sum(jnp.sum(a * a, axis=1, keepdims=True) for a in parts)
-        scale = lax.rsqrt(total * (1.0 / (tiles * columns)) + norm_epsilon)
-        for k, a in enumerate(parts):
-            lanes = slice(k * columns, (k + 1) * columns)
-            n_ref[side * tokens : (side + 1) * tokens, lanes] = (
-                a * scale * gain_ref[:, lanes]
-            ).astype(bf16)
-    block = sides * near * rows
-    for k in range(0, planes, 2):
-        for step in (k, k + 1):
-            for copy in copies[step]:
-                copy.wait()
-            if step + AHEAD < planes:
-                for copy in copies[step + AHEAD]:
-                    copy.start()
+    for copy in copies[:AHEAD]:
+        copy.start()
+    tiles, tokens, columns = x_ref.shape
+    states = [x_ref[k].astype(f32) for k in range(tiles)]
+    total = sum(jnp.sum(a * a, axis=1, keepdims=True) for a in states)
+    scale = lax.rsqrt(total * (1.0 / (tiles * columns)) + norm_epsilon)
+    for k, a in enumerate(states):
+        lanes = slice(k * columns, (k + 1) * columns)
+        n_ref[:, lanes] = (a * scale * gain_ref[:, lanes]).astype(bf16)
+
+    def arrive(k):
+        copies[k].wait()
+        if k + AHEAD < len(copies):
+            copies[k + AHEAD].start()
+
+    for k in range(0, blocks, 2):
+        arrive(k)
+        arrive(k + 1)
         part = dot_nn(
-            n_ref[:, k * block : (k + 2) * block],
-            w_ref[k : k + 2, :, :, :, : 2 * third].reshape(2 * block, 2 * third),
+            n_ref[:, k * rows : (k + 2) * rows],
+            w_ref[k : k + 2, :, : 2 * third].reshape(2 * rows, 2 * third),
         )
         if k == 0:
             acc_ref[...] = part
@@ -344,64 +334,30 @@
             acc_ref[...] += part
     gate = acc_ref[:, :third]
     active = (gate / (1.0 + jnp.exp(-gate)) * acc_ref[:, third:]).astype(bf16)
-    per = planes // tiles
+    per = blocks // tiles
     for k in range(tiles):
-        down = w_ref[k * per : (k + 1) * per, :, :, :, 2 * third :].reshape(per * block, third)
-        out = dot_nt(active, down).astype(bf16)
-        for side in range(sides):
-            y_ref[side * tiles + k] = out[side * tokens : (side + 1) * tokens]
-
-
-def feed_forward(far, state, gain, whole):
-    planes, near, sides, rows, width = whole.shape
-    shares, tokens, columns = state.shape
+        for step in range(k * per, (k + 1) * per):
+            arrive(blocks + step)
+        down = w_ref[k * per : (k + 1) * per, :, 2 * third :].reshape(per * rows, third)
+        y_ref[k] = dot_nt(active, down).astype(bf16)
+
+
+def feed_forward(state, gain, whole):
+    tiles, tokens, columns = state.shape
+    blocks, rows, width = whole.shape
     return pl.pallas_call(
         feed_kernel,
-        out_shape=array((shares, tokens, columns), bf16),
-        in_specs=[SMEM, VMEM, VMEM, HBM],
+        out_shape=array((tiles, tokens, columns), bf16),
+        in_specs=[VMEM, VMEM, HBM],
         out_specs=VMEM,
         scratch_shapes=[
-            pltpu.VMEM((planes, sides, near, rows, width), bf16),
-            pltpu.VMEM((sides * tokens, gain.shape[1]), bf16),
-            pltpu.VMEM((sides * tokens, 2 * width // 3), f32),
-            pltpu.SemaphoreType.DMA((planes, sides)),
+            pltpu.VMEM((blocks, rows, width), bf16),
+            pltpu.VMEM((tokens, gain.shape[1]), bf16),
+            pltpu.VMEM((tokens, 2 * width // 3), f32),
+            pltpu.SemaphoreType.DMA((2, blocks)),
         ],
         compiler_params=pltpu.CompilerParams(vmem_limit_bytes=60_000_000),
-    )(far, state, gain, whole)
-
-
-def pack_kernel(far_ref, *refs):
-    inputs, (kept_ref, given_ref), scratch, sems = refs[:3], refs[3:5], refs[5:8], refs[8]
-    copies = fetch(inputs, scratch, sems)
-    wide = kept_ref.shape[1] // 3
-    first = far_ref[0] == 0
-    for k, copy in enumerate(copies):
-        copy.wait()
-        lanes = slice(k * wide, (k + 1) * wide)
-        near = scratch[k][:, :wide]
-        rest = scratch[k][:, wide:]
-        blank = jnp.zeros((rest.shape[0], 2 * wide - scratch[k].shape[1]), bf16)
-        far = jnp.concatenate([rest, blank], axis=1)
-        kept_ref[:, lanes] = jnp.where(first, near, far)
-        given_ref[:, lanes] = jnp.where(first, far, near)
-
-
-def swapped(far, parts):
-    rows, hidden = parts[0].shape
-    wide = -(-hidden // (2 * LANES)) * LANES
-    packed = array((rows, 3 * wide), bf16)
-    kept, given = call(pack_kernel, (packed, packed), [SMEM] + [HBM] * 3, parts, 62_000_000)(
-        far, *parts
-    )
-    return kept, lax.ppermute(given, FAR, [(0, 1), (1, 0)])
-
-
-def gathered(kept, taken):
-    both = jnp.concatenate([kept, taken], axis=0)
-    whole = lax.all_gather(both, GATHER, axis=0, tiled=True)
-    planes = lax.axis_size(PLANE)
-    near = lax.axis_size(NEAR) * lax.axis_size(CORE)
-    return whole.reshape(planes, near, 2, *kept.shape)
+    )(state, gain, whole)
 
 
 VMEM = pl.BlockSpec(memory_space=pltpu.VMEM)
@@ -460,8 +416,13 @@
 ):
     features = perceptron_scaling_factor.shape[0]
     columns = features // lax.axis_size(TP)
-    far = lax.axis_index(FAR).astype(jnp.int32).reshape(1)
-    kept, taken = swapped(far, [switching_matrix, widening_matrix, shrinking_matrix.T])
+    planes = lax.axis_size(PLANE)
+    whole = lax.all_gather(
+        jnp.concatenate([switching_matrix, widening_matrix, shrinking_matrix.T], axis=1),
+        SP,
+        axis=0,
+        tiled=True,
+    )
     blocks = array((4, TOK, LANES), f32)
     inputs = (
         acceptance_query,
@@ -491,9 +452,7 @@
     )(*inputs)
     place = lax.axis_index(PLANE).astype(jnp.int32).reshape(1)
     first_column = (lax.axis_index(TP) * columns).astype(jnp.uint32)
-    send, taken, place, first_column = lax.optimization_barrier((send, taken, place, first_column))
-    whole = gathered(kept, taken)
-    planes = lax.axis_size(PLANE)
+    send, place, first_column = lax.optimization_barrier((send, place, first_column))
     prefix, total = call(
         row_kernel,
         (
@@ -526,12 +485,11 @@
     attention = jnp.sum(exchange(terms, TP).astype(f32), axis=0)
     own_state = (residual.astype(f32) + attention).astype(bf16)
     tiles = feed_forward(
-        far,
-        from_everyone(own_state, POOL),
+        from_everyone(own_state, TP),
         perceptron_scaling_factor.reshape(1, features),
-        whole,
-    )
-    mixer = jnp.sum(exchange(tiles, POOL).astype(f32), axis=0)
+        whole.reshape(planes, features // planes, -1),
+    )
+    mixer = jnp.sum(exchange(tiles, TP).astype(f32), axis=0)
     return (own_state.astype(f32) + mixer).astype(bf16)
 
 

time: 148 us -> 149 us (level)
  waiting for transfers between devices: 0.02 us -> 18 us
  blocking collectives: 105 us -> 88.5 us
  starting transfers between devices: 2.21 us -> 0.01 us
    all_gather x1, waiting for transfers between devices: 0.01 us -> 18 us  [on_device(): lax.all_gather(jnp.concatenate([switching_matrix, widening_matrix, shrink...]
    all_to_all x6, blocking collectives: 105 us -> 88.5 us  [exchange(): return lax.all_to_all(value, axis, 0, 0, tiled=True)]
    ppermute x1 -> x0, starting transfers between devices: 2.21 us -> none  [swapped(): return (kept, lax.ppermute(given, FAR, [(0, 1), (1, 0)]))]
    pallas_call x2 -> x1, Pallas kernels: 9.37 us -> 9.83 us  [feed_forward(): pl.pallas_call(feed_kernel, out_shape=array((tiles, tokens, columns), bf1...]
  transfers between devices with their start and end apart: 2 -> 1, of which waited for: 0 -> 1; matrix products, arithmetic and copies ran while one was open for 1% -> 1% of each run, Pallas kernels for 10% -> 10%
where the time goes in v6:
time: 149 us; the launch traced here: 148 us
  blocking collectives  88.5 us (59%)
  Pallas kernels  24 us (16%)
  waiting for transfers between devices  18 us (12%)
  between operations  13.5 us (9%)
  other arithmetic  3.57 us (2%)
    all_to_all x6, blocking collectives, exchange(): return lax.all_to_all(value, axis, 0, 0, tiled=True)  88.5 us
    all_gather x1, waiting for transfers between devices, on_device(): lax.all_gather(jnp.concatenate([switching_matrix, widening_matrix, shrink...  18 us
    pallas_call x1, Pallas kernels, feed_forward(): pl.pallas_call(feed_kernel, out_shape=array((tiles, tokens, columns), bf1...  9.83 us
    pallas_call x1, Pallas kernels, on_device(): call(local_kernel, (array((SHARES, LANES + HALF, LANES), bf16), blocks, a...  8.82 us
    pallas_call x1, Pallas kernels, on_device(): call(mix_kernel, array((features // columns, TOK, columns), bf16), [HBM]...  3.28 us
  transfers between devices with their start and end apart: 1, of which 1 were waited for; matrix products, arithmetic and copies ran while one was open for 1% of the time, Pallas kernels for 10%

profile of v6, /device:TPU:2, one launch (start us, length us, event | category | flops | bytes accessed | tf_op | source)
XLA Modules:
  0.0 147.6 jit_solution(15263256929628192235)
XLA Ops:
  6.5 0.0 all-gather.2.cloned.1.call-start
  6.5 1.7 %pad_maximum_fusion = bf16[32,4224]{1,0:T(8,128)(2,1)} fusion(bf16[32,1408]{1,0:T(8,128)(2,1)} %bitcast.7, bf16[32,1408]{1,0:T(8,128)(2,1)} %param.28, bf16[32,1408]{1,0:T(8,128)(2,1)} %param.27), kind=kLoop, calls=%fused_computation.2 | loop fusion | flops 811008 | bytes 540672 | tf_op jit(solution)/shard_map/concatenate | solution.py:421
  8.3 0.0 all-gather.2.cloned.1.call-update
  8.3 8.8 %shard_map.145 = (bf16[8,192,128]{2,1,0:T(8,128)(2,1)}, f32[4,128,128]{2,1,0:T(8,128)}, bf16[4,128,256]{2,1,0:T(8,128)(2,1)}, f32[4,128,128]{2,1,0:T(8,128)}, f32[4,128,128]{2,1,0:T(8,128)}) custom-call(bf16[2,128,256]{2,1,0:T(8,128)(2,1)} %refs_0_.1, bf16[2,128,256]{2,1,0:T(8,128)(2,1)} %refs_1_.1, bf16[2,128,256]{2,1,0:T(8,128)(2,1)} %refs_2_.1, ...), custom_call_target="tpu_custom_call" | custom-call | tf_op jit(solution)/shard_map/pallas_call | solution.py:438
  17.1 14.6 %all_to_all.30.got_ref = bf16[8,192,128]{2,1,0:T(8,128)(2,1)S(1)} all-to-all(bf16[8,192,128]{2,1,0:T(8,128)(2,1)} %get-tuple-element.22), channel_id=1, replica_groups=mesh['plane'=8,'far'=2,'near'=2,'core'=2,'tp'=4] {'far','near','core'}, dimensions={0} | all-to-all | bytes 786432 | tf_op jit(solution)/shard_map/all_to_all | solution.py:392
  31.7 0.9 shard_map.146
  32.7 24.6 %all_to_all.31.every_ref = bf16[8,192,128]{2,1,0:T(8,128)(2,1)S(1)} all-to-all(bf16[8,192,128]{2,1,0:T(8,128)(2,1)S(1)} %get-tuple-element.23), channel_id=1, replica_groups=mesh['plane'=8,'far'=2,'near'=2,'core'=2,'tp'=4] {'plane'}, dimensions={0} | all-to-all | bytes 786432 | tf_op jit(solution)/shard_map/all_to_all | solution.py:392
  57.3 1.1 shard_map.147
  58.5 9.6 %all_to_all.32.refs_4_ = bf16[8,64,128]{2,1,0:T(8,128)(2,1)} all-to-all(bf16[8,64,128]{2,1,0:T(8,128)(2,1)S(1)} %shard_map.147), channel_id=1, replica_groups=mesh['plane'=8,'far'=2,'near'=2,'core'=2,'tp'=4] {'far','near','core'}, dimensions={0} | all-to-all | bytes 262144 | tf_op jit(solution)/shard_map/all_to_all | solution.py:392
  68.0 3.3 %shard_map.148 = bf16[4,128,512]{2,1,0:T(8,128)(2,1)} custom-call(f32[4,128,128]{2,1,0:T(8,128)} %get-tuple-element.17.refs_0_, bf16[4,128,256]{2,1,0:T(8,128)(2,1)} %get-tuple-element.18.refs_1_, f32[4,128,128]{2,1,0:T(8,128)} %get-tuple-element.19.refs_2_, f32[4,128,128]{2,1,0:T(8,128)} %get-tuple-element.20.refs_3_, ...), custom_call_target="tpu_custom_call" | custom-call | tf_op jit(solution)/shard_map/pallas_call | solution.py:475
  71.3 13.9 %all_to_all.33 = bf16[4,128,512]{2,1,0:T(8,128)(2,1)S(1)} all-to-all(bf16[4,128,512]{2,1,0:T(8,128)(2,1)} %shard_map.148), channel_id=1, replica_groups=mesh['plane'=8,'far'=2,'near'=2,'core'=2,'tp'=4] {'tp'}, dimensions={0} | all-to-all | bytes 1048576 | tf_op jit(solution)/shard_map/all_to_all | solution.py:392
  85.3 0.1 convert_reduce_fusion.1
  85.3 1.0 add_convert_fusion.1
  86.4 11.5 %all_to_all.34.x_ref = bf16[4,128,512]{2,1,0:T(8,128)(2,1)} all-to-all(bf16[4,128,512]{2,1,0:T(8,128)(2,1)S(1)} %broadcast_in_dim.2), channel_id=1, replica_groups=mesh['plane'=8,'far'=2,'near'=2,'core'=2,'tp'=4] {'tp'}, dimensions={0} | all-to-all | bytes 1048576 | tf_op jit(solution)/shard_map/all_to_all | solution.py:392
  97.9 18.0 %all-gather.2.cloned.1.call-done = bf16[2048,4224]{1,0:T(8,128)(2,1)} async-done(((bf16[32,4224]{1,0:T(8,128)(2,1)}), bf16[2048,4224]{1,0:T(8,128)(2,1)}) %all-gather.2.cloned.1.call-update) | async-done | bytes 17301520 | tf_op jit(solution)/shard_map/all_gather | solution.py:420
  115.9 9.8 %shard_map.149 = bf16[4,128,512]{2,1,0:T(8,128)(2,1)} custom-call(bf16[4,128,512]{2,1,0:T(8,128)(2,1)} %all_to_all.34.x_ref, f32[1,2048]{1,0:T(1,128)} %bitcast.8, bf16[8,256,4224]{2,1,0:T(8,128)(2,1)} %bitcast.5), custom_call_target="tpu_custom_call" | custom-call | tf_op jit(solution)/shard_map/pallas_call | solution.py:348
  125.8 14.2 %all_to_all.35 = bf16[4,128,512]{2,1,0:T(8,128)(2,1)S(1)} all-to-all(bf16[4,128,512]{2,1,0:T(8,128)(2,1)} %shard_map.149), channel_id=1, replica_groups=mesh['plane'=8,'far'=2,'near'=2,'core'=2,'tp'=4] {'tp'}, dimensions={0} | all-to-all | bytes 1048576 | tf_op jit(solution)/shard_map/all_to_all | solution.py:392
  140.0 0.1 convert_reduce_fusion
  140.0 0.7 add_convert_fusion
  (1 shorter events, 0.0 us)
Async XLA Ops:
  6.5 109.4 %all-gather.2.cloned.1.call-start = ((), (), s32[]{:S(2)}) async-start(), calls=%async_computation.6 | async-start | bytes 17571840 | tf_op jit(solution)/shard_map/all_gather | solution.py:420
Sparse Core Ops, SparseCore 0:
  10.1 105.8 all-gather.1

commit v7 on v5

--- a/solution.py
+++ b/solution.py
@@ -53,12 +53,6 @@
     return dot_nt(jnp.concatenate([ah, al], 1), jnp.concatenate([bh, bh], 1)) + dot_nt(ah, bl)
 
 
-def mm_tn(a, b):
-    ah, al = a
-    bh, bl = b
-    return dot_tn(jnp.concatenate([ah, al], 0), jnp.concatenate([bh, bh], 0)) + dot_tn(ah, bl)
-
-
 def head_masks(group):
     lane = lax.broadcasted_iota(jnp.int32, (1, LANES), 1)
     if group == 0:
@@ -83,29 +77,49 @@
     return copies
 
 
-def local_kernel(*refs):
-    inputs, outputs, scratch, results = refs[:9], refs[9:14], refs[14:23], refs[23:28]
-    sems, small_sems, out_sems = refs[28:]
-    send_ref, out_ref, read_ref, scale_ref, extra_ref = results
-    q_ref, k_ref, v_ref, f_ref, l_ref, e_ref, gate_ref, gain_ref, own_ref = scratch
+def slot_lanes(slot):
+    cut = (slot % 2) * LANES
+    return slot // 2, slice(cut, cut + LANES)
+
+
+def group_copies(inputs, scratch, sems):
     copies = [
-        pltpu.make_async_copy(a.at[group], b.at[group], sems.at[k, group])
+        [
+            pltpu.make_async_copy(a.at[group], b.at[group], sems.at[k, group])
+            for k, (a, b) in enumerate(zip(inputs, scratch))
+        ]
         for group in range(2)
-        for k, (a, b) in enumerate(zip(inputs[:7], scratch[:7]))
     ]
-    small = fetch(inputs[7:], scratch[7:], small_sems)
-    for copy in copies:
+    for copy in copies[0] + copies[1]:
         copy.start()
+    return copies
+
+
+def writer(results, outputs, sems):
     pending = []
 
-    def put(which, slot, count):
-        part = pl.ds(slot * count, count)
+    def put(which, index, count):
+        part = pl.ds(index * count, count)
         copy = pltpu.make_async_copy(
-            results[which].at[part], outputs[which].at[part], out_sems.at[which, slot]
+            results[which].at[part], outputs[which].at[part], sems.at[which, index]
         )
         copy.start()
         pending.append(copy)
 
+    def finish():
+        for copy in pending:
+            copy.wait()
+
+    return put, finish
+
+
+def solve_kernel(*refs):
+    inputs, outputs, scratch, results = refs[:6], refs[6:11], refs[11:17], refs[17:22]
+    sems, out_sems = refs[22:]
+    send_ref, qr_ref, qk_ref, solved_ref, grown_ref = results
+    q_ref, k_ref, v_ref, f_ref, l_ref, e_ref = scratch
+    copies = group_copies(inputs, scratch, sems)
+    put, finish = writer(results, outputs, out_sems)
     row = lax.broadcasted_iota(jnp.int32, (TOK, TOK), 0)
     col = lax.broadcasted_iota(jnp.int32, (TOK, TOK), 1)
     strict = row > col
@@ -115,27 +129,18 @@
     slots = []
     heads = []
     for slot in range(4):
-        group, cut = slot // 2, (slot % 2) * LANES
-        if cut == 0:
-            for copy in copies[group * 7 : group * 7 + 7] + small:
+        group, lanes = slot_lanes(slot)
+        if slot % 2 == 0:
+            for copy in copies[group]:
                 copy.wait()
-            small = []
-        lanes = slice(cut, cut + LANES)
         q = q_ref[group, :, lanes].astype(f32)
         k = k_ref[group, :, lanes].astype(f32)
-        v = v_ref[group, :, lanes].astype(f32)
         fade = f_ref[group, :, lanes].astype(f32)
         speed = l_ref[group, :, lanes].astype(f32)
         log_decay = e_ref[group, :, lanes] - jnp.exp(-0.5) / (1.0 + jnp.exp(-fade))
         learn = 1.0 / (1.0 + jnp.exp(-speed))
         masks = head_masks(group)
         removal = k * lax.rsqrt(head_sum(k * k, masks) + key_epsilon)
-        gate = gate_ref[group, :, lanes].astype(f32)
-        scale_ref[slot] = gain_ref[group : group + 1, lanes] * gate
-        own = head_sum(q * k * own_ref[group : group + 1, lanes], masks)
-        extra_ref[slot] = own * v * gate
-        put(3, slot, 1)
-        put(4, slot, 1)
         d0 = log_decay.astype(bf16)
         rest = log_decay - d0.astype(f32)
         d1 = rest.astype(bf16)
@@ -148,33 +153,34 @@
         right = learn * removal
         queries = jnp.concatenate([-removal * undo * forward, q * forward], 0)
         sources = halves(jnp.concatenate([right * backward, k * backward], 0))
-        grown = jnp.exp(cum)
         final = cum[TOK - 1 : TOK, :]
         tail = jnp.exp(final - cum)
+        grown_ref[slot] = q * jnp.exp(cum)
+        put(4, slot, 1)
         slots.append(
             dict(
                 masks=masks,
-                v=halves(v),
+                v=v_ref[group, :, lanes],
                 start=-removal * jnp.exp(cum - log_decay),
-                grown=q * grown,
-                right=halves(right * tail),
-                keys=halves(k * tail),
+                ends=jnp.concatenate([right * tail, k * tail], 0).astype(bf16),
                 kept=jnp.exp(final),
-                heads=[],
             )
         )
         for mask in masks:
             pairs = mm_nt(halves(masked(queries, mask)), sources)
-            head = dict(
-                slot=slot,
-                mask=mask,
-                n=jnp.where(strict, pairs[:TOK, :TOK], 0.0),
-                rk=jnp.where(strict, pairs[:TOK, TOK:], 0.0),
-                qr=jnp.where(inclusive, pairs[TOK:, :TOK], 0.0),
-                qk=jnp.where(inclusive, pairs[TOK:, TOK:], 0.0),
+            head = len(heads)
+            qr_ref[head] = jnp.where(inclusive, pairs[TOK:, :TOK], 0.0).astype(bf16)
+            qk_ref[head] = jnp.where(inclusive, pairs[TOK:, TOK:], 0.0).astype(bf16)
+            put(1, head, 1)
+            put(2, head, 1)
+            heads.append(
+                dict(
+                    slot=slot,
+                    mask=mask,
+                    n=jnp.where(strict, pairs[:TOK, :TOK], 0.0),
+                    rk=jnp.where(strict, pairs[:TOK, TOK:], 0.0),
+                )
             )
-            heads.append(head)
-            slots[slot]["heads"].append(head)
     same = (row // 8) == (col // 8)
     for head in heads:
         head["m"] = jnp.where(same, head["n"], 0.0)
@@ -194,31 +200,27 @@
         for head in heads:
             head["x"] = head["x"] + mm(halves(head["x"]), head["y"])
         size *= 2
+    for head in heads:
+        part = slots[head["slot"]]
+        high, low = halves(head["rk"])
+        v = part["v"]
+        pulled = dot_nn(jnp.concatenate([high, low], 1), jnp.concatenate([v, v], 0))
+        head["solved"] = mm(
+            halves(head["x"]), halves(jnp.concatenate([pulled, part["start"]], 1))
+        )
     for slot, part in enumerate(slots):
-        carried = start = local = read = None
-        for head in part["heads"]:
-            mask = head["mask"]
-            target = jnp.concatenate([mm(halves(head["rk"]), part["v"]), part["start"]], 1)
-            solved = mm(halves(head["x"]), halves(target))
-            from_solved = mm(halves(head["qr"]), halves(solved))
-            pieces = [
-                masked(solved[:, :LANES], mask),
-                masked(solved[:, LANES:], mask),
-                masked(from_solved[:, :LANES] + mm(halves(head["qk"]), part["v"]), mask),
-                masked(from_solved[:, LANES:], mask),
-            ]
-            if carried is None:
-                carried, start, local, read = pieces
-            else:
-                carried, start, local, read = (
-                    carried + pieces[0],
-                    start + pieces[1],
-                    local + pieces[2],
-                    read + pieces[3],
-                )
-        transit = mm_tn(halves(start), part["right"])
-        added = mm_tn(halves(carried), part["right"]) + mm_tn(part["v"], part["keys"])
-        if len(part["heads"]) == 2:
+        mine = [head for head in heads if head["slot"] == slot]
+        solved = mine[0]["solved"]
+        if len(mine) == 2:
+            first = jnp.concatenate([mine[0]["mask"]] * 2, 1) > 0.5
+            solved = jnp.where(first, solved, mine[1]["solved"])
+        solved = solved.astype(bf16)
+        solved_ref[slot] = solved
+        put(3, slot, 1)
+        carried, start = solved[:, :LANES], solved[:, LANES:]
+        transit = dot_tn(start, part["ends"][:TOK])
+        added = dot_tn(jnp.concatenate([carried, part["v"]], 0), part["ends"])
+        if len(mine) == 2:
             block = (row // HALF) == (col // HALF)
             transit = jnp.where(block, transit, 0.0)
             added = jnp.where(block, added, 0.0)
@@ -228,14 +230,45 @@
             send_ref[2 * slot + half, :LANES, :] = transit
             send_ref[2 * slot + half, LANES:, :] = added[half * HALF : (half + 1) * HALF, :]
         put(0, slot, 2)
+    finish()
+
+
+def read_kernel(*refs):
+    inputs, outputs, scratch, results = refs[:10], refs[10:14], refs[14:24], refs[24:28]
+    sems, out_sems = refs[28:]
+    qr_ref, qk_ref, solved_ref, grown_ref, q_ref, k_ref, v_ref, gate_ref, gain_ref, own_ref = scratch
+    out_ref, read_ref, scale_ref, extra_ref = results
+    for copy in fetch(inputs, scratch, sems):
+        copy.wait()
+    put, finish = writer(results, outputs, out_sems)
+    head = 0
+    for slot in range(4):
+        group, lanes = slot_lanes(slot)
+        masks = head_masks(group)
+        v = v_ref[group, :, lanes]
+        found = local = None
+        for mask in masks:
+            one = dot_nn(qr_ref[head], solved_ref[slot])
+            here = one[:, :LANES] + dot_nn(qk_ref[head], v)
+            if found is None:
+                found, local = one[:, LANES:], here
+            else:
+                found = jnp.where(mask > 0.5, one[:, LANES:], found)
+                local = jnp.where(mask > 0.5, here, local)
+            head += 1
         out_ref[slot] = local
-        high, low = halves(part["grown"] + read)
+        high, low = halves(grown_ref[slot] + found)
         read_ref[slot, :, :LANES] = high
         read_ref[slot, :, LANES:] = low
-        put(1, slot, 1)
-        put(2, slot, 1)
-    for copy in pending:
-        copy.wait()
+        gate = gate_ref[group, :, lanes].astype(f32)
+        scale_ref[slot] = gain_ref[group : group + 1, lanes] * gate
+        q = q_ref[group, :, lanes].astype(f32)
+        k = k_ref[group, :, lanes].astype(f32)
+        own = head_sum(q * k * own_ref[group : group + 1, lanes], masks)
+        extra_ref[slot] = own * v.astype(f32) * gate
+        for which in range(4):
+            put(which, slot, 1)
+    finish()
 
 
 def row_kernel(got_ref, prefix_ref, total_ref):
@@ -272,10 +305,10 @@
 
 
 def mix_kernel(*refs):
-    inputs, y_ref, scratch, sems = refs[:6], refs[6], refs[7:13], refs[13]
-    out_ref, read_ref, scale_ref, extra_ref, state_ref, w_ref = scratch
+    state_ref, inputs, y_ref, scratch, sems = refs[0], refs[1:6], refs[6], refs[7:12], refs[12]
+    out_ref, read_ref, scale_ref, extra_ref, w_ref = scratch
     copies = fetch(inputs, scratch, sems)
-    for copy in copies[:5]:
+    for copy in copies[:4]:
         copy.wait()
     mixed = []
     for slot in range(4):
@@ -288,7 +321,7 @@
         normed = centered * lax.rsqrt(variance + head_epsilon) * scale_ref[slot]
         mixed.append((normed + extra_ref[slot]).astype(bf16))
     mixed = jnp.concatenate(mixed, 1)
-    copies[5].wait()
+    copies[4].wait()
     tiles, _, columns = y_ref.shape
     for k in range(tiles):
         y_ref[k] = dot_nn(mixed, w_ref[:, k * columns : (k + 1) * columns]).astype(bf16)
@@ -378,30 +411,30 @@
     for k, copy in enumerate(copies):
         copy.wait()
         lanes = slice(k * wide, (k + 1) * wide)
+        kept_ref[given_ref.shape[0] :, lanes] = jnp.zeros((given_ref.shape[0], wide), bf16)
         near = scratch[k][:, :wide]
         rest = scratch[k][:, wide:]
         blank = jnp.zeros((rest.shape[0], 2 * wide - scratch[k].shape[1]), bf16)
         far = jnp.concatenate([rest, blank], axis=1)
-        kept_ref[:, lanes] = jnp.where(first, near, far)
+        kept_ref[: near.shape[0], lanes] = jnp.where(first, near, far)
         given_ref[:, lanes] = jnp.where(first, far, near)
 
 
 def swapped(far, parts):
     rows, hidden = parts[0].shape
     wide = -(-hidden // (2 * LANES)) * LANES
-    packed = array((rows, 3 * wide), bf16)
-    kept, given = call(pack_kernel, (packed, packed), [SMEM] + [HBM] * 3, parts, 62_000_000)(
-        far, *parts
-    )
+    packed = (array((2 * rows, 3 * wide), bf16), array((rows, 3 * wide), bf16))
+    kept, given = call(pack_kernel, packed, [SMEM] + [HBM] * 3, parts, 62_000_000)(far, *parts)
     return kept, lax.ppermute(given, FAR, [(0, 1), (1, 0)])
 
 
 def gathered(kept, taken):
-    both = jnp.concatenate([kept, taken], axis=0)
+    rows, width = taken.shape
+    both = lax.dynamic_update_slice(kept, taken, (rows, 0))
     whole = lax.all_gather(both, GATHER, axis=0, tiled=True)
     planes = lax.axis_size(PLANE)
     near = lax.axis_size(NEAR) * lax.axis_size(CORE)
-    return whole.reshape(planes, near, 2, *kept.shape)
+    return whole.reshape(planes, near, 2, rows, width)
 
 
 VMEM = pl.BlockSpec(memory_space=pltpu.VMEM)
@@ -463,6 +496,8 @@
     far = lax.axis_index(FAR).astype(jnp.int32).reshape(1)
     kept, taken = swapped(far, [switching_matrix, widening_matrix, shrinking_matrix.T])
     blocks = array((4, TOK, LANES), f32)
+    pairs = array((6, TOK, TOK), bf16)
+    doubled = array((4, TOK, 2 * LANES), bf16)
     inputs = (
         acceptance_query,
         cluster_lookup_matrix,
@@ -470,24 +505,15 @@
         fading_logit,
         adaptation_speed_logit,
         additional_fading_exponent,
-        result_switch_pair,
-        attender_scaling_factor,
-        present_item_factor,
-    )
-    send, local_out, start_read, scale, extra = call(
-        local_kernel,
-        (
-            array((SHARES, LANES + HALF, LANES), bf16),
-            blocks,
-            array((4, TOK, 2 * LANES), bf16),
-            blocks,
-            blocks,
-        ),
+    )
+    send, *found = call(
+        solve_kernel,
+        (array((SHARES, LANES + HALF, LANES), bf16), pairs, pairs, doubled, blocks),
         [HBM] * len(inputs),
         inputs,
         66_400_000,
-        4,
-        [(7, 2), (2,)],
+        6,
+        [(len(inputs), 2)],
     )(*inputs)
     place = lax.axis_index(PLANE).astype(jnp.int32).reshape(1)
     first_column = (lax.axis_index(TP) * columns).astype(jnp.uint32)
@@ -502,24 +528,33 @@
         ),
         [VMEM],
     )(exchange(send, ROW))
+    total, *found = lax.optimization_barrier((total, *found))
+    reading = (
+        *found,
+        *inputs[:3],
+        result_switch_pair,
+        attender_scaling_factor,
+        present_item_factor,
+    )
+    read = call(
+        read_kernel,
+        (blocks, doubled, blocks, blocks),
+        [HBM] * len(reading),
+        reading,
+        66_400_000,
+        4,
+    )(*reading)
     states = call(state_kernel, array((SHARES, HALF, LANES), bf16), [SMEM, VMEM, VMEM])(
         place, exchange(total, PLANE), prefix
     )
-    mixing = (
-        local_out,
-        start_read,
-        scale,
-        extra,
-        exchange(states, ROW),
-        final_mapping_matrix.reshape(-1, features),
-    )
+    mixing = (*read, final_mapping_matrix.reshape(-1, features))
     terms = call(
         mix_kernel,
         array((features // columns, TOK, columns), bf16),
-        [HBM] * len(mixing),
+        [VMEM] + [HBM] * len(mixing),
         mixing,
         64_000_000,
-    )(*mixing)
+    )(exchange(states, ROW), *mixing)
     residual = lax.dynamic_slice(
         stratum_source_matrix, (jnp.uint32(0), first_column), (TOK, columns)
     )

time: 148 us -> 147 us (level)
  blocking collectives: 105 us -> 93.2 us
  starting transfers between devices: 2.21 us -> 7.07 us
  waiting for transfers between devices: 0.02 us -> 3.42 us
  Pallas kernels: 23.5 us -> 25.8 us
  other arithmetic: 3.58 us -> 1.93 us
    all_to_all x6 -> x5, blocking collectives: 105 us -> 93.2 us  [exchange(): return lax.all_to_all(value, axis, 0, 0, tiled=True)]
    all_to_all x0 -> x1, starting transfers between devices: none -> 4.86 us  [exchange(): return lax.all_to_all(value, axis, 0, 0, tiled=True)]
    all_to_all x0 -> x1, waiting for transfers between devices: none -> 3.4 us  [exchange(): return lax.all_to_all(value, axis, 0, 0, tiled=True)]
    concatenate x1 -> x0, other arithmetic: 1.66 us -> none  [gathered(): both = jnp.concatenate([kept, taken], axis=0)]
    pallas_call x3 -> x4, Pallas kernels: 13.8 us -> 15.4 us  [the longest x1 6.69 us: on_device(): call(solve_kernel, (array((SHARES, LANES + HALF, LANES), bf16), pairs, pa...]
  transfers between devices with their start and end apart: 2 -> 3, of which waited for: 0 -> 1; matrix products, arithmetic and copies ran while one was open for 1% -> 1% of each run, Pallas kernels for 10% -> 11%
where the time goes in v7:
time: 147 us; the launch traced here: 146 us
  blocking collectives  93.2 us (63%)
  Pallas kernels  25.8 us (18%)
  between operations  13.5 us (9%)
  starting transfers between devices  7.07 us (5%)
  waiting for transfers between devices  3.42 us (2%)
  other arithmetic  1.93 us (1%)
    all_to_all x5, blocking collectives, exchange(): return lax.all_to_all(value, axis, 0, 0, tiled=True)  93.2 us
    pallas_call x1, Pallas kernels, feed_forward(): pl.pallas_call(feed_kernel, out_shape=array((shares, tokens, columns), bf...  7.65 us
    pallas_call x1, Pallas kernels, on_device(): call(solve_kernel, (array((SHARES, LANES + HALF, LANES), bf16), pairs, pa...  6.69 us
    all_to_all x1, starting transfers between devices, exchange(): return lax.all_to_all(value, axis, 0, 0, tiled=True)  4.86 us
    pallas_call x1, Pallas kernels, on_device(): call(mix_kernel, array((features // columns, TOK, columns), bf16), [VMEM]...  4.18 us
    all_to_all x1, waiting for transfers between devices, exchange(): return lax.all_to_all(value, axis, 0, 0, tiled=True)  3.4 us
  transfers between devices with their start and end apart: 3, of which 1 were waited for; matrix products, arithmetic and copies ran while one was open for 1% of the time, Pallas kernels for 11%

profile of v7, /device:TPU:2, one launch (start us, length us, event | category | flops | bytes accessed | tf_op | source)
XLA Modules:
  0.0 146.3 jit_solution(17569366305997968012)
XLA Ops:
  6.5 0.0 all-gather.2.cloned.1.call-start
  6.5 1.8 %shard_map.146 = (bf16[64,2304]{1,0:T(8,128)(2,1)}, bf16[32,2304]{1,0:T(8,128)(2,1)}) custom-call(s32[1]{0:T(128)} %bitcast.far_ref, bf16[32,1408]{1,0:T(8,128)(2,1)} %refs_0_.3, bf16[32,1408]{1,0:T(8,128)(2,1)} %refs_1_.3, bf16[32,1408]{1,0:T(8,128)(2,1)} %bitcast.8), custom_call_target="tpu_custom_call" | custom-call | tf_op jit(solution)/shard_map/pallas_call | solution.py:427
  8.3 2.2 %collective-permute-start = (bf16[32,2304]{1,0:T(8,128)(2,1)}, bf16[32,2304]{1,0:T(8,128)(2,1)S(1)}, u32[]{:S(2)}, u32[]{:S(2)}) collective-permute-start(bf16[32,2304]{1,0:T(8,128)(2,1)} %get-tuple-element.28), channel_id=1, source_target_pairs={{0,16},{16,0},{1,17},{17,1},{2,18},{18,2},{3,19},{19,3},{4,20},{20... | collective-permute-start | bytes 442376 | tf_op jit(solution)/shard_map/ppermute | solution.py:428
  10.5 6.7 %shard_map.145 = (bf16[8,192,128]{2,1,0:T(8,128)(2,1)}, bf16[6,128,128]{2,1,0:T(8,128)(2,1)}, bf16[6,128,128]{2,1,0:T(8,128)(2,1)}, bf16[4,128,256]{2,1,0:T(8,128)(2,1)}, f32[4,128,128]{2,1,0:T(8,128)}) custom-call(bf16[2,128,256]{2,1,0:T(8,128)(2,1)} %refs_4_.3, bf16[2,128,256]{2,1,0:T(8,128)(2,1)} %refs_5_.3, bf16[2,128,256]{2,1,0:T(8,128)(2,1)} %refs_6_.1, ...), custom_call_target="tpu_custom_call" | custom-call | tf_op jit(solution)/shard_map/pallas_call | solution.py:509
  17.2 0.0 collective-permute-done
  17.2 0.7 constant_dynamic-update-slice_fusion
  17.9 0.0 all-gather.2.cloned.1.call-update
  17.9 12.4 %all_to_all.30.got_ref = bf16[8,192,128]{2,1,0:T(8,128)(2,1)S(1)} all-to-all(bf16[8,192,128]{2,1,0:T(8,128)(2,1)} %get-tuple-element.31), channel_id=1, replica_groups=mesh['plane'=8,'far'=2,'near'=2,'core'=2,'tp'=4] {'far','near','core'}, dimensions={0} | all-to-all | bytes 786432 | tf_op jit(solution)/shard_map/all_to_all | solution.py:469
  30.3 0.9 shard_map.147
  31.2 27.3 %all_to_all.31.every_ref = bf16[8,192,128]{2,1,0:T(8,128)(2,1)S(1)} all-to-all(bf16[8,192,128]{2,1,0:T(8,128)(2,1)S(1)} %get-tuple-element.37), channel_id=1, replica_groups=mesh['plane'=8,'far'=2,'near'=2,'core'=2,'tp'=4] {'plane'}, dimensions={0} | all-to-all | bytes 786432 | tf_op jit(solution)/shard_map/all_to_all | solution.py:469
  58.5 1.8 %shard_map.148 = bf16[8,64,128]{2,1,0:T(8,128)(2,1)} custom-call(s32[1]{0:T(128)} %bitcast.2.place_ref, bf16[8,192,128]{2,1,0:T(8,128)(2,1)S(1)} %all_to_all.31.every_ref, f32[8,192,128]{2,1,0:T(8,128)S(1)} %get-tuple-element.38.prefix_ref), custom_call_target="tpu_custom_call" | custom-call | tf_op jit(solution)/shard_map/pallas_call | solution.py:547
  60.3 4.9 %all-to-all-start.2 = ((bf16[8,64,128]{2,1,0:T(8,128)(2,1)}), bf16[8,64,128]{2,1,0:T(8,128)(2,1)S(1)}, u32[]{:S(2)}, u32[]{:S(2)}) async-start(bf16[8,64,128]{2,1,0:T(8,128)(2,1)} %shard_map.148), calls=%async_computation.2 | async-start | bytes 262144 | tf_op jit(solution)/shard_map/all_to_all | solution.py:469
  65.2 2.8 %shard_map.149 = (f32[4,128,128]{2,1,0:T(8,128)}, bf16[4,128,256]{2,1,0:T(8,128)(2,1)}, f32[4,128,128]{2,1,0:T(8,128)}, f32[4,128,128]{2,1,0:T(8,128)}) custom-call(bf16[6,128,128]{2,1,0:T(8,128)(2,1)} %get-tuple-element.39.refs_0_, bf16[6,128,128]{2,1,0:T(8,128)(2,1)} %get-tuple-element.40.refs_1_, bf16[4,128,256]{2,1,0:T(8,128)(2,1)} %get-tuple-element.41.refs_2_, ...), custom_call_target="tpu_custom_call" | custom-call | tf_op jit(solution)/shard_map/pallas_call | solution.py:539
  68.0 3.4 %all-to-all-done.2.refs_0_ = bf16[8,64,128]{2,1,0:T(8,128)(2,1)S(1)} async-done(((bf16[8,64,128]{2,1,0:T(8,128)(2,1)}), bf16[8,64,128]{2,1,0:T(8,128)(2,1)S(1)}, u32[]{:S(2)}, u32[]{:S(2)}) %all-to-all-start.2) | async-done | bytes 131104 | tf_op jit(solution)/shard_map/all_to_all | solution.py:469
  71.4 0.0 copy-start
  71.4 0.7 copy-done
  72.0 4.2 %shard_map.150 = bf16[4,128,512]{2,1,0:T(8,128)(2,1)} custom-call(bf16[8,64,128]{2,1,0:T(8,128)(2,1)} %copy-done, f32[4,128,128]{2,1,0:T(8,128)} %get-tuple-element.43.refs_1_, bf16[4,128,256]{2,1,0:T(8,128)(2,1)} %get-tuple-element.44.refs_2_, f32[4,128,128]{2,1,0:T(8,128)} %get-tuple-element.45.refs_3_, f32[4,128,128]{2,1,0:T(8,128)} %get-tuple-element.46.refs_4_, ...), custom_call_target="tpu_custom_call" | custom-call | tf_op jit(solution)/shard_map/pallas_call | solution.py:551
  76.2 13.9 %all_to_all.32 = bf16[4,128,512]{2,1,0:T(8,128)(2,1)S(1)} all-to-all(bf16[4,128,512]{2,1,0:T(8,128)(2,1)} %shard_map.150), channel_id=1, replica_groups=mesh['plane'=8,'far'=2,'near'=2,'core'=2,'tp'=4] {'tp'}, dimensions={0} | all-to-all | bytes 1048576 | tf_op jit(solution)/shard_map/all_to_all | solution.py:469
  90.1 0.1 convert_reduce_fusion.1
  90.2 1.0 add_convert_fusion.1
  91.2 0.1 broadcast_in_dim.2
  91.3 20.5 %all_to_all.33.x_ref = bf16[8,128,512]{2,1,0:T(8,128)(2,1)} all-to-all(bf16[8,128,512]{2,1,0:T(8,128)(2,1)S(1)} %broadcast_in_dim.2), channel_id=1, replica_groups=mesh['plane'=8,'far'=2,'near'=2,'core'=2,'tp'=4] {'far','tp'}, dimensions={0} | all-to-all | bytes 2097152 | tf_op jit(solution)/shard_map/all_to_all | solution.py:469
  111.8 0.0 all-gather.2.cloned.1.call-done
  111.8 7.7 %shard_map.151 = bf16[8,128,512]{2,1,0:T(8,128)(2,1)} custom-call(s32[1]{0:T(128)} %bitcast.far_ref, bf16[8,128,512]{2,1,0:T(8,128)(2,1)} %all_to_all.33.x_ref, f32[1,2048]{1,0:T(1,128)} %bitcast.9, bf16[8,4,2,32,2304]{4,3,2,1,0:T(8,128)(2,1)} %bitcast.6), custom_call_target="tpu_custom_call" | custom-call | tf_op jit(solution)/shard_map/pallas_call | solution.py:391
  119.4 19.2 %all_to_all.34 = bf16[8,128,512]{2,1,0:T(8,128)(2,1)S(1)} all-to-all(bf16[8,128,512]{2,1,0:T(8,128)(2,1)} %shard_map.151), channel_id=1, replica_groups=mesh['plane'=8,'far'=2,'near'=2,'core'=2,'tp'=4] {'far','tp'}, dimensions={0} | all-to-all | bytes 2097152 | tf_op jit(solution)/shard_map/all_to_all | solution.py:469
  138.6 0.1 convert_reduce_fusion
  138.8 0.7 add_convert_fusion
Async XLA Ops:
  6.5 105.2 %all-gather.2.cloned.1.call-start = ((), (), s32[]{:S(2)}) async-start(), calls=%async_computation.6 | async-start | bytes 9732096 | tf_op jit(solution)/shard_map/all_gather | solution.py:434
  8.3 8.9 %collective-permute-start = (bf16[32,2304]{1,0:T(8,128)(2,1)}, bf16[32,2304]{1,0:T(8,128)(2,1)S(1)}, u32[]{:S(2)}, u32[]{:S(2)}) collective-permute-start(bf16[32,2304]{1,0:T(8,128)(2,1)} %get-tuple-element.28), channel_id=1, source_target_pairs={{0,16},{16,0},{1,17},{17,1},{2,18},{18,2},{3,19},{19,3},{4,20},{20... | collective-permute-start | bytes 442376 | tf_op jit(solution)/shard_map/ppermute | solution.py:428
  60.3 11.1 %all-to-all-start.2 = ((bf16[8,64,128]{2,1,0:T(8,128)(2,1)}), bf16[8,64,128]{2,1,0:T(8,128)(2,1)S(1)}, u32[]{:S(2)}, u32[]{:S(2)}) async-start(bf16[8,64,128]{2,1,0:T(8,128)(2,1)} %shard_map.148), calls=%async_computation.2 | async-start | bytes 262144 | tf_op jit(solution)/shard_map/all_to_all | solution.py:469
  71.4 0.7 copy-start
Sparse Core Ops, SparseCore 0:
  18.0 81.8 all-gather.1

commit v8 on v7

--- a/solution.py
+++ b/solution.py
@@ -305,10 +305,18 @@
 
 
 def mix_kernel(*refs):
-    state_ref, inputs, y_ref, scratch, sems = refs[0], refs[1:6], refs[6], refs[7:12], refs[12]
-    out_ref, read_ref, scale_ref, extra_ref, w_ref = scratch
+    inputs, outputs, scratch, results, sems, out_sems = (
+        refs[:6],
+        refs[6:7],
+        refs[7:13],
+        refs[13:14],
+        refs[14],
+        refs[15],
+    )
+    state_ref, out_ref, read_ref, scale_ref, extra_ref, w_ref = scratch
     copies = fetch(inputs, scratch, sems)
-    for copy in copies[:4]:
+    put, finish = writer(results, outputs, out_sems)
+    for copy in copies[:5]:
         copy.wait()
     mixed = []
     for slot in range(4):
@@ -321,16 +329,35 @@
         normed = centered * lax.rsqrt(variance + head_epsilon) * scale_ref[slot]
         mixed.append((normed + extra_ref[slot]).astype(bf16))
     mixed = jnp.concatenate(mixed, 1)
-    copies[4].wait()
-    tiles, _, columns = y_ref.shape
+    copies[5].wait()
+    tiles, _, columns = results[0].shape
     for k in range(tiles):
-        y_ref[k] = dot_nn(mixed, w_ref[:, k * columns : (k + 1) * columns]).astype(bf16)
+        results[0][k] = dot_nn(mixed, w_ref[:, k * columns : (k + 1) * columns]).astype(bf16)
+        put(0, k, 1)
+    finish()
 
 
 AHEAD = 4
 
 
-def feed_kernel(far_ref, x_ref, gain_ref, whole_ref, y_ref, w_ref, n_ref, acc_ref, sems):
+def feed_kernel(
+    far_ref,
+    state_ref,
+    gain_in_ref,
+    whole_ref,
+    sent_ref,
+    w_ref,
+    n_ref,
+    acc_ref,
+    x_ref,
+    gain_ref,
+    y_ref,
+    sems,
+    in_sems,
+    out_sems,
+):
+    tokens_here = fetch([state_ref, gain_in_ref], [x_ref, gain_ref], in_sems)
+    put, finish = writer([y_ref], [sent_ref], out_sems)
     planes, sides, near, rows, width = w_ref.shape
     third = width // 3
     far = far_ref[0]
@@ -350,6 +377,8 @@
             copy.start()
     shares, tokens, columns = x_ref.shape
     tiles = shares // sides
+    for copy in tokens_here:
+        copy.wait()
     for side in range(sides):
         parts = [x_ref[side * tiles + k].astype(f32) for k in range(tiles)]
         total = sum(jnp.sum(a * a, axis=1, keepdims=True) for a in parts)
@@ -383,6 +412,8 @@
         out = dot_nt(active, down).astype(bf16)
         for side in range(sides):
             y_ref[side * tiles + k] = out[side * tokens : (side + 1) * tokens]
+            put(0, side * tiles + k, 1)
+    finish()
 
 
 def feed_forward(far, state, gain, whole):
@@ -391,13 +422,18 @@
     return pl.pallas_call(
         feed_kernel,
         out_shape=array((shares, tokens, columns), bf16),
-        in_specs=[SMEM, VMEM, VMEM, HBM],
-        out_specs=VMEM,
+        in_specs=[SMEM, HBM, HBM, HBM],
+        out_specs=HBM,
         scratch_shapes=[
             pltpu.VMEM((planes, sides, near, rows, width), bf16),
             pltpu.VMEM((sides * tokens, gain.shape[1]), bf16),
             pltpu.VMEM((sides * tokens, 2 * width // 3), f32),
+            pltpu.VMEM(state.shape, bf16),
+            pltpu.VMEM(gain.shape, f32),
+            pltpu.VMEM(state.shape, bf16),
             pltpu.SemaphoreType.DMA((planes, sides)),
+            pltpu.SemaphoreType.DMA((2,)),
+            pltpu.SemaphoreType.DMA((1, shares)),
         ],
         compiler_params=pltpu.CompilerParams(vmem_limit_bytes=60_000_000),
     )(far, state, gain, whole)
@@ -541,20 +577,22 @@
         (blocks, doubled, blocks, blocks),
         [HBM] * len(reading),
         reading,
-        66_400_000,
+        65300000,
         4,
     )(*reading)
+    every, *read = lax.optimization_barrier((exchange(total, PLANE), *read))
     states = call(state_kernel, array((SHARES, HALF, LANES), bf16), [SMEM, VMEM, VMEM])(
-        place, exchange(total, PLANE), prefix
-    )
-    mixing = (*read, final_mapping_matrix.reshape(-1, features))
-    terms = call(
+        place, every, prefix
+    )
+    mixing = (exchange(states, ROW), *read, final_mapping_matrix.reshape(-1, features))
+    (terms,) = call(
         mix_kernel,
-        array((features // columns, TOK, columns), bf16),
-        [VMEM] + [HBM] * len(mixing),
+        (array((features // columns, TOK, columns), bf16),),
+        [HBM] * len(mixing),
         mixing,
         64_000_000,
-    )(exchange(states, ROW), *mixing)
+        features // columns,
+    )(*mixing)
     residual = lax.dynamic_slice(
         stratum_source_matrix, (jnp.uint32(0), first_column), (TOK, columns)
     )

time: 147 us -> 145 us (0.986)
  blocking collectives: 93.2 us -> 76.6 us
  waiting for transfers between devices: 3.42 us -> 16.5 us
  starting transfers between devices: 7.07 us -> 10.6 us
    all_to_all x5, blocking collectives: 93.2 us -> 76.6 us  [exchange(): return lax.all_to_all(value, axis, 0, 0, tiled=True)]
    all_to_all x1, waiting for transfers between devices: 3.4 us -> 16.5 us  [exchange(): return lax.all_to_all(value, axis, 0, 0, tiled=True)]
    all_to_all x1, starting transfers between devices: 4.86 us -> 8.34 us  [exchange(): return lax.all_to_all(value, axis, 0, 0, tiled=True)]
where the time goes in v8:
time: 145 us; the launch traced here: 144 us
  blocking collectives  76.6 us (53%)
  Pallas kernels  24.7 us (17%)
  waiting for transfers between devices  16.5 us (11%)
  between operations  13.5 us (9%)
  starting transfers between devices  10.6 us (7%)
  other arithmetic  1.92 us (1%)
    all_to_all x5, blocking collectives, exchange(): return lax.all_to_all(value, axis, 0, 0, tiled=True)  76.6 us
    all_to_all x1, waiting for transfers between devices, exchange(): return lax.all_to_all(value, axis, 0, 0, tiled=True)  16.5 us
    all_to_all x1, starting transfers between devices, exchange(): return lax.all_to_all(value, axis, 0, 0, tiled=True)  8.34 us
    pallas_call x1, Pallas kernels, feed_forward(): pl.pallas_call(feed_kernel, out_shape=array((shares, tokens, columns), bf...  7.44 us
    pallas_call x1, Pallas kernels, on_device(): call(solve_kernel, (array((SHARES, LANES + HALF, LANES), bf16), pairs, pa...  6.7 us
    pallas_call x1, Pallas kernels, on_device(): call(mix_kernel, (array((features // columns, TOK, columns), bf16),), [HB...  3.23 us
  transfers between devices with their start and end apart: 3, of which 1 were waited for; matrix products, arithmetic and copies ran while one was open for 1% of the time, Pallas kernels for 11%

profile of v8, /device:TPU:2, one launch (start us, length us, event | category | flops | bytes accessed | tf_op | source)
XLA Modules:
  0.0 144.5 jit_solution(10117304564744316789)
XLA Ops:
  6.5 0.0 all-gather.2.cloned.1.call-start
  6.5 1.8 %shard_map.146 = (bf16[64,2304]{1,0:T(8,128)(2,1)}, bf16[32,2304]{1,0:T(8,128)(2,1)}) custom-call(s32[1]{0:T(128)} %bitcast.far_ref, bf16[32,1408]{1,0:T(8,128)(2,1)} %refs_0_.3, bf16[32,1408]{1,0:T(8,128)(2,1)} %refs_1_.3, bf16[32,1408]{1,0:T(8,128)(2,1)} %bitcast.8), custom_call_target="tpu_custom_call" | custom-call | tf_op jit(solution)/shard_map/pallas_call | solution.py:463
  8.3 2.2 %collective-permute-start = (bf16[32,2304]{1,0:T(8,128)(2,1)}, bf16[32,2304]{1,0:T(8,128)(2,1)S(1)}, u32[]{:S(2)}, u32[]{:S(2)}) collective-permute-start(bf16[32,2304]{1,0:T(8,128)(2,1)} %get-tuple-element.33), channel_id=1, source_target_pairs={{0,16},{16,0},{1,17},{17,1},{2,18},{18,2},{3,19},{19,3},{4,20},{20... | collective-permute-start | bytes 442376 | tf_op jit(solution)/shard_map/ppermute | solution.py:464
  10.5 6.7 %shard_map.145 = (bf16[8,192,128]{2,1,0:T(8,128)(2,1)}, bf16[6,128,128]{2,1,0:T(8,128)(2,1)}, bf16[6,128,128]{2,1,0:T(8,128)(2,1)}, bf16[4,128,256]{2,1,0:T(8,128)(2,1)}, f32[4,128,128]{2,1,0:T(8,128)}) custom-call(bf16[2,128,256]{2,1,0:T(8,128)(2,1)} %refs_4_.3, bf16[2,128,256]{2,1,0:T(8,128)(2,1)} %refs_5_.3, bf16[2,128,256]{2,1,0:T(8,128)(2,1)} %refs_6_.1, ...), custom_call_target="tpu_custom_call" | custom-call | tf_op jit(solution)/shard_map/pallas_call | solution.py:545
  17.2 0.0 collective-permute-done
  17.2 0.7 constant_dynamic-update-slice_fusion
  17.9 0.0 all-gather.2.cloned.1.call-update
  17.9 12.4 %all_to_all.30.got_ref = bf16[8,192,128]{2,1,0:T(8,128)(2,1)S(1)} all-to-all(bf16[8,192,128]{2,1,0:T(8,128)(2,1)} %get-tuple-element.36), channel_id=1, replica_groups=mesh['plane'=8,'far'=2,'near'=2,'core'=2,'tp'=4] {'far','near','core'}, dimensions={0} | all-to-all | bytes 786432 | tf_op jit(solution)/shard_map/all_to_all | solution.py:505
  30.3 1.7 %shard_map.147 = (f32[8,192,128]{2,1,0:T(8,128)S(1)}, bf16[8,192,128]{2,1,0:T(8,128)(2,1)}) custom-call(bf16[8,192,128]{2,1,0:T(8,128)(2,1)S(1)} %all_to_all.30.got_ref), custom_call_target="tpu_custom_call" | custom-call | tf_op jit(solution)/shard_map/pallas_call | solution.py:559
  32.0 8.3 %all-to-all-start.1 = ((bf16[8,192,128]{2,1,0:T(8,128)(2,1)}), bf16[8,192,128]{2,1,0:T(8,128)(2,1)S(1)}, u32[]{:S(2)}, u32[]{:S(2)}) async-start(bf16[8,192,128]{2,1,0:T(8,128)(2,1)} %get-tuple-element.42), calls=%async_computation.1 | async-start | bytes 786432 | tf_op jit(solution)/shard_map/all_to_all | solution.py:505
  40.3 2.8 %shard_map.148 = (f32[4,128,128]{2,1,0:T(8,128)}, bf16[4,128,256]{2,1,0:T(8,128)(2,1)}, f32[4,128,128]{2,1,0:T(8,128)}, f32[4,128,128]{2,1,0:T(8,128)}) custom-call(bf16[6,128,128]{2,1,0:T(8,128)(2,1)} %get-tuple-element.43.refs_0_, bf16[6,128,128]{2,1,0:T(8,128)(2,1)} %get-tuple-element.44.refs_1_, bf16[4,128,256]{2,1,0:T(8,128)(2,1)} %get-tuple-element.45.refs_2_, ...), custom_call_target="tpu_custom_call" | custom-call | tf_op jit(solution)/shard_map/pallas_call | solution.py:575
  43.1 16.5 %all-to-all-done.1.every_ref = bf16[8,192,128]{2,1,0:T(8,128)(2,1)S(1)} async-done(((bf16[8,192,128]{2,1,0:T(8,128)(2,1)}), bf16[8,192,128]{2,1,0:T(8,128)(2,1)S(1)}, u32[]{:S(2)}, u32[]{:S(2)}) %all-to-all-start.1) | async-done | bytes 393248 | tf_op jit(solution)/shard_map/all_to_all | solution.py:505
  59.6 1.1 shard_map.149
  60.8 10.6 %all_to_all.31.refs_0_ = bf16[8,64,128]{2,1,0:T(8,128)(2,1)} all-to-all(bf16[8,64,128]{2,1,0:T(8,128)(2,1)S(1)} %shard_map.149), channel_id=1, replica_groups=mesh['plane'=8,'far'=2,'near'=2,'core'=2,'tp'=4] {'far','near','core'}, dimensions={0} | all-to-all | bytes 262144 | tf_op jit(solution)/shard_map/all_to_all | solution.py:505
  71.4 3.2 %shard_map.150 = bf16[4,128,512]{2,1,0:T(8,128)(2,1)} custom-call(bf16[8,64,128]{2,1,0:T(8,128)(2,1)} %all_to_all.31.refs_0_, f32[4,128,128]{2,1,0:T(8,128)} %get-tuple-element.53.refs_1_, bf16[4,128,256]{2,1,0:T(8,128)(2,1)} %get-tuple-element.54.refs_2_, f32[4,128,128]{2,1,0:T(8,128)} %get-tuple-element.55.refs_3_, ...), custom_call_target="tpu_custom_call" | custom-call | tf_op jit(solution)/shard_map/pallas_call | solution.py:588
  74.6 13.5 %all_to_all.32 = bf16[4,128,512]{2,1,0:T(8,128)(2,1)S(1)} all-to-all(bf16[4,128,512]{2,1,0:T(8,128)(2,1)} %shard_map.150), channel_id=1, replica_groups=mesh['plane'=8,'far'=2,'near'=2,'core'=2,'tp'=4] {'tp'}, dimensions={0} | all-to-all | bytes 1048576 | tf_op jit(solution)/shard_map/all_to_all | solution.py:505
  88.1 0.1 convert_reduce_fusion.1
  88.2 1.0 add_convert_fusion.1
  89.2 0.1 broadcast_in_dim.2
  89.3 21.2 %all_to_all.33.state_ref = bf16[8,128,512]{2,1,0:T(8,128)(2,1)} all-to-all(bf16[8,128,512]{2,1,0:T(8,128)(2,1)S(1)} %broadcast_in_dim.2), channel_id=1, replica_groups=mesh['plane'=8,'far'=2,'near'=2,'core'=2,'tp'=4] {'far','tp'}, dimensions={0} | all-to-all | bytes 2097152 | tf_op jit(solution)/shard_map/all_to_all | solution.py:505
  110.6 0.0 all-gather.2.cloned.1.call-done
  110.6 7.4 %shard_map.151 = bf16[8,128,512]{2,1,0:T(8,128)(2,1)} custom-call(s32[1]{0:T(128)} %bitcast.far_ref, bf16[8,128,512]{2,1,0:T(8,128)(2,1)} %all_to_all.33.state_ref, f32[1,2048]{1,0:T(1,128)} %bitcast.9, bf16[8,4,2,32,2304]{4,3,2,1,0:T(8,128)(2,1)} %bitcast.6), custom_call_target="tpu_custom_call" | custom-call | tf_op jit(solution)/shard_map/pallas_call | solution.py:422
  118.0 18.8 %all_to_all.34 = bf16[8,128,512]{2,1,0:T(8,128)(2,1)S(1)} all-to-all(bf16[8,128,512]{2,1,0:T(8,128)(2,1)} %shard_map.151), channel_id=1, replica_groups=mesh['plane'=8,'far'=2,'near'=2,'core'=2,'tp'=4] {'far','tp'}, dimensions={0} | all-to-all | bytes 2097152 | tf_op jit(solution)/shard_map/all_to_all | solution.py:505
  136.8 0.1 convert_reduce_fusion
  137.0 0.7 add_convert_fusion
Async XLA Ops:
  6.5 104.0 %all-gather.2.cloned.1.call-start = ((), (), s32[]{:S(2)}) async-start(), calls=%async_computation.6 | async-start | bytes 9732096 | tf_op jit(solution)/shard_map/all_gather | solution.py:470
  8.3 8.9 %collective-permute-start = (bf16[32,2304]{1,0:T(8,128)(2,1)}, bf16[32,2304]{1,0:T(8,128)(2,1)S(1)}, u32[]{:S(2)}, u32[]{:S(2)}) collective-permute-start(bf16[32,2304]{1,0:T(8,128)(2,1)} %get-tuple-element.33), channel_id=1, source_target_pairs={{0,16},{16,0},{1,17},{17,1},{2,18},{18,2},{3,19},{19,3},{4,20},{20... | collective-permute-start | bytes 442376 | tf_op jit(solution)/shard_map/ppermute | solution.py:464
  32.0 27.6 %all-to-all-start.1 = ((bf16[8,192,128]{2,1,0:T(8,128)(2,1)}), bf16[8,192,128]{2,1,0:T(8,128)(2,1)S(1)}, u32[]{:S(2)}, u32[]{:S(2)}) async-start(bf16[8,192,128]{2,1,0:T(8,128)(2,1)} %get-tuple-element.42), calls=%async_computation.1 | async-start | bytes 786432 | tf_op jit(solution)/shard_map/all_to_all | solution.py:505
Sparse Core Ops, SparseCore 0:
  18.1 82.8 all-gather.1

commit v9 on v8

--- a/solution.py
+++ b/solution.py
@@ -151,7 +151,8 @@
         backward = jnp.exp(middle - cum)
         undo = jnp.exp(-log_decay)
         right = learn * removal
-        queries = jnp.concatenate([-removal * undo * forward, q * forward], 0)
+        removers = -removal * undo * forward
+        queries = q * forward
         sources = halves(jnp.concatenate([right * backward, k * backward], 0))
         final = cum[TOK - 1 : TOK, :]
         tail = jnp.exp(final - cum)
@@ -167,18 +168,19 @@
             )
         )
         for mask in masks:
-            pairs = mm_nt(halves(masked(queries, mask)), sources)
+            pairs = mm_nt(halves(masked(removers, mask)), sources)
+            reads = dot_nt(masked(queries, mask).astype(bf16), sources[0])
             head = len(heads)
-            qr_ref[head] = jnp.where(inclusive, pairs[TOK:, :TOK], 0.0).astype(bf16)
-            qk_ref[head] = jnp.where(inclusive, pairs[TOK:, TOK:], 0.0).astype(bf16)
+            qr_ref[head] = jnp.where(inclusive, reads[:, :TOK], 0.0).astype(bf16)
+            qk_ref[head] = jnp.where(inclusive, reads[:, TOK:], 0.0).astype(bf16)
             put(1, head, 1)
             put(2, head, 1)
             heads.append(
                 dict(
                     slot=slot,
                     mask=mask,
-                    n=jnp.where(strict, pairs[:TOK, :TOK], 0.0),
-                    rk=jnp.where(strict, pairs[:TOK, TOK:], 0.0),
+                    n=jnp.where(strict, pairs[:, :TOK], 0.0),
+                    rk=jnp.where(strict, pairs[:, TOK:], 0.0),
                 )
             )
     same = (row // 8) == (col // 8)
@@ -205,8 +207,9 @@
         high, low = halves(head["rk"])
         v = part["v"]
         pulled = dot_nn(jnp.concatenate([high, low], 1), jnp.concatenate([v, v], 0))
-        head["solved"] = mm(
-            halves(head["x"]), halves(jnp.concatenate([pulled, part["start"]], 1))
+        target = jnp.concatenate([pulled, part["start"]], 1).astype(bf16)
+        head["solved"] = dot_nn(
+            jnp.concatenate(halves(head["x"]), 1), jnp.concatenate([target, target], 0)
         )
     for slot, part in enumerate(slots):
         mine = [head for head in heads if head["slot"] == slot]
@@ -435,7 +438,7 @@
             pltpu.SemaphoreType.DMA((2,)),
             pltpu.SemaphoreType.DMA((1, shares)),
         ],
-        compiler_params=pltpu.CompilerParams(vmem_limit_bytes=60_000_000),
+        compiler_params=pltpu.CompilerParams(vmem_limit_bytes=55_000_000),
     )(far, state, gain, whole)
 
 

time: 145 us -> 145 us (level)
  no operation moved by 1% of the time
where the time goes in v9:
time: 145 us; the launch traced here: 144 us
  blocking collectives  76.2 us (53%)
  Pallas kernels  24.8 us (17%)
  waiting for transfers between devices  16.5 us (11%)
  between operations  13.5 us (9%)
  starting transfers between devices  10.6 us (7%)
  other arithmetic  1.93 us (1%)
    all_to_all x5, blocking collectives, exchange(): return lax.all_to_all(value, axis, 0, 0, tiled=True)  76.2 us
    all_to_all x1, waiting for transfers between devices, exchange(): return lax.all_to_all(value, axis, 0, 0, tiled=True)  16.5 us
    all_to_all x1, starting transfers between devices, exchange(): return lax.all_to_all(value, axis, 0, 0, tiled=True)  8.34 us
    pallas_call x1, Pallas kernels, feed_forward(): pl.pallas_call(feed_kernel, out_shape=array((shares, tokens, columns), bf...  7.78 us
    pallas_call x1, Pallas kernels, on_device(): call(solve_kernel, (array((SHARES, LANES + HALF, LANES), bf16), pairs, pa...  6.46 us
    pallas_call x1, Pallas kernels, on_device(): call(mix_kernel, (array((features // columns, TOK, columns), bf16),), [HB...  3.23 us
  transfers between devices with their start and end apart: 3, of which 1 were waited for; matrix products, arithmetic and copies ran while one was open for 1% of the time, Pallas kernels for 11%

profile of v9, /device:TPU:2, one launch (start us, length us, event | category | flops | bytes accessed | tf_op | source)
XLA Modules:
  0.0 144.3 jit_solution(10192182551636846908)
XLA Ops:
  6.5 0.0 all-gather.2.cloned.1.call-start
  6.5 1.8 %shard_map.146 = (bf16[64,2304]{1,0:T(8,128)(2,1)}, bf16[32,2304]{1,0:T(8,128)(2,1)}) custom-call(s32[1]{0:T(128)} %bitcast.far_ref, bf16[32,1408]{1,0:T(8,128)(2,1)} %refs_0_.3, bf16[32,1408]{1,0:T(8,128)(2,1)} %refs_1_.3, bf16[32,1408]{1,0:T(8,128)(2,1)} %bitcast.9), custom_call_target="tpu_custom_call" | custom-call | tf_op jit(solution)/shard_map/pallas_call | solution.py:466
  8.3 2.2 %collective-permute-start = (bf16[32,2304]{1,0:T(8,128)(2,1)}, bf16[32,2304]{1,0:T(8,128)(2,1)S(1)}, u32[]{:S(2)}, u32[]{:S(2)}) collective-permute-start(bf16[32,2304]{1,0:T(8,128)(2,1)} %get-tuple-element.33), channel_id=1, source_target_pairs={{0,16},{16,0},{1,17},{17,1},{2,18},{18,2},{3,19},{19,3},{4,20},{20... | collective-permute-start | bytes 442376 | tf_op jit(solution)/shard_map/ppermute | solution.py:467
  10.5 6.5 %shard_map.145 = (bf16[8,192,128]{2,1,0:T(8,128)(2,1)}, bf16[6,128,128]{2,1,0:T(8,128)(2,1)}, bf16[6,128,128]{2,1,0:T(8,128)(2,1)}, bf16[4,128,256]{2,1,0:T(8,128)(2,1)}, f32[4,128,128]{2,1,0:T(8,128)}) custom-call(bf16[2,128,256]{2,1,0:T(8,128)(2,1)} %refs_4_.3, bf16[2,128,256]{2,1,0:T(8,128)(2,1)} %refs_5_.3, bf16[2,128,256]{2,1,0:T(8,128)(2,1)} %refs_6_.1, ...), custom_call_target="tpu_custom_call" | custom-call | tf_op jit(solution)/shard_map/pallas_call | solution.py:548
  17.0 0.0 collective-permute-done
  17.0 0.7 constant_dynamic-update-slice_fusion
  17.7 0.0 all-gather.2.cloned.1.call-update
  17.7 12.4 %all_to_all.30.got_ref = bf16[8,192,128]{2,1,0:T(8,128)(2,1)S(1)} all-to-all(bf16[8,192,128]{2,1,0:T(8,128)(2,1)} %get-tuple-element.36), channel_id=1, replica_groups=mesh['plane'=8,'far'=2,'near'=2,'core'=2,'tp'=4] {'far','near','core'}, dimensions={0} | all-to-all | bytes 786432 | tf_op jit(solution)/shard_map/all_to_all | solution.py:508
  30.1 1.7 %shard_map.147 = (f32[8,192,128]{2,1,0:T(8,128)S(1)}, bf16[8,192,128]{2,1,0:T(8,128)(2,1)}) custom-call(bf16[8,192,128]{2,1,0:T(8,128)(2,1)S(1)} %all_to_all.30.got_ref), custom_call_target="tpu_custom_call" | custom-call | tf_op jit(solution)/shard_map/pallas_call | solution.py:562
  31.8 8.3 %all-to-all-start.1 = ((bf16[8,192,128]{2,1,0:T(8,128)(2,1)}), bf16[8,192,128]{2,1,0:T(8,128)(2,1)S(1)}, u32[]{:S(2)}, u32[]{:S(2)}) async-start(bf16[8,192,128]{2,1,0:T(8,128)(2,1)} %get-tuple-element.42), calls=%async_computation.1 | async-start | bytes 786432 | tf_op jit(solution)/shard_map/all_to_all | solution.py:508
  40.1 2.8 %shard_map.148 = (f32[4,128,128]{2,1,0:T(8,128)}, bf16[4,128,256]{2,1,0:T(8,128)(2,1)}, f32[4,128,128]{2,1,0:T(8,128)}, f32[4,128,128]{2,1,0:T(8,128)}) custom-call(bf16[6,128,128]{2,1,0:T(8,128)(2,1)} %get-tuple-element.43.refs_0_, bf16[6,128,128]{2,1,0:T(8,128)(2,1)} %get-tuple-element.44.refs_1_, bf16[4,128,256]{2,1,0:T(8,128)(2,1)} %get-tuple-element.45.refs_2_, ...), custom_call_target="tpu_custom_call" | custom-call | tf_op jit(solution)/shard_map/pallas_call | solution.py:578
  42.9 16.5 %all-to-all-done.1.every_ref = bf16[8,192,128]{2,1,0:T(8,128)(2,1)S(1)} async-done(((bf16[8,192,128]{2,1,0:T(8,128)(2,1)}), bf16[8,192,128]{2,1,0:T(8,128)(2,1)S(1)}, u32[]{:S(2)}, u32[]{:S(2)}) %all-to-all-start.1) | async-done | bytes 393248 | tf_op jit(solution)/shard_map/all_to_all | solution.py:508
  59.4 1.1 shard_map.149
  60.5 10.6 %all_to_all.31.refs_0_ = bf16[8,64,128]{2,1,0:T(8,128)(2,1)} all-to-all(bf16[8,64,128]{2,1,0:T(8,128)(2,1)S(1)} %shard_map.149), channel_id=1, replica_groups=mesh['plane'=8,'far'=2,'near'=2,'core'=2,'tp'=4] {'far','near','core'}, dimensions={0} | all-to-all | bytes 262144 | tf_op jit(solution)/shard_map/all_to_all | solution.py:508
  71.2 3.2 %shard_map.150 = bf16[4,128,512]{2,1,0:T(8,128)(2,1)} custom-call(bf16[8,64,128]{2,1,0:T(8,128)(2,1)} %all_to_all.31.refs_0_, f32[4,128,128]{2,1,0:T(8,128)} %get-tuple-element.53.refs_1_, bf16[4,128,256]{2,1,0:T(8,128)(2,1)} %get-tuple-element.54.refs_2_, f32[4,128,128]{2,1,0:T(8,128)} %get-tuple-element.55.refs_3_, ...), custom_call_target="tpu_custom_call" | custom-call | tf_op jit(solution)/shard_map/pallas_call | solution.py:591
  74.4 13.5 %all_to_all.32 = bf16[4,128,512]{2,1,0:T(8,128)(2,1)S(1)} all-to-all(bf16[4,128,512]{2,1,0:T(8,128)(2,1)} %shard_map.150), channel_id=1, replica_groups=mesh['plane'=8,'far'=2,'near'=2,'core'=2,'tp'=4] {'tp'}, dimensions={0} | all-to-all | bytes 1048576 | tf_op jit(solution)/shard_map/all_to_all | solution.py:508
  87.9 0.1 convert_reduce_fusion.1
  88.0 0.0 copy-start
  88.0 1.0 add_convert_fusion.1
  89.0 0.1 broadcast_in_dim.2
  89.1 21.2 %all_to_all.33.state_ref = bf16[8,128,512]{2,1,0:T(8,128)(2,1)} all-to-all(bf16[8,128,512]{2,1,0:T(8,128)(2,1)S(1)} %broadcast_in_dim.2), channel_id=1, replica_groups=mesh['plane'=8,'far'=2,'near'=2,'core'=2,'tp'=4] {'far','tp'}, dimensions={0} | all-to-all | bytes 2097152 | tf_op jit(solution)/shard_map/all_to_all | solution.py:508
  110.3 0.0 all-gather.2.cloned.1.call-done
  110.3 0.0 copy-done
  110.3 7.8 %shard_map.151 = bf16[8,128,512]{2,1,0:T(8,128)(2,1)S(1)} custom-call(s32[1]{0:T(128)} %bitcast.far_ref, bf16[8,128,512]{2,1,0:T(8,128)(2,1)} %all_to_all.33.state_ref, f32[1,2048]{1,0:T(1,128)S(1)} %bitcast.6, bf16[8,4,2,32,2304]{4,3,2,1,0:T(8,128)(2,1)} %bitcast.7), custom_call_target="tpu_custom_call" | custom-call | tf_op jit(solution)/shard_map/pallas_call | solution.py:425
  118.1 18.5 %all_to_all.34 = bf16[8,128,512]{2,1,0:T(8,128)(2,1)S(1)} all-to-all(bf16[8,128,512]{2,1,0:T(8,128)(2,1)S(1)} %shard_map.151), channel_id=1, replica_groups=mesh['plane'=8,'far'=2,'near'=2,'core'=2,'tp'=4] {'far','tp'}, dimensions={0} | all-to-all | bytes 2097152 | tf_op jit(solution)/shard_map/all_to_all | solution.py:508
  136.6 0.1 convert_reduce_fusion
  136.8 0.7 add_convert_fusion
Async XLA Ops:
  6.5 103.8 %all-gather.2.cloned.1.call-start = ((), (), s32[]{:S(2)}) async-start(), calls=%async_computation.6 | async-start | bytes 9732096 | tf_op jit(solution)/shard_map/all_gather | solution.py:473
  8.3 8.7 %collective-permute-start = (bf16[32,2304]{1,0:T(8,128)(2,1)}, bf16[32,2304]{1,0:T(8,128)(2,1)S(1)}, u32[]{:S(2)}, u32[]{:S(2)}) collective-permute-start(bf16[32,2304]{1,0:T(8,128)(2,1)} %get-tuple-element.33), channel_id=1, source_target_pairs={{0,16},{16,0},{1,17},{17,1},{2,18},{18,2},{3,19},{19,3},{4,20},{20... | collective-permute-start | bytes 442376 | tf_op jit(solution)/shard_map/ppermute | solution.py:467
  31.8 27.6 %all-to-all-start.1 = ((bf16[8,192,128]{2,1,0:T(8,128)(2,1)}), bf16[8,192,128]{2,1,0:T(8,128)(2,1)S(1)}, u32[]{:S(2)}, u32[]{:S(2)}) async-start(bf16[8,192,128]{2,1,0:T(8,128)(2,1)} %get-tuple-element.42), calls=%async_computation.1 | async-start | bytes 786432 | tf_op jit(solution)/shard_map/all_to_all | solution.py:508
  88.0 22.3 %copy-start = (f32[2048]{0:T(1024)S(1)}, f32[2048]{0:T(1024)}, u32[]{:S(2)}) copy-start(f32[2048]{0:T(1024)} %param.26) | copy-start | bytes 24580
Sparse Core Ops, SparseCore 0:
  17.8 82.9 all-gather.1

commit v10 on v9

--- a/solution.py
+++ b/solution.py
@@ -382,15 +382,18 @@
     tiles = shares // sides
     for copy in tokens_here:
         copy.wait()
+    scales = []
     for side in range(sides):
-        parts = [x_ref[side * tiles + k].astype(f32) for k in range(tiles)]
-        total = sum(jnp.sum(a * a, axis=1, keepdims=True) for a in parts)
-        scale = lax.rsqrt(total * (1.0 / (tiles * columns)) + norm_epsilon)
-        for k, a in enumerate(parts):
+        total = 0.0
+        for k in range(tiles):
             lanes = slice(k * columns, (k + 1) * columns)
-            n_ref[side * tokens : (side + 1) * tokens, lanes] = (
-                a * scale * gain_ref[:, lanes]
-            ).astype(bf16)
+            a = x_ref[side * tiles + k].astype(f32)
+            n_ref[side * tokens : (side + 1) * tokens, lanes] = (a * gain_ref[:, lanes]).astype(
+                bf16
+            )
+            total = total + jnp.sum(a * a, axis=1, keepdims=True)
+        scales.append(lax.rsqrt(total * (1.0 / (tiles * columns)) + norm_epsilon))
+    scale = jnp.concatenate(scales, 0)
     block = sides * near * rows
     for k in range(0, planes, 2):
         for step in (k, k + 1):
@@ -407,8 +410,9 @@
             acc_ref[...] = part
         else:
             acc_ref[...] += part
-    gate = acc_ref[:, :third]
-    active = (gate / (1.0 + jnp.exp(-gate)) * acc_ref[:, third:]).astype(bf16)
+    gate = acc_ref[:, :third] * scale
+    up = acc_ref[:, third:] * scale
+    active = (gate / (1.0 + jnp.exp(-gate)) * up).astype(bf16)
     per = planes // tiles
     for k in range(tiles):
         down = w_ref[k * per : (k + 1) * per, :, :, :, 2 * third :].reshape(per * block, third)
@@ -567,7 +571,7 @@
         ),
         [VMEM],
     )(exchange(send, ROW))
-    total, *found = lax.optimization_barrier((total, *found))
+    total, first_column, *found = lax.optimization_barrier((total, first_column, *found))
     reading = (
         *found,
         *inputs[:3],
@@ -580,10 +584,13 @@
         (blocks, doubled, blocks, blocks),
         [HBM] * len(reading),
         reading,
-        65300000,
+        64_500_000,
         4,
     )(*reading)
-    every, *read = lax.optimization_barrier((exchange(total, PLANE), *read))
+    residual = lax.dynamic_slice(
+        stratum_source_matrix, (jnp.uint32(0), first_column), (TOK, columns)
+    )
+    every, residual, *read = lax.optimization_barrier((exchange(total, PLANE), residual, *read))
     states = call(state_kernel, array((SHARES, HALF, LANES), bf16), [SMEM, VMEM, VMEM])(
         place, every, prefix
     )
@@ -596,9 +603,6 @@
         64_000_000,
         features // columns,
     )(*mixing)
-    residual = lax.dynamic_slice(
-        stratum_source_matrix, (jnp.uint32(0), first_column), (TOK, columns)
-    )
     attention = jnp.sum(exchange(terms, TP).astype(f32), axis=0)
     own_state = (residual.astype(f32) + attention).astype(bf16)
     tiles = feed_forward(

time: 145 us -> 145 us (level)
  transfers between devices with their start and end apart: 3 -> 3, of which waited for: 1 -> 1; matrix products, arithmetic and copies ran while one was open for 1% -> 0% of each run, Pallas kernels for 11% -> 11%
where the time goes in v10:
time: 145 us; the launch traced here: 144 us
  blocking collectives  76.2 us (53%)
  Pallas kernels  24.9 us (17%)
  waiting for transfers between devices  16.4 us (11%)
  between operations  13.5 us (9%)
  starting transfers between devices  10.6 us (7%)
  local copies, waits for them, and re-layouts  1.78 us (1%)
    all_to_all x5, blocking collectives, exchange(): return lax.all_to_all(value, axis, 0, 0, tiled=True)  76.2 us
    all_to_all x1, waiting for transfers between devices, exchange(): return lax.all_to_all(value, axis, 0, 0, tiled=True)  16.4 us
    all_to_all x1, starting transfers between devices, exchange(): return lax.all_to_all(value, axis, 0, 0, tiled=True)  8.34 us
    pallas_call x1, Pallas kernels, feed_forward(): pl.pallas_call(feed_kernel, out_shape=array((shares, tokens, columns), bf...  7.81 us
    pallas_call x1, Pallas kernels, on_device(): call(solve_kernel, (array((SHARES, LANES + HALF, LANES), bf16), pairs, pa...  6.46 us
    pallas_call x1, Pallas kernels, on_device(): call(mix_kernel, (array((features // columns, TOK, columns), bf16),), [HB...  3.23 us
  transfers between devices with their start and end apart: 3, of which 1 were waited for; matrix products, arithmetic and copies ran while one was open for 0% of the time, Pallas kernels for 11%

profile of v10, /device:TPU:2, one launch (start us, length us, event | category | flops | bytes accessed | tf_op | source)
XLA Modules:
  0.0 144.3 jit_solution(12670525589715818273)
XLA Ops:
  6.5 0.0 copy-start
  6.5 0.0 all-gather.2.cloned.1.call-start
  6.5 1.8 %shard_map.146 = (bf16[64,2304]{1,0:T(8,128)(2,1)}, bf16[32,2304]{1,0:T(8,128)(2,1)}) custom-call(s32[1]{0:T(128)} %bitcast.far_ref, bf16[32,1408]{1,0:T(8,128)(2,1)} %refs_0_.3, bf16[32,1408]{1,0:T(8,128)(2,1)} %refs_1_.3, bf16[32,1408]{1,0:T(8,128)(2,1)} %bitcast.9), custom_call_target="tpu_custom_call" | custom-call | tf_op jit(solution)/shard_map/pallas_call | solution.py:470
  8.4 2.2 %collective-permute-start = (bf16[32,2304]{1,0:T(8,128)(2,1)}, bf16[32,2304]{1,0:T(8,128)(2,1)}, u32[]{:S(2)}, u32[]{:S(2)}) collective-permute-start(bf16[32,2304]{1,0:T(8,128)(2,1)} %get-tuple-element.35), channel_id=1, source_target_pairs={{0,16},{16,0},{1,17},{17,1},{2,18},{18,2},{3,19},{19,3},{4,20},{20... | collective-permute-start | bytes 442376 | tf_op jit(solution)/shard_map/ppermute | solution.py:471
  10.6 6.5 %shard_map.145 = (bf16[8,192,128]{2,1,0:T(8,128)(2,1)}, bf16[6,128,128]{2,1,0:T(8,128)(2,1)}, bf16[6,128,128]{2,1,0:T(8,128)(2,1)}, bf16[4,128,256]{2,1,0:T(8,128)(2,1)}, f32[4,128,128]{2,1,0:T(8,128)}) custom-call(bf16[2,128,256]{2,1,0:T(8,128)(2,1)} %refs_4_.3, bf16[2,128,256]{2,1,0:T(8,128)(2,1)} %refs_5_.3, bf16[2,128,256]{2,1,0:T(8,128)(2,1)} %refs_6_.1, ...), custom_call_target="tpu_custom_call" | custom-call | tf_op jit(solution)/shard_map/pallas_call | solution.py:552
  17.1 0.0 collective-permute-done
  17.1 1.6 %constant_dynamic-update-slice_fusion = bf16[64,2304]{1,0:T(8,128)(2,1)} fusion(bf16[64,2304]{1,0:T(8,128)(2,1)} %get-tuple-element.61, bf16[32,2304]{1,0:T(8,128)(2,1)} %collective-permute-done), kind=kLoop, calls=%fused_computation.4 | loop fusion | bytes 294912 | tf_op jit(solution)/shard_map/dynamic_update_slice | solution.py:476
  18.7 0.0 all-gather.2.cloned.1.call-update
  18.7 12.4 %all_to_all.30.got_ref = bf16[8,192,128]{2,1,0:T(8,128)(2,1)S(1)} all-to-all(bf16[8,192,128]{2,1,0:T(8,128)(2,1)} %get-tuple-element.36), channel_id=1, replica_groups=mesh['plane'=8,'far'=2,'near'=2,'core'=2,'tp'=4] {'far','near','core'}, dimensions={0} | all-to-all | bytes 786432 | tf_op jit(solution)/shard_map/all_to_all | solution.py:512
  31.1 1.7 %shard_map.147 = (f32[8,192,128]{2,1,0:T(8,128)S(1)}, bf16[8,192,128]{2,1,0:T(8,128)(2,1)}) custom-call(bf16[8,192,128]{2,1,0:T(8,128)(2,1)S(1)} %all_to_all.30.got_ref), custom_call_target="tpu_custom_call" | custom-call | tf_op jit(solution)/shard_map/pallas_call | solution.py:566
  32.7 8.3 %all-to-all-start.1 = ((bf16[8,192,128]{2,1,0:T(8,128)(2,1)}), bf16[8,192,128]{2,1,0:T(8,128)(2,1)S(1)}, u32[]{:S(2)}, u32[]{:S(2)}) async-start(bf16[8,192,128]{2,1,0:T(8,128)(2,1)} %get-tuple-element.43), calls=%async_computation.1 | async-start | bytes 786432 | tf_op jit(solution)/shard_map/all_to_all | solution.py:512
  41.1 2.8 %shard_map.148 = (f32[4,128,128]{2,1,0:T(8,128)}, bf16[4,128,256]{2,1,0:T(8,128)(2,1)}, f32[4,128,128]{2,1,0:T(8,128)}, f32[4,128,128]{2,1,0:T(8,128)}) custom-call(bf16[6,128,128]{2,1,0:T(8,128)(2,1)} %get-tuple-element.45.refs_0_, bf16[6,128,128]{2,1,0:T(8,128)(2,1)} %get-tuple-element.46.refs_1_, bf16[4,128,256]{2,1,0:T(8,128)(2,1)} %get-tuple-element.47.refs_2_, ...), custom_call_target="tpu_custom_call" | custom-call | tf_op jit(solution)/shard_map/pallas_call | solution.py:582
  43.9 0.0 copy-done
  43.9 0.1 constant_dynamic-slice_fusion
  44.0 16.4 %all-to-all-done.1.every_ref = bf16[8,192,128]{2,1,0:T(8,128)(2,1)S(1)} async-done(((bf16[8,192,128]{2,1,0:T(8,128)(2,1)}), bf16[8,192,128]{2,1,0:T(8,128)(2,1)S(1)}, u32[]{:S(2)}, u32[]{:S(2)}) %all-to-all-start.1) | async-done | bytes 393248 | tf_op jit(solution)/shard_map/all_to_all | solution.py:512
  60.4 1.1 shard_map.149
  61.5 10.6 %all_to_all.31.refs_0_ = bf16[8,64,128]{2,1,0:T(8,128)(2,1)} all-to-all(bf16[8,64,128]{2,1,0:T(8,128)(2,1)S(1)} %shard_map.149), channel_id=1, replica_groups=mesh['plane'=8,'far'=2,'near'=2,'core'=2,'tp'=4] {'far','near','core'}, dimensions={0} | all-to-all | bytes 262144 | tf_op jit(solution)/shard_map/all_to_all | solution.py:512
  72.1 3.2 %shard_map.150 = bf16[4,128,512]{2,1,0:T(8,128)(2,1)} custom-call(bf16[8,64,128]{2,1,0:T(8,128)(2,1)} %all_to_all.31.refs_0_, f32[4,128,128]{2,1,0:T(8,128)} %get-tuple-element.57.refs_1_, bf16[4,128,256]{2,1,0:T(8,128)(2,1)} %get-tuple-element.58.refs_2_, f32[4,128,128]{2,1,0:T(8,128)} %get-tuple-element.59.refs_3_, ...), custom_call_target="tpu_custom_call" | custom-call | tf_op jit(solution)/shard_map/pallas_call | solution.py:598
  75.4 13.5 %all_to_all.32 = bf16[4,128,512]{2,1,0:T(8,128)(2,1)S(1)} all-to-all(bf16[4,128,512]{2,1,0:T(8,128)(2,1)} %shard_map.150), channel_id=1, replica_groups=mesh['plane'=8,'far'=2,'near'=2,'core'=2,'tp'=4] {'tp'}, dimensions={0} | all-to-all | bytes 1048576 | tf_op jit(solution)/shard_map/all_to_all | solution.py:512
  88.9 0.1 convert_reduce_fusion.1
  89.0 0.0 copy-start.1
  89.0 0.1 broadcast_in_dim.2
  89.1 21.6 %all_to_all.33.state_ref = bf16[8,128,512]{2,1,0:T(8,128)(2,1)} all-to-all(bf16[8,128,512]{2,1,0:T(8,128)(2,1)S(1)} %broadcast_in_dim.2), channel_id=1, replica_groups=mesh['plane'=8,'far'=2,'near'=2,'core'=2,'tp'=4] {'far','tp'}, dimensions={0} | all-to-all | bytes 2097152 | tf_op jit(solution)/shard_map/all_to_all | solution.py:512
  110.7 0.0 all-gather.2.cloned.1.call-done
  110.7 0.0 copy-done.1
  110.7 7.8 %shard_map.151 = bf16[8,128,512]{2,1,0:T(8,128)(2,1)S(1)} custom-call(s32[1]{0:T(128)} %bitcast.far_ref, bf16[8,128,512]{2,1,0:T(8,128)(2,1)} %all_to_all.33.state_ref, f32[1,2048]{1,0:T(1,128)S(1)} %bitcast.6, bf16[8,4,2,32,2304]{4,3,2,1,0:T(8,128)(2,1)} %bitcast.7), custom_call_target="tpu_custom_call" | custom-call | tf_op jit(solution)/shard_map/pallas_call | solution.py:429
  118.5 18.1 %all_to_all.34 = bf16[8,128,512]{2,1,0:T(8,128)(2,1)S(1)} all-to-all(bf16[8,128,512]{2,1,0:T(8,128)(2,1)S(1)} %shard_map.151), channel_id=1, replica_groups=mesh['plane'=8,'far'=2,'near'=2,'core'=2,'tp'=4] {'far','tp'}, dimensions={0} | all-to-all | bytes 2097152 | tf_op jit(solution)/shard_map/all_to_all | solution.py:512
  136.6 0.1 convert_reduce_fusion
  136.8 0.7 add_convert_fusion
  (1 shorter events, 0.0 us)
Async XLA Ops:
  6.5 37.4 %copy-start = (bf16[128,2048]{1,0:T(8,128)(2,1)S(1)}, bf16[128,2048]{1,0:T(8,128)(2,1)}, u32[]{:S(2)}) copy-start(bf16[128,2048]{1,0:T(8,128)(2,1)} %param.15) | copy-start | bytes 1572868
  6.5 104.2 %all-gather.2.cloned.1.call-start = ((), (), s32[]{:S(2)}) async-start(), calls=%async_computation.6 | async-start | bytes 9732096 | tf_op jit(solution)/shard_map/all_gather | solution.py:477
  8.4 8.7 %collective-permute-start = (bf16[32,2304]{1,0:T(8,128)(2,1)}, bf16[32,2304]{1,0:T(8,128)(2,1)}, u32[]{:S(2)}, u32[]{:S(2)}) collective-permute-start(bf16[32,2304]{1,0:T(8,128)(2,1)} %get-tuple-element.35), channel_id=1, source_target_pairs={{0,16},{16,0},{1,17},{17,1},{2,18},{18,2},{3,19},{19,3},{4,20},{20... | collective-permute-start | bytes 442376 | tf_op jit(solution)/shard_map/ppermute | solution.py:471
  32.7 27.6 %all-to-all-start.1 = ((bf16[8,192,128]{2,1,0:T(8,128)(2,1)}), bf16[8,192,128]{2,1,0:T(8,128)(2,1)S(1)}, u32[]{:S(2)}, u32[]{:S(2)}) async-start(bf16[8,192,128]{2,1,0:T(8,128)(2,1)} %get-tuple-element.43), calls=%async_computation.1 | async-start | bytes 786432 | tf_op jit(solution)/shard_map/all_to_all | solution.py:512
  89.0 21.8 %copy-start.1 = (f32[2048]{0:T(1024)S(1)}, f32[2048]{0:T(1024)}, u32[]{:S(2)}) copy-start(f32[2048]{0:T(1024)} %param.26) | copy-start | bytes 24580
Sparse Core Ops, SparseCore 0:
  18.8 83.2 all-gather.1

commit v11 on v10

--- a/solution.py
+++ b/solution.py
@@ -340,7 +340,7 @@
     finish()
 
 
-AHEAD = 4
+AHEAD = 16
 
 
 def feed_kernel(
@@ -364,20 +364,27 @@
     planes, sides, near, rows, width = w_ref.shape
     third = width // 3
     far = far_ref[0]
+    parts = [pl.ds(0, 2 * third), pl.ds(2 * third, third)]
     copies = [
-        [
-            pltpu.make_async_copy(
-                whole_ref.at[k, :, jnp.where(far == side, 0, 1)],
-                w_ref.at[k, side],
-                sems.at[k, side],
-            )
-            for side in range(sides)
-        ]
+        pltpu.make_async_copy(
+            whole_ref.at[k, :, jnp.where(far == side, 0, 1), :, lanes],
+            w_ref.at[k, side, :, :, lanes],
+            sems.at[part, k, side],
+        )
+        for part, lanes in enumerate(parts)
         for k in range(planes)
+        for side in range(sides)
     ]
-    for k in range(AHEAD):
-        for copy in copies[k]:
-            copy.start()
+    for copy in copies[:AHEAD]:
+        copy.start()
+
+    def arrive(part, first, count):
+        start = (part * planes + first) * sides
+        for k in range(start, start + count * sides):
+            copies[k].wait()
+            if k + AHEAD < len(copies):
+                copies[k + AHEAD].start()
+
     shares, tokens, columns = x_ref.shape
     tiles = shares // sides
     for copy in tokens_here:
@@ -396,12 +403,7 @@
     scale = jnp.concatenate(scales, 0)
     block = sides * near * rows
     for k in range(0, planes, 2):
-        for step in (k, k + 1):
-            for copy in copies[step]:
-                copy.wait()
-            if step + AHEAD < planes:
-                for copy in copies[step + AHEAD]:
-                    copy.start()
+        arrive(0, k, 2)
         part = dot_nn(
             n_ref[:, k * block : (k + 2) * block],
             w_ref[k : k + 2, :, :, :, : 2 * third].reshape(2 * block, 2 * third),
@@ -415,6 +417,7 @@
     active = (gate / (1.0 + jnp.exp(-gate)) * up).astype(bf16)
     per = planes // tiles
     for k in range(tiles):
+        arrive(1, k * per, per)
         down = w_ref[k * per : (k + 1) * per, :, :, :, 2 * third :].reshape(per * block, third)
         out = dot_nt(active, down).astype(bf16)
         for side in range(sides):
@@ -438,7 +441,7 @@
             pltpu.VMEM(state.shape, bf16),
             pltpu.VMEM(gain.shape, f32),
             pltpu.VMEM(state.shape, bf16),
-            pltpu.SemaphoreType.DMA((planes, sides)),
+            pltpu.SemaphoreType.DMA((2, planes, sides)),
             pltpu.SemaphoreType.DMA((2,)),
             pltpu.SemaphoreType.DMA((1, shares)),
         ],
@@ -554,7 +557,7 @@
         (array((SHARES, LANES + HALF, LANES), bf16), pairs, pairs, doubled, blocks),
         [HBM] * len(inputs),
         inputs,
-        66_400_000,
+        65_900_000,
         6,
         [(len(inputs), 2)],
     )(*inputs)

time: 145 us -> 143 us (0.986)
  no operation moved by 1% of the time
where the time goes in v11:
time: 143 us
  blocking collectives  76.5 us (53%)
  Pallas kernels  24.2 us (17%)
  waiting for transfers between devices  16.4 us (11%)
  between operations  13.5 us (9%)
  starting transfers between devices  10.6 us (7%)
    all_to_all x5, blocking collectives, exchange(): return lax.all_to_all(value, axis, 0, 0, tiled=True)  76.5 us
    all_to_all x1, waiting for transfers between devices, exchange(): return lax.all_to_all(value, axis, 0, 0, tiled=True)  16.4 us
    all_to_all x1, starting transfers between devices, exchange(): return lax.all_to_all(value, axis, 0, 0, tiled=True)  8.35 us
    pallas_call x1, Pallas kernels, feed_forward(): pl.pallas_call(feed_kernel, out_shape=array((shares, tokens, columns), bf...  7.04 us
    pallas_call x1, Pallas kernels, on_device(): call(solve_kernel, (array((SHARES, LANES + HALF, LANES), bf16), pairs, pa...  6.46 us
    pallas_call x1, Pallas kernels, on_device(): call(mix_kernel, (array((features // columns, TOK, columns), bf16),), [HB...  3.24 us
  transfers between devices with their start and end apart: 3, of which 1 were waited for; matrix products, arithmetic and copies ran while one was open for 0% of the time, Pallas kernels for 11%

profile of v11, /device:TPU:2, one launch (start us, length us, event | category | flops | bytes accessed | tf_op | source)
XLA Modules:
  0.0 142.9 jit_solution(2035742787117759638)
XLA Ops:
  6.5 0.0 copy-start
  6.5 0.0 all-gather.2.cloned.1.call-start
  6.5 1.8 %shard_map.146 = (bf16[64,2304]{1,0:T(8,128)(2,1)}, bf16[32,2304]{1,0:T(8,128)(2,1)}) custom-call(s32[1]{0:T(128)} %bitcast.far_ref, bf16[32,1408]{1,0:T(8,128)(2,1)} %refs_0_.3, bf16[32,1408]{1,0:T(8,128)(2,1)} %refs_1_.3, bf16[32,1408]{1,0:T(8,128)(2,1)} %bitcast.9), custom_call_target="tpu_custom_call" | custom-call | tf_op jit(solution)/shard_map/pallas_call | solution.py:473
  8.4 2.2 %collective-permute-start = (bf16[32,2304]{1,0:T(8,128)(2,1)}, bf16[32,2304]{1,0:T(8,128)(2,1)S(1)}, u32[]{:S(2)}, u32[]{:S(2)}) collective-permute-start(bf16[32,2304]{1,0:T(8,128)(2,1)} %get-tuple-element.35), channel_id=1, source_target_pairs={{0,16},{16,0},{1,17},{17,1},{2,18},{18,2},{3,19},{19,3},{4,20},{20... | collective-permute-start | bytes 442376 | tf_op jit(solution)/shard_map/ppermute | solution.py:474
  10.6 6.5 %shard_map.145 = (bf16[8,192,128]{2,1,0:T(8,128)(2,1)}, bf16[6,128,128]{2,1,0:T(8,128)(2,1)}, bf16[6,128,128]{2,1,0:T(8,128)(2,1)}, bf16[4,128,256]{2,1,0:T(8,128)(2,1)}, f32[4,128,128]{2,1,0:T(8,128)}) custom-call(bf16[2,128,256]{2,1,0:T(8,128)(2,1)} %refs_4_.3, bf16[2,128,256]{2,1,0:T(8,128)(2,1)} %refs_5_.3, bf16[2,128,256]{2,1,0:T(8,128)(2,1)} %refs_6_.1, ...), custom_call_target="tpu_custom_call" | custom-call | tf_op jit(solution)/shard_map/pallas_call | solution.py:555
  17.1 0.0 collective-permute-done
  17.1 0.7 constant_dynamic-update-slice_fusion
  17.7 0.0 all-gather.2.cloned.1.call-update
  17.8 12.4 %all_to_all.30.got_ref = bf16[8,192,128]{2,1,0:T(8,128)(2,1)S(1)} all-to-all(bf16[8,192,128]{2,1,0:T(8,128)(2,1)} %get-tuple-element.36), channel_id=1, replica_groups=mesh['plane'=8,'far'=2,'near'=2,'core'=2,'tp'=4] {'far','near','core'}, dimensions={0} | all-to-all | bytes 786432 | tf_op jit(solution)/shard_map/all_to_all | solution.py:515
  30.1 1.7 %shard_map.147 = (f32[8,192,128]{2,1,0:T(8,128)S(1)}, bf16[8,192,128]{2,1,0:T(8,128)(2,1)}) custom-call(bf16[8,192,128]{2,1,0:T(8,128)(2,1)S(1)} %all_to_all.30.got_ref), custom_call_target="tpu_custom_call" | custom-call | tf_op jit(solution)/shard_map/pallas_call | solution.py:569
  31.8 8.3 %all-to-all-start.1 = ((bf16[8,192,128]{2,1,0:T(8,128)(2,1)}), bf16[8,192,128]{2,1,0:T(8,128)(2,1)S(1)}, u32[]{:S(2)}, u32[]{:S(2)}) async-start(bf16[8,192,128]{2,1,0:T(8,128)(2,1)} %get-tuple-element.43), calls=%async_computation.1 | async-start | bytes 786432 | tf_op jit(solution)/shard_map/all_to_all | solution.py:515
  40.2 2.8 %shard_map.148 = (f32[4,128,128]{2,1,0:T(8,128)}, bf16[4,128,256]{2,1,0:T(8,128)(2,1)}, f32[4,128,128]{2,1,0:T(8,128)}, f32[4,128,128]{2,1,0:T(8,128)}) custom-call(bf16[6,128,128]{2,1,0:T(8,128)(2,1)} %get-tuple-element.45.refs_0_, bf16[6,128,128]{2,1,0:T(8,128)(2,1)} %get-tuple-element.46.refs_1_, bf16[4,128,256]{2,1,0:T(8,128)(2,1)} %get-tuple-element.47.refs_2_, ...), custom_call_target="tpu_custom_call" | custom-call | tf_op jit(solution)/shard_map/pallas_call | solution.py:585
  43.0 0.0 copy-done
  43.0 0.1 constant_dynamic-slice_fusion
  43.1 16.4 %all-to-all-done.1.every_ref = bf16[8,192,128]{2,1,0:T(8,128)(2,1)S(1)} async-done(((bf16[8,192,128]{2,1,0:T(8,128)(2,1)}), bf16[8,192,128]{2,1,0:T(8,128)(2,1)S(1)}, u32[]{:S(2)}, u32[]{:S(2)}) %all-to-all-start.1) | async-done | bytes 393248 | tf_op jit(solution)/shard_map/all_to_all | solution.py:515
  59.5 1.1 shard_map.149
  60.6 10.6 %all_to_all.31.refs_0_ = bf16[8,64,128]{2,1,0:T(8,128)(2,1)} all-to-all(bf16[8,64,128]{2,1,0:T(8,128)(2,1)S(1)} %shard_map.149), channel_id=1, replica_groups=mesh['plane'=8,'far'=2,'near'=2,'core'=2,'tp'=4] {'far','near','core'}, dimensions={0} | all-to-all | bytes 262144 | tf_op jit(solution)/shard_map/all_to_all | solution.py:515
  71.2 3.2 %shard_map.150 = bf16[4,128,512]{2,1,0:T(8,128)(2,1)} custom-call(bf16[8,64,128]{2,1,0:T(8,128)(2,1)} %all_to_all.31.refs_0_, f32[4,128,128]{2,1,0:T(8,128)} %get-tuple-element.57.refs_1_, bf16[4,128,256]{2,1,0:T(8,128)(2,1)} %get-tuple-element.58.refs_2_, f32[4,128,128]{2,1,0:T(8,128)} %get-tuple-element.59.refs_3_, ...), custom_call_target="tpu_custom_call" | custom-call | tf_op jit(solution)/shard_map/pallas_call | solution.py:601
  74.5 13.5 %all_to_all.32 = bf16[4,128,512]{2,1,0:T(8,128)(2,1)S(1)} all-to-all(bf16[4,128,512]{2,1,0:T(8,128)(2,1)} %shard_map.150), channel_id=1, replica_groups=mesh['plane'=8,'far'=2,'near'=2,'core'=2,'tp'=4] {'tp'}, dimensions={0} | all-to-all | bytes 1048576 | tf_op jit(solution)/shard_map/all_to_all | solution.py:515
  87.9 0.1 convert_reduce_fusion.1
  88.0 0.0 copy-start.1
  88.1 0.1 broadcast_in_dim.2
  88.1 21.9 %all_to_all.33.state_ref = bf16[8,128,512]{2,1,0:T(8,128)(2,1)} all-to-all(bf16[8,128,512]{2,1,0:T(8,128)(2,1)S(1)} %broadcast_in_dim.2), channel_id=1, replica_groups=mesh['plane'=8,'far'=2,'near'=2,'core'=2,'tp'=4] {'far','tp'}, dimensions={0} | all-to-all | bytes 2097152 | tf_op jit(solution)/shard_map/all_to_all | solution.py:515
  110.1 0.0 all-gather.2.cloned.1.call-done
  110.1 0.0 copy-done.1
  110.1 7.0 %shard_map.151 = bf16[8,128,512]{2,1,0:T(8,128)(2,1)S(1)} custom-call(s32[1]{0:T(128)} %bitcast.far_ref, bf16[8,128,512]{2,1,0:T(8,128)(2,1)} %all_to_all.33.state_ref, f32[1,2048]{1,0:T(1,128)S(1)} %bitcast.6, bf16[8,4,2,32,2304]{4,3,2,1,0:T(8,128)(2,1)} %bitcast.7), custom_call_target="tpu_custom_call" | custom-call | tf_op jit(solution)/shard_map/pallas_call | solution.py:432
  117.1 18.1 %all_to_all.34 = bf16[8,128,512]{2,1,0:T(8,128)(2,1)S(1)} all-to-all(bf16[8,128,512]{2,1,0:T(8,128)(2,1)S(1)} %shard_map.151), channel_id=1, replica_groups=mesh['plane'=8,'far'=2,'near'=2,'core'=2,'tp'=4] {'far','tp'}, dimensions={0} | all-to-all | bytes 2097152 | tf_op jit(solution)/shard_map/all_to_all | solution.py:515
  135.2 0.1 convert_reduce_fusion
  135.4 0.7 add_convert_fusion
  (1 shorter events, 0.0 us)
Async XLA Ops:
  6.5 36.4 %copy-start = (bf16[128,2048]{1,0:T(8,128)(2,1)S(1)}, bf16[128,2048]{1,0:T(8,128)(2,1)}, u32[]{:S(2)}) copy-start(bf16[128,2048]{1,0:T(8,128)(2,1)} %param.15) | copy-start | bytes 1572868
  6.5 103.5 %all-gather.2.cloned.1.call-start = ((), (), s32[]{:S(2)}) async-start(), calls=%async_computation.6 | async-start | bytes 9732096 | tf_op jit(solution)/shard_map/all_gather | solution.py:480
  8.4 8.7 %collective-permute-start = (bf16[32,2304]{1,0:T(8,128)(2,1)}, bf16[32,2304]{1,0:T(8,128)(2,1)S(1)}, u32[]{:S(2)}, u32[]{:S(2)}) collective-permute-start(bf16[32,2304]{1,0:T(8,128)(2,1)} %get-tuple-element.35), channel_id=1, source_target_pairs={{0,16},{16,0},{1,17},{17,1},{2,18},{18,2},{3,19},{19,3},{4,20},{20... | collective-permute-start | bytes 442376 | tf_op jit(solution)/shard_map/ppermute | solution.py:474
  31.8 27.6 %all-to-all-start.1 = ((bf16[8,192,128]{2,1,0:T(8,128)(2,1)}), bf16[8,192,128]{2,1,0:T(8,128)(2,1)S(1)}, u32[]{:S(2)}, u32[]{:S(2)}) async-start(bf16[8,192,128]{2,1,0:T(8,128)(2,1)} %get-tuple-element.43), calls=%async_computation.1 | async-start | bytes 786432 | tf_op jit(solution)/shard_map/all_to_all | solution.py:515
  88.0 22.1 %copy-start.1 = (f32[2048]{0:T(1024)S(1)}, f32[2048]{0:T(1024)}, u32[]{:S(2)}) copy-start(f32[2048]{0:T(1024)} %param.26) | copy-start | bytes 24580
Sparse Core Ops, SparseCore 0:
  17.9 83.2 all-gather.1

commit v12 on v11

--- a/solution.py
+++ b/solution.py
@@ -340,26 +340,25 @@
     finish()
 
 
-AHEAD = 16
+AHEAD = 24
 
 
 def feed_kernel(
     far_ref,
-    state_ref,
+    x_ref,
     gain_in_ref,
     whole_ref,
     sent_ref,
     w_ref,
     n_ref,
     acc_ref,
-    x_ref,
     gain_ref,
     y_ref,
     sems,
     in_sems,
     out_sems,
 ):
-    tokens_here = fetch([state_ref, gain_in_ref], [x_ref, gain_ref], in_sems)
+    (gain_here,) = fetch([gain_in_ref], [gain_ref], in_sems)
     put, finish = writer([y_ref], [sent_ref], out_sems)
     planes, sides, near, rows, width = w_ref.shape
     third = width // 3
@@ -387,8 +386,7 @@
 
     shares, tokens, columns = x_ref.shape
     tiles = shares // sides
-    for copy in tokens_here:
-        copy.wait()
+    gain_here.wait()
     scales = []
     for side in range(sides):
         total = 0.0
@@ -432,20 +430,19 @@
     return pl.pallas_call(
         feed_kernel,
         out_shape=array((shares, tokens, columns), bf16),
-        in_specs=[SMEM, HBM, HBM, HBM],
+        in_specs=[SMEM, VMEM, HBM, HBM],
         out_specs=HBM,
         scratch_shapes=[
             pltpu.VMEM((planes, sides, near, rows, width), bf16),
             pltpu.VMEM((sides * tokens, gain.shape[1]), bf16),
             pltpu.VMEM((sides * tokens, 2 * width // 3), f32),
-            pltpu.VMEM(state.shape, bf16),
             pltpu.VMEM(gain.shape, f32),
             pltpu.VMEM(state.shape, bf16),
             pltpu.SemaphoreType.DMA((2, planes, sides)),
-            pltpu.SemaphoreType.DMA((2,)),
+            pltpu.SemaphoreType.DMA((1,)),
             pltpu.SemaphoreType.DMA((1, shares)),
         ],
-        compiler_params=pltpu.CompilerParams(vmem_limit_bytes=55_000_000),
+        compiler_params=pltpu.CompilerParams(vmem_limit_bytes=52_000_000),
     )(far, state, gain, whole)
 
 

time: 143 us -> 143 us (level)
  no operation moved by 1% of the time
where the time goes in v12:
time: 143 us
  blocking collectives  76.4 us (53%)
  Pallas kernels  23.9 us (17%)
  waiting for transfers between devices  16.4 us (11%)
  between operations  13.5 us (9%)
  starting transfers between devices  10.6 us (7%)
    all_to_all x5, blocking collectives, exchange(): return lax.all_to_all(value, axis, 0, 0, tiled=True)  76.4 us
    all_to_all x1, waiting for transfers between devices, exchange(): return lax.all_to_all(value, axis, 0, 0, tiled=True)  16.4 us
    all_to_all x1, starting transfers between devices, exchange(): return lax.all_to_all(value, axis, 0, 0, tiled=True)  8.35 us
    pallas_call x1, Pallas kernels, feed_forward(): pl.pallas_call(feed_kernel, out_shape=array((shares, tokens, columns), bf...  6.73 us
    pallas_call x1, Pallas kernels, on_device(): call(solve_kernel, (array((SHARES, LANES + HALF, LANES), bf16), pairs, pa...  6.46 us
    pallas_call x1, Pallas kernels, on_device(): call(mix_kernel, (array((features // columns, TOK, columns), bf16),), [HB...  3.24 us
  transfers between devices with their start and end apart: 3, of which 1 were waited for; matrix products, arithmetic and copies ran while one was open for 0% of the time, Pallas kernels for 11%

profile of v12, /device:TPU:2, one launch (start us, length us, event | category | flops | bytes accessed | tf_op | source)
XLA Modules:
  0.0 142.5 jit_solution(1948658272035561169)
XLA Ops:
  6.5 0.0 copy-start
  6.5 0.0 all-gather.2.cloned.1.call-start
  6.5 1.8 %shard_map.146 = (bf16[64,2304]{1,0:T(8,128)(2,1)}, bf16[32,2304]{1,0:T(8,128)(2,1)}) custom-call(s32[1]{0:T(128)} %bitcast.far_ref, bf16[32,1408]{1,0:T(8,128)(2,1)} %refs_0_.3, bf16[32,1408]{1,0:T(8,128)(2,1)} %refs_1_.3, bf16[32,1408]{1,0:T(8,128)(2,1)} %bitcast.9), custom_call_target="tpu_custom_call" | custom-call | tf_op jit(solution)/shard_map/pallas_call | solution.py:470
  8.4 2.2 %collective-permute-start = (bf16[32,2304]{1,0:T(8,128)(2,1)}, bf16[32,2304]{1,0:T(8,128)(2,1)S(1)}, u32[]{:S(2)}, u32[]{:S(2)}) collective-permute-start(bf16[32,2304]{1,0:T(8,128)(2,1)} %get-tuple-element.35), channel_id=1, source_target_pairs={{0,16},{16,0},{1,17},{17,1},{2,18},{18,2},{3,19},{19,3},{4,20},{20... | collective-permute-start | bytes 442376 | tf_op jit(solution)/shard_map/ppermute | solution.py:471
  10.6 6.5 %shard_map.145 = (bf16[8,192,128]{2,1,0:T(8,128)(2,1)}, bf16[6,128,128]{2,1,0:T(8,128)(2,1)}, bf16[6,128,128]{2,1,0:T(8,128)(2,1)}, bf16[4,128,256]{2,1,0:T(8,128)(2,1)}, f32[4,128,128]{2,1,0:T(8,128)}) custom-call(bf16[2,128,256]{2,1,0:T(8,128)(2,1)} %refs_4_.3, bf16[2,128,256]{2,1,0:T(8,128)(2,1)} %refs_5_.3, bf16[2,128,256]{2,1,0:T(8,128)(2,1)} %refs_6_.1, ...), custom_call_target="tpu_custom_call" | custom-call | tf_op jit(solution)/shard_map/pallas_call | solution.py:552
  17.1 0.0 collective-permute-done
  17.1 0.7 constant_dynamic-update-slice_fusion
  17.7 0.0 all-gather.2.cloned.1.call-update
  17.8 12.4 %all_to_all.30.got_ref = bf16[8,192,128]{2,1,0:T(8,128)(2,1)S(1)} all-to-all(bf16[8,192,128]{2,1,0:T(8,128)(2,1)} %get-tuple-element.36), channel_id=1, replica_groups=mesh['plane'=8,'far'=2,'near'=2,'core'=2,'tp'=4] {'far','near','core'}, dimensions={0} | all-to-all | bytes 786432 | tf_op jit(solution)/shard_map/all_to_all | solution.py:512
  30.1 1.7 %shard_map.147 = (f32[8,192,128]{2,1,0:T(8,128)S(1)}, bf16[8,192,128]{2,1,0:T(8,128)(2,1)}) custom-call(bf16[8,192,128]{2,1,0:T(8,128)(2,1)S(1)} %all_to_all.30.got_ref), custom_call_target="tpu_custom_call" | custom-call | tf_op jit(solution)/shard_map/pallas_call | solution.py:566
  31.8 8.3 %all-to-all-start.1 = ((bf16[8,192,128]{2,1,0:T(8,128)(2,1)}), bf16[8,192,128]{2,1,0:T(8,128)(2,1)S(1)}, u32[]{:S(2)}, u32[]{:S(2)}) async-start(bf16[8,192,128]{2,1,0:T(8,128)(2,1)} %get-tuple-element.43), calls=%async_computation.1 | async-start | bytes 786432 | tf_op jit(solution)/shard_map/all_to_all | solution.py:512
  40.2 2.8 %shard_map.148 = (f32[4,128,128]{2,1,0:T(8,128)}, bf16[4,128,256]{2,1,0:T(8,128)(2,1)}, f32[4,128,128]{2,1,0:T(8,128)}, f32[4,128,128]{2,1,0:T(8,128)}) custom-call(bf16[6,128,128]{2,1,0:T(8,128)(2,1)} %get-tuple-element.45.refs_0_, bf16[6,128,128]{2,1,0:T(8,128)(2,1)} %get-tuple-element.46.refs_1_, bf16[4,128,256]{2,1,0:T(8,128)(2,1)} %get-tuple-element.47.refs_2_, ...), custom_call_target="tpu_custom_call" | custom-call | tf_op jit(solution)/shard_map/pallas_call | solution.py:582
  43.0 0.0 copy-done
  43.0 0.1 constant_dynamic-slice_fusion
  43.1 16.4 %all-to-all-done.1.every_ref = bf16[8,192,128]{2,1,0:T(8,128)(2,1)S(1)} async-done(((bf16[8,192,128]{2,1,0:T(8,128)(2,1)}), bf16[8,192,128]{2,1,0:T(8,128)(2,1)S(1)}, u32[]{:S(2)}, u32[]{:S(2)}) %all-to-all-start.1) | async-done | bytes 393248 | tf_op jit(solution)/shard_map/all_to_all | solution.py:512
  59.5 1.1 shard_map.149
  60.6 10.6 %all_to_all.31.refs_0_ = bf16[8,64,128]{2,1,0:T(8,128)(2,1)} all-to-all(bf16[8,64,128]{2,1,0:T(8,128)(2,1)S(1)} %shard_map.149), channel_id=1, replica_groups=mesh['plane'=8,'far'=2,'near'=2,'core'=2,'tp'=4] {'far','near','core'}, dimensions={0} | all-to-all | bytes 262144 | tf_op jit(solution)/shard_map/all_to_all | solution.py:512
  71.2 3.2 %shard_map.150 = bf16[4,128,512]{2,1,0:T(8,128)(2,1)} custom-call(bf16[8,64,128]{2,1,0:T(8,128)(2,1)} %all_to_all.31.refs_0_, f32[4,128,128]{2,1,0:T(8,128)} %get-tuple-element.57.refs_1_, bf16[4,128,256]{2,1,0:T(8,128)(2,1)} %get-tuple-element.58.refs_2_, f32[4,128,128]{2,1,0:T(8,128)} %get-tuple-element.59.refs_3_, ...), custom_call_target="tpu_custom_call" | custom-call | tf_op jit(solution)/shard_map/pallas_call | solution.py:598
  74.5 13.5 %all_to_all.32 = bf16[4,128,512]{2,1,0:T(8,128)(2,1)S(1)} all-to-all(bf16[4,128,512]{2,1,0:T(8,128)(2,1)} %shard_map.150), channel_id=1, replica_groups=mesh['plane'=8,'far'=2,'near'=2,'core'=2,'tp'=4] {'tp'}, dimensions={0} | all-to-all | bytes 1048576 | tf_op jit(solution)/shard_map/all_to_all | solution.py:512
  87.9 0.1 convert_reduce_fusion.1
  88.0 0.0 copy-start.1
  88.1 0.1 broadcast_in_dim.2
  88.1 21.8 %all_to_all.33.x_ref = bf16[8,128,512]{2,1,0:T(8,128)(2,1)S(1)} all-to-all(bf16[8,128,512]{2,1,0:T(8,128)(2,1)S(1)} %broadcast_in_dim.2), channel_id=1, replica_groups=mesh['plane'=8,'far'=2,'near'=2,'core'=2,'tp'=4] {'far','tp'}, dimensions={0} | all-to-all | bytes 2097152 | tf_op jit(solution)/shard_map/all_to_all | solution.py:512
  110.0 0.0 all-gather.2.cloned.1.call-done
  110.0 0.0 copy-done.1
  110.0 6.7 %shard_map.151 = bf16[8,128,512]{2,1,0:T(8,128)(2,1)S(1)} custom-call(s32[1]{0:T(128)} %bitcast.far_ref, bf16[8,128,512]{2,1,0:T(8,128)(2,1)S(1)} %all_to_all.33.x_ref, f32[1,2048]{1,0:T(1,128)S(1)} %bitcast.6, bf16[8,4,2,32,2304]{4,3,2,1,0:T(8,128)(2,1)} %bitcast.7), custom_call_target="tpu_custom_call" | custom-call | tf_op jit(solution)/shard_map/pallas_call | solution.py:430
  116.7 18.1 %all_to_all.34 = bf16[8,128,512]{2,1,0:T(8,128)(2,1)S(1)} all-to-all(bf16[8,128,512]{2,1,0:T(8,128)(2,1)S(1)} %shard_map.151), channel_id=1, replica_groups=mesh['plane'=8,'far'=2,'near'=2,'core'=2,'tp'=4] {'far','tp'}, dimensions={0} | all-to-all | bytes 2097152 | tf_op jit(solution)/shard_map/all_to_all | solution.py:512
  134.8 0.1 convert_reduce_fusion
  135.0 0.7 add_convert_fusion
  (1 shorter events, 0.0 us)
Async XLA Ops:
  6.5 36.4 %copy-start = (bf16[128,2048]{1,0:T(8,128)(2,1)S(1)}, bf16[128,2048]{1,0:T(8,128)(2,1)}, u32[]{:S(2)}) copy-start(bf16[128,2048]{1,0:T(8,128)(2,1)} %param.15) | copy-start | bytes 1572868
  6.5 103.4 %all-gather.2.cloned.1.call-start = ((), (), s32[]{:S(2)}) async-start(), calls=%async_computation.6 | async-start | bytes 9732096 | tf_op jit(solution)/shard_map/all_gather | solution.py:477
  8.4 8.7 %collective-permute-start = (bf16[32,2304]{1,0:T(8,128)(2,1)}, bf16[32,2304]{1,0:T(8,128)(2,1)S(1)}, u32[]{:S(2)}, u32[]{:S(2)}) collective-permute-start(bf16[32,2304]{1,0:T(8,128)(2,1)} %get-tuple-element.35), channel_id=1, source_target_pairs={{0,16},{16,0},{1,17},{17,1},{2,18},{18,2},{3,19},{19,3},{4,20},{20... | collective-permute-start | bytes 442376 | tf_op jit(solution)/shard_map/ppermute | solution.py:471
  31.8 27.6 %all-to-all-start.1 = ((bf16[8,192,128]{2,1,0:T(8,128)(2,1)}), bf16[8,192,128]{2,1,0:T(8,128)(2,1)S(1)}, u32[]{:S(2)}, u32[]{:S(2)}) async-start(bf16[8,192,128]{2,1,0:T(8,128)(2,1)} %get-tuple-element.43), calls=%async_computation.1 | async-start | bytes 786432 | tf_op jit(solution)/shard_map/all_to_all | solution.py:512
  88.0 22.0 %copy-start.1 = (f32[2048]{0:T(1024)S(1)}, f32[2048]{0:T(1024)}, u32[]{:S(2)}) copy-start(f32[2048]{0:T(1024)} %param.26) | copy-start | bytes 24580
Sparse Core Ops, SparseCore 0:
  17.9 83.2 all-gather.1

commit v13 on v12

--- a/solution.py
+++ b/solution.py
@@ -447,27 +447,42 @@
 
 
 def pack_kernel(far_ref, *refs):
-    inputs, (kept_ref, given_ref), scratch, sems = refs[:3], refs[3:5], refs[5:8], refs[8]
+    inputs, outputs, scratch, (kept_ref, given_ref), sems, out_sems = (
+        refs[:3],
+        refs[3:5],
+        refs[5:8],
+        refs[8:10],
+        refs[10],
+        refs[11],
+    )
+    rows = given_ref.shape[0]
+    puts = []
     copies = fetch(inputs, scratch, sems)
     wide = kept_ref.shape[1] // 3
     first = far_ref[0] == 0
     for k, copy in enumerate(copies):
         copy.wait()
         lanes = slice(k * wide, (k + 1) * wide)
-        kept_ref[given_ref.shape[0] :, lanes] = jnp.zeros((given_ref.shape[0], wide), bf16)
         near = scratch[k][:, :wide]
         rest = scratch[k][:, wide:]
         blank = jnp.zeros((rest.shape[0], 2 * wide - scratch[k].shape[1]), bf16)
         far = jnp.concatenate([rest, blank], axis=1)
-        kept_ref[: near.shape[0], lanes] = jnp.where(first, near, far)
+        kept_ref[:rows, lanes] = jnp.where(first, near, far)
         given_ref[:, lanes] = jnp.where(first, far, near)
+        window = (pl.ds(0, rows), pl.ds(k * wide, wide))
+        for which, (a, b) in enumerate(zip((kept_ref, given_ref), outputs)):
+            put = pltpu.make_async_copy(a.at[window], b.at[window], out_sems.at[which, k])
+            put.start()
+            puts.append(put)
+    for put in puts:
+        put.wait()
 
 
 def swapped(far, parts):
     rows, hidden = parts[0].shape
     wide = -(-hidden // (2 * LANES)) * LANES
     packed = (array((2 * rows, 3 * wide), bf16), array((rows, 3 * wide), bf16))
-    kept, given = call(pack_kernel, packed, [SMEM] + [HBM] * 3, parts, 62_000_000)(far, *parts)
+    kept, given = call(pack_kernel, packed, [SMEM] + [HBM] * 3, parts, 62_000_000, 3)(far, *parts)
     return kept, lax.ppermute(given, FAR, [(0, 1), (1, 0)])
 
 
@@ -560,7 +575,7 @@
     )(*inputs)
     place = lax.axis_index(PLANE).astype(jnp.int32).reshape(1)
     first_column = (lax.axis_index(TP) * columns).astype(jnp.uint32)
-    send, taken, place, first_column = lax.optimization_barrier((send, taken, place, first_column))
+    send, place, first_column = lax.optimization_barrier((send, place, first_column))
     whole = gathered(kept, taken)
     planes = lax.axis_size(PLANE)
     prefix, total = call(

time: 143 us -> 149 us (1.042)
  waiting for transfers between devices: 16.4 us -> 21.1 us
    ppermute x1, waiting for transfers between devices: 0.01 us -> 5.18 us  [swapped(): return (kept, lax.ppermute(given, FAR, [(0, 1), (1, 0)]))]
  transfers between devices with their start and end apart: 3 -> 3, of which waited for: 1 -> 2; matrix products, arithmetic and copies ran while one was open for 0% -> 0% of each run, Pallas kernels for 11% -> 10%
where the time goes in v13:
time: 149 us; the launch traced here: 148 us
  blocking collectives  77 us (52%)
  Pallas kernels  23.8 us (16%)
  waiting for transfers between devices  21.1 us (14%)
  between operations  13.5 us (9%)
  starting transfers between devices  11 us (7%)
    all_to_all x5, blocking collectives, exchange(): return lax.all_to_all(value, axis, 0, 0, tiled=True)  77 us
    all_to_all x1, waiting for transfers between devices, exchange(): return lax.all_to_all(value, axis, 0, 0, tiled=True)  16 us
    all_to_all x1, starting transfers between devices, exchange(): return lax.all_to_all(value, axis, 0, 0, tiled=True)  8.79 us
    pallas_call x1, Pallas kernels, feed_forward(): pl.pallas_call(feed_kernel, out_shape=array((shares, tokens, columns), bf...  6.74 us
    pallas_call x1, Pallas kernels, on_device(): call(solve_kernel, (array((SHARES, LANES + HALF, LANES), bf16), pairs, pa...  6.47 us
    ppermute x1, waiting for transfers between devices, swapped(): return (kept, lax.ppermute(given, FAR, [(0, 1), (1, 0)]))  5.18 us
    pallas_call x1, Pallas kernels, on_device(): call(mix_kernel, (array((features // columns, TOK, columns), bf16),), [HB...  3.2 us
  transfers between devices with their start and end apart: 3, of which 2 were waited for; matrix products, arithmetic and copies ran while one was open for 0% of the time, Pallas kernels for 10%

profile of v13, /device:TPU:2, one launch (start us, length us, event | category | flops | bytes accessed | tf_op | source)
XLA Modules:
  0.0 148.3 jit_solution(4715480952768945775)
XLA Ops:
  6.5 0.0 copy-start
  6.5 0.0 all-gather.2.cloned.1.call-start
  6.5 1.8 %shard_map.150 = (bf16[64,2304]{1,0:T(8,128)(2,1)}, bf16[32,2304]{1,0:T(8,128)(2,1)}) custom-call(s32[1]{0:T(128)} %bitcast.2.far_ref, bf16[32,1408]{1,0:T(8,128)(2,1)} %refs_0_.3, bf16[32,1408]{1,0:T(8,128)(2,1)} %refs_1_.3, bf16[32,1408]{1,0:T(8,128)(2,1)} %bitcast.9), custom_call_target="tpu_custom_call" | custom-call | tf_op jit(solution)/shard_map/pallas_call | solution.py:485
  8.3 2.2 %collective-permute-start = (bf16[32,2304]{1,0:T(8,128)(2,1)}, bf16[32,2304]{1,0:T(8,128)(2,1)S(1)}, u32[]{:S(2)}, u32[]{:S(2)}) collective-permute-start(bf16[32,2304]{1,0:T(8,128)(2,1)} %get-tuple-element.60), channel_id=1, source_target_pairs={{0,16},{16,0},{1,17},{17,1},{2,18},{18,2},{3,19},{19,3},{4,20},{20... | collective-permute-start | bytes 442376 | tf_op jit(solution)/shard_map/ppermute | solution.py:486
  10.5 5.2 %collective-permute-done = bf16[32,2304]{1,0:T(8,128)(2,1)S(1)} collective-permute-done((bf16[32,2304]{1,0:T(8,128)(2,1)}, bf16[32,2304]{1,0:T(8,128)(2,1)S(1)}, u32[]{:S(2)}, u32[]{:S(2)}) %collective-permute-start) | collective-permute-done | bytes 147488 | tf_op jit(solution)/shard_map/ppermute | solution.py:486
  15.7 0.7 constant_dynamic-update-slice_fusion
  16.4 0.0 all-gather.2.cloned.1.call-update
  16.4 6.5 %shard_map.145 = (bf16[8,192,128]{2,1,0:T(8,128)(2,1)}, bf16[6,128,128]{2,1,0:T(8,128)(2,1)}, bf16[6,128,128]{2,1,0:T(8,128)(2,1)}, bf16[4,128,256]{2,1,0:T(8,128)(2,1)}, f32[4,128,128]{2,1,0:T(8,128)}) custom-call(bf16[2,128,256]{2,1,0:T(8,128)(2,1)} %refs_4_.3, bf16[2,128,256]{2,1,0:T(8,128)(2,1)} %refs_5_.3, bf16[2,128,256]{2,1,0:T(8,128)(2,1)} %refs_6_.1, ...), custom_call_target="tpu_custom_call" | custom-call | tf_op jit(solution)/shard_map/pallas_call | solution.py:567
  22.9 14.9 %all_to_all.30.got_ref = bf16[8,192,128]{2,1,0:T(8,128)(2,1)S(1)} all-to-all(bf16[8,192,128]{2,1,0:T(8,128)(2,1)} %get-tuple-element.34), channel_id=1, replica_groups=mesh['plane'=8,'far'=2,'near'=2,'core'=2,'tp'=4] {'far','near','core'}, dimensions={0} | all-to-all | bytes 786432 | tf_op jit(solution)/shard_map/all_to_all | solution.py:527
  37.8 1.7 %shard_map.146 = (f32[8,192,128]{2,1,0:T(8,128)S(1)}, bf16[8,192,128]{2,1,0:T(8,128)(2,1)}) custom-call(bf16[8,192,128]{2,1,0:T(8,128)(2,1)S(1)} %all_to_all.30.got_ref), custom_call_target="tpu_custom_call" | custom-call | tf_op jit(solution)/shard_map/pallas_call | solution.py:581
  39.5 8.8 %all-to-all-start.1 = ((bf16[8,192,128]{2,1,0:T(8,128)(2,1)}), bf16[8,192,128]{2,1,0:T(8,128)(2,1)S(1)}, u32[]{:S(2)}, u32[]{:S(2)}) async-start(bf16[8,192,128]{2,1,0:T(8,128)(2,1)} %get-tuple-element.41), calls=%async_computation.1 | async-start | bytes 786432 | tf_op jit(solution)/shard_map/all_to_all | solution.py:527
  48.3 2.9 %shard_map.147 = (f32[4,128,128]{2,1,0:T(8,128)}, bf16[4,128,256]{2,1,0:T(8,128)(2,1)}, f32[4,128,128]{2,1,0:T(8,128)}, f32[4,128,128]{2,1,0:T(8,128)}) custom-call(bf16[6,128,128]{2,1,0:T(8,128)(2,1)} %get-tuple-element.43.refs_0_, bf16[6,128,128]{2,1,0:T(8,128)(2,1)} %get-tuple-element.44.refs_1_, bf16[4,128,256]{2,1,0:T(8,128)(2,1)} %get-tuple-element.45.refs_2_, ...), custom_call_target="tpu_custom_call" | custom-call | tf_op jit(solution)/shard_map/pallas_call | solution.py:597
  51.2 0.0 copy-done
  51.2 0.1 constant_dynamic-slice_fusion
  51.3 16.0 %all-to-all-done.1.every_ref = bf16[8,192,128]{2,1,0:T(8,128)(2,1)S(1)} async-done(((bf16[8,192,128]{2,1,0:T(8,128)(2,1)}), bf16[8,192,128]{2,1,0:T(8,128)(2,1)S(1)}, u32[]{:S(2)}, u32[]{:S(2)}) %all-to-all-start.1) | async-done | bytes 393248 | tf_op jit(solution)/shard_map/all_to_all | solution.py:527
  67.3 1.1 shard_map.148
  68.4 10.8 %all_to_all.31.refs_0_ = bf16[8,64,128]{2,1,0:T(8,128)(2,1)} all-to-all(bf16[8,64,128]{2,1,0:T(8,128)(2,1)S(1)} %shard_map.148), channel_id=1, replica_groups=mesh['plane'=8,'far'=2,'near'=2,'core'=2,'tp'=4] {'far','near','core'}, dimensions={0} | all-to-all | bytes 262144 | tf_op jit(solution)/shard_map/all_to_all | solution.py:527
  79.2 3.2 %shard_map.149 = bf16[4,128,512]{2,1,0:T(8,128)(2,1)} custom-call(bf16[8,64,128]{2,1,0:T(8,128)(2,1)} %all_to_all.31.refs_0_, f32[4,128,128]{2,1,0:T(8,128)} %get-tuple-element.55.refs_1_, bf16[4,128,256]{2,1,0:T(8,128)(2,1)} %get-tuple-element.56.refs_2_, f32[4,128,128]{2,1,0:T(8,128)} %get-tuple-element.57.refs_3_, ...), custom_call_target="tpu_custom_call" | custom-call | tf_op jit(solution)/shard_map/pallas_call | solution.py:613
  82.4 13.8 %all_to_all.32 = bf16[4,128,512]{2,1,0:T(8,128)(2,1)S(1)} all-to-all(bf16[4,128,512]{2,1,0:T(8,128)(2,1)} %shard_map.149), channel_id=1, replica_groups=mesh['plane'=8,'far'=2,'near'=2,'core'=2,'tp'=4] {'tp'}, dimensions={0} | all-to-all | bytes 1048576 | tf_op jit(solution)/shard_map/all_to_all | solution.py:527
  96.2 0.1 convert_reduce_fusion.1
  96.2 0.0 copy-start.1
  96.3 0.1 broadcast_in_dim.2
  96.4 19.5 %all_to_all.33.x_ref = bf16[8,128,512]{2,1,0:T(8,128)(2,1)S(1)} all-to-all(bf16[8,128,512]{2,1,0:T(8,128)(2,1)S(1)} %broadcast_in_dim.2), channel_id=1, replica_groups=mesh['plane'=8,'far'=2,'near'=2,'core'=2,'tp'=4] {'far','tp'}, dimensions={0} | all-to-all | bytes 2097152 | tf_op jit(solution)/shard_map/all_to_all | solution.py:527
  115.8 0.0 all-gather.2.cloned.1.call-done
  115.8 0.0 copy-done.1
  115.8 6.7 %shard_map.151 = bf16[8,128,512]{2,1,0:T(8,128)(2,1)S(1)} custom-call(s32[1]{0:T(128)} %bitcast.2.far_ref, bf16[8,128,512]{2,1,0:T(8,128)(2,1)S(1)} %all_to_all.33.x_ref, f32[1,2048]{1,0:T(1,128)S(1)} %bitcast.6, bf16[8,4,2,32,2304]{4,3,2,1,0:T(8,128)(2,1)} %bitcast.7), custom_call_target="tpu_custom_call" | custom-call | tf_op jit(solution)/shard_map/pallas_call | solution.py:430
  122.6 18.0 %all_to_all.34 = bf16[8,128,512]{2,1,0:T(8,128)(2,1)S(1)} all-to-all(bf16[8,128,512]{2,1,0:T(8,128)(2,1)S(1)} %shard_map.151), channel_id=1, replica_groups=mesh['plane'=8,'far'=2,'near'=2,'core'=2,'tp'=4] {'far','tp'}, dimensions={0} | all-to-all | bytes 2097152 | tf_op jit(solution)/shard_map/all_to_all | solution.py:527
  140.6 0.1 convert_reduce_fusion
  140.7 0.7 add_convert_fusion
  (1 shorter events, 0.0 us)
Async XLA Ops:
  6.5 44.6 %copy-start = (bf16[128,2048]{1,0:T(8,128)(2,1)S(1)}, bf16[128,2048]{1,0:T(8,128)(2,1)}, u32[]{:S(2)}) copy-start(bf16[128,2048]{1,0:T(8,128)(2,1)} %param.15) | copy-start | bytes 1572868
  6.5 109.3 %all-gather.2.cloned.1.call-start = ((), (), s32[]{:S(2)}) async-start(), calls=%async_computation.6 | async-start | bytes 9732096 | tf_op jit(solution)/shard_map/all_gather | solution.py:492
  8.3 7.4 %collective-permute-start = (bf16[32,2304]{1,0:T(8,128)(2,1)}, bf16[32,2304]{1,0:T(8,128)(2,1)S(1)}, u32[]{:S(2)}, u32[]{:S(2)}) collective-permute-start(bf16[32,2304]{1,0:T(8,128)(2,1)} %get-tuple-element.60), channel_id=1, source_target_pairs={{0,16},{16,0},{1,17},{17,1},{2,18},{18,2},{3,19},{19,3},{4,20},{20... | collective-permute-start | bytes 442376 | tf_op jit(solution)/shard_map/ppermute | solution.py:486
  39.5 27.7 %all-to-all-start.1 = ((bf16[8,192,128]{2,1,0:T(8,128)(2,1)}), bf16[8,192,128]{2,1,0:T(8,128)(2,1)S(1)}, u32[]{:S(2)}, u32[]{:S(2)}) async-start(bf16[8,192,128]{2,1,0:T(8,128)(2,1)} %get-tuple-element.41), calls=%async_computation.1 | async-start | bytes 786432 | tf_op jit(solution)/shard_map/all_to_all | solution.py:527
  96.2 19.6 %copy-start.1 = (f32[2048]{0:T(1024)S(1)}, f32[2048]{0:T(1024)}, u32[]{:S(2)}) copy-start(f32[2048]{0:T(1024)} %param.26) | copy-start | bytes 24580
Sparse Core Ops, SparseCore 0:
  16.5 84.1 all-gather.1

commit v14 on v13

--- a/solution.py
+++ b/solution.py
@@ -575,7 +575,7 @@
     )(*inputs)
     place = lax.axis_index(PLANE).astype(jnp.int32).reshape(1)
     first_column = (lax.axis_index(TP) * columns).astype(jnp.uint32)
-    send, place, first_column = lax.optimization_barrier((send, place, first_column))
+    send, taken, place, first_column = lax.optimization_barrier((send, taken, place, first_column))
     whole = gathered(kept, taken)
     planes = lax.axis_size(PLANE)
     prefix, total = call(

time: 149 us -> 143 us (0.960)
  waiting for transfers between devices: 21.1 us -> 16.4 us
    ppermute x1, waiting for transfers between devices: 5.18 us -> 0.01 us  [swapped(): return (kept, lax.ppermute(given, FAR, [(0, 1), (1, 0)]))]
  transfers between devices with their start and end apart: 3 -> 3, of which waited for: 2 -> 1; matrix products, arithmetic and copies ran while one was open for 0% -> 0% of each run, Pallas kernels for 10% -> 11%
where the time goes in v14:
time: 143 us; the launch traced here: 142 us
  blocking collectives  76.3 us (53%)
  Pallas kernels  23.8 us (17%)
  waiting for transfers between devices  16.4 us (11%)
  between operations  13.5 us (9%)
  starting transfers between devices  10.6 us (7%)
    all_to_all x5, blocking collectives, exchange(): return lax.all_to_all(value, axis, 0, 0, tiled=True)  76.3 us
    all_to_all x1, waiting for transfers between devices, exchange(): return lax.all_to_all(value, axis, 0, 0, tiled=True)  16.4 us
    all_to_all x1, starting transfers between devices, exchange(): return lax.all_to_all(value, axis, 0, 0, tiled=True)  8.34 us
    pallas_call x1, Pallas kernels, feed_forward(): pl.pallas_call(feed_kernel, out_shape=array((shares, tokens, columns), bf...  6.73 us
    pallas_call x1, Pallas kernels, on_device(): call(solve_kernel, (array((SHARES, LANES + HALF, LANES), bf16), pairs, pa...  6.46 us
    pallas_call x1, Pallas kernels, on_device(): call(mix_kernel, (array((features // columns, TOK, columns), bf16),), [HB...  3.23 us
  transfers between devices with their start and end apart: 3, of which 1 were waited for; matrix products, arithmetic and copies ran while one was open for 0% of the time, Pallas kernels for 11%

profile of v14, /device:TPU:2, one launch (start us, length us, event | category | flops | bytes accessed | tf_op | source)
XLA Modules:
  0.0 142.3 jit_solution(1914465580269182076)
XLA Ops:
  6.5 0.0 copy-start
  6.5 0.0 all-gather.2.cloned.1.call-start
  6.5 1.8 %shard_map.146 = (bf16[64,2304]{1,0:T(8,128)(2,1)}, bf16[32,2304]{1,0:T(8,128)(2,1)}) custom-call(s32[1]{0:T(128)} %bitcast.far_ref, bf16[32,1408]{1,0:T(8,128)(2,1)} %refs_0_.3, bf16[32,1408]{1,0:T(8,128)(2,1)} %refs_1_.3, bf16[32,1408]{1,0:T(8,128)(2,1)} %bitcast.9), custom_call_target="tpu_custom_call" | custom-call | tf_op jit(solution)/shard_map/pallas_call | solution.py:485
  8.3 2.2 %collective-permute-start = (bf16[32,2304]{1,0:T(8,128)(2,1)}, bf16[32,2304]{1,0:T(8,128)(2,1)S(1)}, u32[]{:S(2)}, u32[]{:S(2)}) collective-permute-start(bf16[32,2304]{1,0:T(8,128)(2,1)} %get-tuple-element.35), channel_id=1, source_target_pairs={{0,16},{16,0},{1,17},{17,1},{2,18},{18,2},{3,19},{19,3},{4,20},{20... | collective-permute-start | bytes 442376 | tf_op jit(solution)/shard_map/ppermute | solution.py:486
  10.5 6.5 %shard_map.145 = (bf16[8,192,128]{2,1,0:T(8,128)(2,1)}, bf16[6,128,128]{2,1,0:T(8,128)(2,1)}, bf16[6,128,128]{2,1,0:T(8,128)(2,1)}, bf16[4,128,256]{2,1,0:T(8,128)(2,1)}, f32[4,128,128]{2,1,0:T(8,128)}) custom-call(bf16[2,128,256]{2,1,0:T(8,128)(2,1)} %refs_4_.3, bf16[2,128,256]{2,1,0:T(8,128)(2,1)} %refs_5_.3, bf16[2,128,256]{2,1,0:T(8,128)(2,1)} %refs_6_.1, ...), custom_call_target="tpu_custom_call" | custom-call | tf_op jit(solution)/shard_map/pallas_call | solution.py:567
  17.0 0.0 collective-permute-done
  17.0 0.7 constant_dynamic-update-slice_fusion
  17.7 0.0 all-gather.2.cloned.1.call-update
  17.7 12.4 %all_to_all.30.got_ref = bf16[8,192,128]{2,1,0:T(8,128)(2,1)S(1)} all-to-all(bf16[8,192,128]{2,1,0:T(8,128)(2,1)} %get-tuple-element.36), channel_id=1, replica_groups=mesh['plane'=8,'far'=2,'near'=2,'core'=2,'tp'=4] {'far','near','core'}, dimensions={0} | all-to-all | bytes 786432 | tf_op jit(solution)/shard_map/all_to_all | solution.py:527
  30.1 1.7 %shard_map.147 = (f32[8,192,128]{2,1,0:T(8,128)S(1)}, bf16[8,192,128]{2,1,0:T(8,128)(2,1)}) custom-call(bf16[8,192,128]{2,1,0:T(8,128)(2,1)S(1)} %all_to_all.30.got_ref), custom_call_target="tpu_custom_call" | custom-call | tf_op jit(solution)/shard_map/pallas_call | solution.py:581
  31.8 8.3 %all-to-all-start.1 = ((bf16[8,192,128]{2,1,0:T(8,128)(2,1)}), bf16[8,192,128]{2,1,0:T(8,128)(2,1)S(1)}, u32[]{:S(2)}, u32[]{:S(2)}) async-start(bf16[8,192,128]{2,1,0:T(8,128)(2,1)} %get-tuple-element.43), calls=%async_computation.1 | async-start | bytes 786432 | tf_op jit(solution)/shard_map/all_to_all | solution.py:527
  40.1 2.8 %shard_map.148 = (f32[4,128,128]{2,1,0:T(8,128)}, bf16[4,128,256]{2,1,0:T(8,128)(2,1)}, f32[4,128,128]{2,1,0:T(8,128)}, f32[4,128,128]{2,1,0:T(8,128)}) custom-call(bf16[6,128,128]{2,1,0:T(8,128)(2,1)} %get-tuple-element.45.refs_0_, bf16[6,128,128]{2,1,0:T(8,128)(2,1)} %get-tuple-element.46.refs_1_, bf16[4,128,256]{2,1,0:T(8,128)(2,1)} %get-tuple-element.47.refs_2_, ...), custom_call_target="tpu_custom_call" | custom-call | tf_op jit(solution)/shard_map/pallas_call | solution.py:597
  42.9 0.0 copy-done
  42.9 0.1 constant_dynamic-slice_fusion
  43.0 16.4 %all-to-all-done.1.every_ref = bf16[8,192,128]{2,1,0:T(8,128)(2,1)S(1)} async-done(((bf16[8,192,128]{2,1,0:T(8,128)(2,1)}), bf16[8,192,128]{2,1,0:T(8,128)(2,1)S(1)}, u32[]{:S(2)}, u32[]{:S(2)}) %all-to-all-start.1) | async-done | bytes 393248 | tf_op jit(solution)/shard_map/all_to_all | solution.py:527
  59.4 1.1 shard_map.149
  60.5 10.6 %all_to_all.31.refs_0_ = bf16[8,64,128]{2,1,0:T(8,128)(2,1)} all-to-all(bf16[8,64,128]{2,1,0:T(8,128)(2,1)S(1)} %shard_map.149), channel_id=1, replica_groups=mesh['plane'=8,'far'=2,'near'=2,'core'=2,'tp'=4] {'far','near','core'}, dimensions={0} | all-to-all | bytes 262144 | tf_op jit(solution)/shard_map/all_to_all | solution.py:527
  71.2 3.2 %shard_map.150 = bf16[4,128,512]{2,1,0:T(8,128)(2,1)} custom-call(bf16[8,64,128]{2,1,0:T(8,128)(2,1)} %all_to_all.31.refs_0_, f32[4,128,128]{2,1,0:T(8,128)} %get-tuple-element.57.refs_1_, bf16[4,128,256]{2,1,0:T(8,128)(2,1)} %get-tuple-element.58.refs_2_, f32[4,128,128]{2,1,0:T(8,128)} %get-tuple-element.59.refs_3_, ...), custom_call_target="tpu_custom_call" | custom-call | tf_op jit(solution)/shard_map/pallas_call | solution.py:613
  74.4 13.5 %all_to_all.32 = bf16[4,128,512]{2,1,0:T(8,128)(2,1)S(1)} all-to-all(bf16[4,128,512]{2,1,0:T(8,128)(2,1)} %shard_map.150), channel_id=1, replica_groups=mesh['plane'=8,'far'=2,'near'=2,'core'=2,'tp'=4] {'tp'}, dimensions={0} | all-to-all | bytes 1048576 | tf_op jit(solution)/shard_map/all_to_all | solution.py:527
  87.9 0.1 convert_reduce_fusion.1
  88.0 0.0 copy-start.1
  88.0 0.1 broadcast_in_dim.2
  88.1 21.6 %all_to_all.33.x_ref = bf16[8,128,512]{2,1,0:T(8,128)(2,1)S(1)} all-to-all(bf16[8,128,512]{2,1,0:T(8,128)(2,1)S(1)} %broadcast_in_dim.2), channel_id=1, replica_groups=mesh['plane'=8,'far'=2,'near'=2,'core'=2,'tp'=4] {'far','tp'}, dimensions={0} | all-to-all | bytes 2097152 | tf_op jit(solution)/shard_map/all_to_all | solution.py:527
  109.7 0.0 all-gather.2.cloned.1.call-done
  109.7 0.0 copy-done.1
  109.7 6.7 %shard_map.151 = bf16[8,128,512]{2,1,0:T(8,128)(2,1)S(1)} custom-call(s32[1]{0:T(128)} %bitcast.far_ref, bf16[8,128,512]{2,1,0:T(8,128)(2,1)S(1)} %all_to_all.33.x_ref, f32[1,2048]{1,0:T(1,128)S(1)} %bitcast.6, bf16[8,4,2,32,2304]{4,3,2,1,0:T(8,128)(2,1)} %bitcast.7), custom_call_target="tpu_custom_call" | custom-call | tf_op jit(solution)/shard_map/pallas_call | solution.py:430
  116.5 18.2 %all_to_all.34 = bf16[8,128,512]{2,1,0:T(8,128)(2,1)S(1)} all-to-all(bf16[8,128,512]{2,1,0:T(8,128)(2,1)S(1)} %shard_map.151), channel_id=1, replica_groups=mesh['plane'=8,'far'=2,'near'=2,'core'=2,'tp'=4] {'far','tp'}, dimensions={0} | all-to-all | bytes 2097152 | tf_op jit(solution)/shard_map/all_to_all | solution.py:527
  134.7 0.1 convert_reduce_fusion
  134.8 0.7 add_convert_fusion
  (1 shorter events, 0.0 us)
Async XLA Ops:
  6.5 36.4 %copy-start = (bf16[128,2048]{1,0:T(8,128)(2,1)S(1)}, bf16[128,2048]{1,0:T(8,128)(2,1)}, u32[]{:S(2)}) copy-start(bf16[128,2048]{1,0:T(8,128)(2,1)} %param.15) | copy-start | bytes 1572868
  6.5 103.2 %all-gather.2.cloned.1.call-start = ((), (), s32[]{:S(2)}) async-start(), calls=%async_computation.6 | async-start | bytes 9732096 | tf_op jit(solution)/shard_map/all_gather | solution.py:492
  8.3 8.7 %collective-permute-start = (bf16[32,2304]{1,0:T(8,128)(2,1)}, bf16[32,2304]{1,0:T(8,128)(2,1)S(1)}, u32[]{:S(2)}, u32[]{:S(2)}) collective-permute-start(bf16[32,2304]{1,0:T(8,128)(2,1)} %get-tuple-element.35), channel_id=1, source_target_pairs={{0,16},{16,0},{1,17},{17,1},{2,18},{18,2},{3,19},{19,3},{4,20},{20... | collective-permute-start | bytes 442376 | tf_op jit(solution)/shard_map/ppermute | solution.py:486
  31.8 27.6 %all-to-all-start.1 = ((bf16[8,192,128]{2,1,0:T(8,128)(2,1)}), bf16[8,192,128]{2,1,0:T(8,128)(2,1)S(1)}, u32[]{:S(2)}, u32[]{:S(2)}) async-start(bf16[8,192,128]{2,1,0:T(8,128)(2,1)} %get-tuple-element.43), calls=%async_computation.1 | async-start | bytes 786432 | tf_op jit(solution)/shard_map/all_to_all | solution.py:527
  88.0 21.7 %copy-start.1 = (f32[2048]{0:T(1024)S(1)}, f32[2048]{0:T(1024)}, u32[]{:S(2)}) copy-start(f32[2048]{0:T(1024)} %param.26) | copy-start | bytes 24580
Sparse Core Ops, SparseCore 0:
  17.8 83.2 all-gather.1
